TPU v7x, 32 devices: a whole 2x2x4 slice. The times are simulated.
32 devices in a mesh: sp: 8 (over z, y), tp: 4 (over x, core).
Axes of the slice: x: 2, y: 2, z: 4, core: 2. Of those that a mesh axis runs over, the one named last changes fastest.
Arguments:
- q_proj: bfloat16 [4096, 1024], P('sp', 'tp'), may hold values from -5.25 to 5.25
- k_proj: bfloat16 [4096, 512], P('sp', 'tp'), may hold values from -5.25 to 5.25
- v_proj: bfloat16 [4096, 512], P('sp', 'tp'), may hold values from -6 to 6
- doc_ids: int32 [4096], P('sp'), may hold values from 0 to 3, never falling along the last dimension, each value on 1 to 2048 neighbouring positions
- sinks: float32 [16], P('tp'), may hold values from 0.5 to 5.5
- resid: bfloat16 [4096, 2048], P(('sp', 'tp')), may hold values from -12 to 12
- w_out: bfloat16 [1024, 2048], P('tp'), may hold values from -4 to 4
- norm_gain: float32 [2048], replicated, may hold values from 0.1 to 1.9
- w_gate: bfloat16 [2048, 5632], P('sp', 'tp'), may hold values from -0.125 to 0.125
- w_up: bfloat16 [2048, 5632], P('sp', 'tp'), may hold values from -0.125 to 0.125
- w_down: bfloat16 [5632, 2048], P('tp', 'sp'), may hold values from -0.078125 to 0.078125
Outputs:
- layer_out: bfloat16 [4096, 2048], P(('sp', 'tp'))
Inputs may be any that keep to these rules, and one draw needn't show every extreme that they name: `doc_ids`: document numbers never fall along the sequence; each document covers at most 2048 positions and one covers exactly that many.
All inputs are finite; a program needn't handle non-finite values.
Results may differ from a plain program's by a relative error of at most 0.015.
Values may be sent and summed in bfloat16 or wider, within the bound.
No kernel may reach another device: no remote copies, remote signals or barrier semaphores. Data moves between devices by JAX's collectives and lax.ppermute only.
A program may use at most 64 MiB of HBM per device.

v0:
```python
import functools

import jax
import jax.numpy as jnp
from jax import lax
from jax.experimental import pallas as pl
from jax.experimental.pallas import tpu as pltpu
from jax.sharding import PartitionSpec as P


HEAD = 64
WINDOW = 128

norm_eps = 1e-06
masked = -1e30


def swap(block, sp_mask=0, tp_mask=0):
    n_sp, n_tp = lax.axis_size("sp"), lax.axis_size("tp")
    if sp_mask and tp_mask:
        axis = ("sp", "tp")
        pairs = [
            (s * n_tp + t, (s ^ sp_mask) * n_tp + (t ^ tp_mask))
            for s in range(n_sp)
            for t in range(n_tp)
        ]
    elif sp_mask:
        axis, pairs = "sp", [(s, s ^ sp_mask) for s in range(n_sp)]
    elif tp_mask:
        axis, pairs = "tp", [(t, t ^ tp_mask) for t in range(n_tp)]
    else:
        return block
    return lax.ppermute(block, axis, pairs)


def edges(block, width):
    count = lax.axis_size("sp")
    forward = [(i, i + 1) for i in range(count - 1)]
    backward = [(b, a) for a, b in forward]
    low = lax.ppermute(block[block.shape[0] - width :], "sp", forward)
    high = lax.ppermute(block[:width], "sp", backward)
    return low, high


def attention_kernel(sinks_ref, docs_ref, q_ref, k_ref, v_ref, low_ref, high_ref, out_ref):
    kv_cols = k_ref.shape[1]
    kv_heads = kv_cols // HEAD
    groups = q_ref.shape[1] // kv_cols
    count = q_ref.shape[0] // WINDOW
    span = 3 * WINDOW
    shape = (WINDOW, span)
    offset = lax.broadcasted_iota(jnp.int32, shape, 1) - lax.broadcasted_iota(jnp.int32, shape, 0)
    near = (offset >= 0) & (offset <= 2 * WINDOW)

    def band(own_ref, column, block):
        pieces = []
        for i in range(block - 1, block + 2):
            if i < 0:
                pieces.append(low_ref[:, column : column + kv_cols])
            elif i == count:
                pieces.append(high_ref[:, column : column + kv_cols])
            else:
                pieces.append(own_ref[i * WINDOW : (i + 1) * WINDOW, :])
        return jnp.concatenate(pieces, axis=0)

    for block in range(count):
        rows = slice(block * WINDOW, (block + 1) * WINDOW)
        own_docs = docs_ref[:, (block + 1) * WINDOW : (block + 2) * WINDOW]
        query_docs = jnp.broadcast_to(own_docs, (WINDOW, WINDOW)).T
        band_docs = docs_ref[:, block * WINDOW : block * WINDOW + span]
        valid = near & (jnp.concatenate([query_docs] * 3, axis=1) == band_docs)
        keys, values = band(k_ref, 0, block), band(v_ref, kv_cols, block)
        outs = []
        for head in range(kv_heads):
            cols = slice(head * HEAD, (head + 1) * HEAD)
            for group in range(groups):
                index = head * groups + group
                query = q_ref[rows, index * HEAD : (index + 1) * HEAD]
                scores = lax.dot_general(
                    query, keys[:, cols], (((1,), (1,)), ((), ())), preferred_element_type=jnp.float32
                ) * HEAD ** (-0.5)
                scores = jnp.where(valid, scores, masked)
                sink = sinks_ref[index]
                top = jnp.maximum(jnp.max(scores, axis=-1, keepdims=True), sink)
                expd = jnp.exp(scores - top)
                total = jnp.sum(expd, axis=-1, keepdims=True) + jnp.exp(sink - top)
                probs = (expd * (1.0 / total)).astype(jnp.bfloat16)
                outs.append(jnp.dot(probs, values[:, cols], preferred_element_type=jnp.float32))
        out_ref[rows, :] = jnp.concatenate(outs, axis=1).astype(jnp.bfloat16)


def attention(q_proj, k_proj, v_proj, doc_ids, sinks):
    tok_rows = q_proj.shape[0]
    kv = jnp.concatenate([k_proj, v_proj], axis=1)
    kv_low, kv_high = edges(kv, WINDOW)
    doc_low, doc_high = edges(doc_ids, WINDOW)
    docs = jnp.concatenate([doc_low, doc_ids, doc_high], axis=0)
    positions = (
        lax.axis_index("sp") * tok_rows
        - WINDOW
        + jnp.arange(tok_rows + 2 * WINDOW, dtype=jnp.int32)
    )
    inside = (positions >= 0) & (positions < tok_rows * lax.axis_size("sp"))
    docs = jnp.where(inside, docs, -1)[None, :]
    return pl.pallas_call(
        attention_kernel,
        out_shape=jax.ShapeDtypeStruct(q_proj.shape, jnp.bfloat16),
        in_specs=[SMEM] + [VMEM] * 6,
        out_specs=VMEM,
        cost_estimate=pl.CostEstimate(
            flops=12 * tok_rows * WINDOW * q_proj.shape[1],
            bytes_accessed=1 << 20,
            transcendentals=0,
        ),
    )(sinks, docs, q_proj, k_proj, v_proj, kv_low, kv_high)


SMEM = pl.BlockSpec(memory_space=pltpu.SMEM)
VMEM = pl.BlockSpec(memory_space=pltpu.VMEM)
ANY = pl.BlockSpec(memory_space=pl.ANY)


def project_kernel(count, resid_ref, gain_ref, *refs):
    heads, weights, (middle_ref, normed_ref) = refs[:count], refs[count : 2 * count], refs[2 * count :]
    width = middle_ref.shape[1]
    tile = min(512, width)
    squares = jnp.zeros((middle_ref.shape[0], 1), jnp.float32)
    for lower in range(0, width, tile):
        cols = pl.ds(lower, tile)
        total = resid_ref[:, cols].astype(jnp.float32)
        for head, weight in zip(heads, weights):
            total += jnp.dot(head[...], weight[:, cols], preferred_element_type=jnp.float32)
        middle_ref[:, cols] = total
        squares += jnp.sum(total * total, axis=-1, keepdims=True)
    factor = lax.rsqrt(squares / width + norm_eps)
    for lower in range(0, width, tile):
        cols = pl.ds(lower, tile)
        normed_ref[:, cols] = (middle_ref[:, cols] * factor * gain_ref[:, cols]).astype(jnp.bfloat16)


def project(resid, gain, heads, weights):
    rows, width = resid.shape
    count = len(heads)
    return pl.pallas_call(
        functools.partial(project_kernel, count),
        out_shape=(
            jax.ShapeDtypeStruct((rows, width), jnp.float32),
            jax.ShapeDtypeStruct((rows, width), jnp.bfloat16),
        ),
        in_specs=[VMEM] * (2 + 2 * count),
        out_specs=(VMEM, VMEM),
        cost_estimate=pl.CostEstimate(
            flops=2 * rows * width * count * heads[0].shape[1], bytes_accessed=6 << 20, transcendentals=0
        ),
    )(resid, gain, *heads, *weights)


def hidden_kernel(n_rows, n_parts, starts_ref, *refs):
    row_refs, part_refs = refs[:n_rows], refs[n_rows : n_rows + n_parts]
    hidden_ref, rows, weight, row_sems, part_sems = refs[n_rows + n_parts :]
    copies = []
    height = row_refs[0].shape[0]
    for i, ref in enumerate(row_refs):
        copies.append(pltpu.make_async_copy(ref, rows.at[pl.ds(i * height, height)], row_sems.at[i]))
    for i, ref in enumerate(part_refs):
        start = pl.multiple_of(starts_ref[i], ref.shape[0])
        copies.append(pltpu.make_async_copy(ref, weight.at[pl.ds(start, ref.shape[0])], part_sems.at[i]))
    for copy in copies[n_rows:] + copies[:n_rows]:
        copy.start()
    for copy in copies[n_rows:]:
        copy.wait()
    half = hidden_ref.shape[1]
    tile = min(256, rows.shape[0])
    for lower in range(0, rows.shape[0], tile):
        for i in range(lower // height, (lower + tile) // height):
            copies[i].wait()
        both = jnp.dot(rows[pl.ds(lower, tile), :], weight[...], preferred_element_type=jnp.float32)
        gate, up = both[:, :half], both[:, half:]
        hidden_ref[pl.ds(lower, tile), :] = (gate / (1.0 + jnp.exp(-gate)) * up).astype(jnp.bfloat16)


def hidden_units(starts, row_blocks, parts):
    rows = sum(block.shape[0] for block in row_blocks)
    depth, width = row_blocks[0].shape[1], parts[0].shape[1]
    return pl.pallas_call(
        functools.partial(hidden_kernel, len(row_blocks), len(parts)),
        out_shape=jax.ShapeDtypeStruct((rows, width // 2), jnp.bfloat16),
        in_specs=[SMEM] + [ANY] * (len(row_blocks) + len(parts)),
        out_specs=VMEM,
        scratch_shapes=[
            pltpu.VMEM((rows, depth), jnp.bfloat16),
            pltpu.VMEM((depth, width), jnp.bfloat16),
            pltpu.SemaphoreType.DMA((len(row_blocks),)),
            pltpu.SemaphoreType.DMA((len(parts),)),
        ],
        cost_estimate=pl.CostEstimate(
            flops=2 * rows * width * depth, bytes_accessed=11 << 20, transcendentals=rows * width // 2
        ),
        compiler_params=pltpu.CompilerParams(vmem_limit_bytes=40 << 20),
    )(starts, *row_blocks, *parts)


def down_kernel(n_parts, starts_ref, hidden_ref, *refs):
    part_refs, (keep_ref, send_ref, weight, sems) = refs[:n_parts], refs[n_parts:]
    copies = []
    for i, ref in enumerate(part_refs):
        start = pl.multiple_of(starts_ref[i], ref.shape[1]) if n_parts > 1 else 0
        copies.append(pltpu.make_async_copy(ref, weight.at[:, pl.ds(start, ref.shape[1])], sems.at[i]))
    for copy in copies:
        copy.start()
    for copy in copies:
        copy.wait()
    keep = keep_ref.shape[0]
    tile = min(256, keep)
    for target, base in ((send_ref, keep), (keep_ref, 0)):
        for lower in range(0, keep, tile):
            target[pl.ds(lower, tile), :] = jnp.dot(
                hidden_ref[pl.ds(base + lower, tile), :], weight[...], preferred_element_type=jnp.float32
            ).astype(jnp.bfloat16)


def down_rows(starts, hidden, parts):
    rows, depth = hidden.shape
    width = sum(part.shape[1] for part in parts)
    shape = jax.ShapeDtypeStruct((rows // 2, width), jnp.bfloat16)
    return pl.pallas_call(
        functools.partial(down_kernel, len(parts)),
        out_shape=(shape, shape),
        in_specs=[SMEM, VMEM] + [ANY] * len(parts),
        out_specs=(VMEM, VMEM),
        scratch_shapes=[
            pltpu.VMEM((depth, width), jnp.bfloat16),
            pltpu.SemaphoreType.DMA((len(parts),)),
        ],
        cost_estimate=pl.CostEstimate(
            flops=2 * rows * width * depth, bytes_accessed=4 << 20, transcendentals=0
        ),
        compiler_params=pltpu.CompilerParams(vmem_limit_bytes=24 << 20),
    )(starts, hidden, *parts)


def finish_kernel(plan, per_chunk, bases_ref, middle_ref, *refs):
    out_ref = refs[-1]
    for chunk, (strips, pitch, shift) in enumerate(plan):
        totals = refs[chunk * per_chunk : (chunk + 1) * per_chunk]
        width = totals[0].shape[1] // strips
        for strip in range(strips):
            start = bases_ref[chunk] + (strip * pitch + shift)
            cols = pl.ds(pl.multiple_of(start, width), width)
            total = middle_ref[:, cols]
            for ref in totals:
                total += ref[:, strip * width : (strip + 1) * width].astype(jnp.float32)
            out_ref[:, cols] = total.astype(jnp.bfloat16)


def finish(plan, bases, middle, chunks):
    return pl.pallas_call(
        functools.partial(finish_kernel, plan, len(chunks[0])),
        out_shape=jax.ShapeDtypeStruct(middle.shape, jnp.bfloat16),
        in_specs=[SMEM] + [VMEM] * (1 + len(chunks) * len(chunks[0])),
        out_specs=VMEM,
        cost_estimate=pl.CostEstimate(
            flops=8 * middle.size, bytes_accessed=8 * middle.size, transcendentals=0
        ),
    )(bases, middle, *[block for chunk in chunks for block in chunk])


def lay_out(parts, starts, axis):
    total = sum(part.shape[axis] for part in parts)
    shape = list(parts[0].shape)
    shape[axis] = total
    whole = jnp.zeros(shape, parts[0].dtype)
    for part, start in zip(parts, starts):
        whole = lax.dynamic_update_slice_in_dim(whole, part, start, axis)
    return whole


def y_count(n_sp):
    return 1 << ((n_sp.bit_length() - 1) // 2)


def shards(q_proj, k_proj, v_proj, doc_ids, sinks, resid, w_out, norm_gain, w_gate, w_up, w_down):
    n_sp, n_tp = lax.axis_size("sp"), lax.axis_size("tp")
    n_y = y_count(n_sp)
    n_z = n_sp // n_y
    sp, tp = lax.axis_index("sp"), lax.axis_index("tp")
    z = sp // n_y
    half = w_gate.shape[1] // 2
    depth = w_gate.shape[0]
    piece = w_down.shape[1]

    lower = jnp.concatenate([w_gate[:, :half], w_up[:, :half]], axis=1)
    upper = jnp.concatenate([w_gate[:, half:], w_up[:, half:]], axis=1)
    first = z % 2 == 0
    gu_half = (jnp.where(first, lower, upper), jnp.where(first, upper, lower))
    down_half = (
        jnp.where(first, w_down[:half], w_down[half:]),
        jnp.where(first, w_down[half:], w_down[:half]),
    )

    gu_parts, gu_starts = [], []
    for dz in range(n_z):
        cuts = 1 if dz < 2 else 2
        height = depth // cuts
        for cut in range(cuts):
            held = swap(gu_half[dz % 2][cut * height : (cut + 1) * height], dz * n_y)
            for dy in range(n_y):
                gu_parts.append(swap(held, dy))
                gu_starts.append((sp ^ (dz * n_y + dy)) * depth + cut * height)
    down, cuts_of = {}, {}
    for dz in range(n_z):
        cuts = cuts_of[dz // 2] = 2 if dz >= 2 and piece % 256 == 0 else 1
        width = piece // cuts
        for cut in range(cuts):
            held = swap(down_half[dz % 2][:, cut * width : (cut + 1) * width], dz * n_y)
            for dy in range(n_y):
                down[dz, cut, dy] = swap(held, dy)

    attended = attention(q_proj, k_proj, v_proj, doc_ids, sinks)

    out_blocks = {}
    for t in range(0, n_tp, 2):
        out_blocks[t] = swap(w_out, 0, t)
        out_blocks[t + 1] = swap(out_blocks[t], 0, 1)
    own_rows = q_proj.shape[0] // n_tp
    heads = [swap(lax.dynamic_slice_in_dim(attended, (tp ^ t) * own_rows, own_rows, 0), 0, t) for t in range(n_tp)]
    middle, normed = project(
        resid, norm_gain[None, :], heads, [out_blocks[t] for t in range(n_tp)]
    )

    rows = {(0, 0): normed, (1, 0): swap(normed, n_y)}
    for t in range(2, n_tp, 2):
        for a in (0, 1):
            rows[a, t] = swap(rows[a, 0], 0, t)
    for (a, t), block in list(rows.items()):
        rows[a, t + 1] = swap(block, 0, 1)
    order = [(a, t + c) for c in (0, 1) for a in (0, 1) for t in range(0, n_tp, 2)]

    hidden = hidden_units(
        jnp.stack(gu_starts).astype(jnp.int32), [rows[key] for key in order], gu_parts
    )

    plan, bases, chunks = [], [], []
    span = 2 * n_y * piece
    for pair, cuts in cuts_of.items():
        width = piece // cuts
        for cut in range(cuts):
            keys = [(2 * pair + b, dy) for b in (0, 1) for dy in range(n_y)]
            starts = [((sp ^ (dz * n_y + dy)) % (2 * n_y)) * width for dz, dy in keys]
            parts = [down[dz, cut, dy] for dz, dy in keys]
            if width % 128:
                parts, starts = [lay_out(parts, starts, 1)], [sp * 0]
            keep, send = down_rows(jnp.stack(starts).astype(jnp.int32), hidden, parts)
            other = swap(send, 0, 1)
            total = (keep.astype(jnp.float32) + other.astype(jnp.float32)).astype(jnp.bfloat16)
            plan.append((1, span, 0) if cuts == 1 else (2 * n_y, piece, cut * width))
            bases.append((z // 2 ^ pair) * span)
            chunks.append(
                [
                    swap(total[i * own_rows : (i + 1) * own_rows], a * n_y, t)
                    for i, (a, t) in enumerate(order[: len(order) // 2])
                ]
            )
    return finish(tuple(plan), jnp.stack(bases).astype(jnp.int32), middle, chunks)


def solution(mesh):
    placed = (
        P("sp", "tp"),
        P("sp", "tp"),
        P("sp", "tp"),
        P("sp"),
        P("tp"),
        P(("sp", "tp"), None),
        P("tp", None),
        P(),
        P("sp", "tp"),
        P("sp", "tp"),
        P("tp", "sp"),
    )

    return jax.shard_map(shards, mesh=mesh, in_specs=placed, out_specs=P(("sp", "tp"), None), check_vma=False)
```

profile of v0, /device:TPU:0, one launch (start us, length us, event | category | flops | bytes accessed | tf_op | source)
XLA Modules:
  0.0 263.8 jit_solution(17164501366622543023)
XLA Ops:
  0.5 2.5 collective-permute-start.8
  5.0 4.5 %collective-permute-start = (s32[128]{0:T(128)S(1)}, s32[128]{0:T(128)S(1)}, u32[]{:S(2)}, u32[]{:S(2)}) collective-permute-start(s32[128]{0:T(128)S(1)} %get-tuple-element.55), channel_id=1, source_target_pairs={{0,4},{4,8},{8,12},{12,16},{16,20},{20,24},{24,28},{1,5},{5,9},{9,... | collective-permute-start | bytes 1544 | tf_op jit(solution)/shard_map/ppermute | solution.py:40
  11.6 4.3 %collective-permute-start.2 = (bf16[128,256]{1,0:T(8,128)(2,1)S(1)}, bf16[128,256]{1,0:T(8,128)(2,1)S(1)}, u32[]{:S(2)}, u32[]{:S(2)}) collective-permute-start(bf16[128,256]{1,0:T(8,128)(2,1)S(1)} %get-tuple-element.54), channel_id=1, source_target_pairs={{0,4},{4,8},{8,12},{12,16},{16,20},{20,24},{24,28},{1,5},{5,9},{9,... | collective-permute-start | bytes 196616 | tf_op jit(solution)/shard_map/ppermute | solution.py:40
  20.3 3.8 %collective-permute-start.35 = (bf16[704,128]{1,0:T(8,128)(2,1)S(1)}, bf16[704,128]{1,0:T(8,128)(2,1)S(1)}, u32[]{:S(2)}, u32[]{:S(2)}) collective-permute-start(bf16[704,128]{1,0:T(8,128)(2,1)S(1)} %get-tuple-element.48), channel_id=1, source_target_pairs={{0,16},{4,20},{8,24},{12,28},{16,0},{20,4},{24,8},{28,12},{1,17},{... | collective-permute-start | bytes 540680 | tf_op jit(solution)/shard_map/ppermute | solution.py:33
  26.0 7.7 %shard_map.109 = bf16[512,256]{1,0:T(8,128)(2,1)} custom-call(f32[4]{0:T(128)} %sinks_ref.1, s32[1,768]{1,0:T(1,128)} %and_select_fusion.docs_ref, bf16[512,256]{1,0:T(8,128)(2,1)} %q_ref.1, bf16[512,128]{1,0:T(8,128)(2,1)} %k_ref.1, bf16[512,128]{1,0:T(8,128)(2,1)} %v_ref.1, bf16[128,256]{1,0:T(8,128)(2,1)} %copy-done.38, bf16[128,256]{1,0:T(8,128)(2,1)} %copy-done.39), custom_call_target="tpu_custom_call" | custom-call | flops 201326592 | bytes 1048576 | tf_op jit(solution)/shard_map/pallas_call | solution.py:105
  38.7 2.8 %collective-permute-done.5.refs_2_ = bf16[128,256]{1,0:T(8,128)(2,1)S(1)} collective-permute-done((bf16[128,256]{1,0:T(8,128)(2,1)S(1)}, bf16[128,256]{1,0:T(8,128)(2,1)S(1)}, u32[]{:S(2)}, u32[]{:S(2)}) %collective-permute-start.5) | collective-permute-done | bytes 65568 | tf_op jit(solution)/shard_map/ppermute | solution.py:33
  41.5 4.9 %collective-permute-start.20 = (bf16[128,1408]{1,0:T(8,128)(2,1)S(1)}, bf16[128,1408]{1,0:T(8,128)(2,1)S(1)}, u32[]{:S(2)}, u32[]{:S(2)}) collective-permute-start(bf16[128,1408]{1,0:T(8,128)(2,1)S(1)} %get-tuple-element.32), channel_id=1, source_target_pairs={{0,16},{4,20},{8,24},{12,28},{16,0},{20,4},{24,8},{28,12},{1,17},{... | collective-permute-start | bytes 1081352 | tf_op jit(solution)/shard_map/ppermute | solution.py:33
  48.0 16.1 %collective-permute-done.37.refs_2_ = bf16[704,128]{1,0:T(8,128)(2,1)S(1)} collective-permute-done((bf16[704,128]{1,0:T(8,128)(2,1)S(1)}, bf16[704,128]{1,0:T(8,128)(2,1)S(1)}, u32[]{:S(2)}, u32[]{:S(2)}) %collective-permute-start.37) | collective-permute-done | bytes 180256 | tf_op jit(solution)/shard_map/ppermute | solution.py:33
  64.1 4.3 %collective-permute-start.24 = (bf16[128,1408]{1,0:T(8,128)(2,1)}, bf16[128,1408]{1,0:T(8,128)(2,1)}, u32[]{:S(2)}, u32[]{:S(2)}) collective-permute-start(bf16[128,1408]{1,0:T(8,128)(2,1)} %get-tuple-element.30), channel_id=1, source_target_pairs={{0,24},{4,28},{8,16},{12,20},{16,8},{20,12},{24,0},{28,4},{1,25},{... | collective-permute-start | bytes 1081352 | tf_op jit(solution)/shard_map/ppermute | solution.py:33
  68.4 10.7 %collective-permute-done.20.refs_12_ = bf16[128,1408]{1,0:T(8,128)(2,1)S(1)} collective-permute-done((bf16[128,1408]{1,0:T(8,128)(2,1)S(1)}, bf16[128,1408]{1,0:T(8,128)(2,1)S(1)}, u32[]{:S(2)}, u32[]{:S(2)}) %collective-permute-start.20) | collective-permute-done | bytes 360480 | tf_op jit(solution)/shard_map/ppermute | solution.py:33
  79.1 4.0 %collective-permute-start.17 = (bf16[256,1408]{1,0:T(8,128)(2,1)S(1)}, bf16[256,1408]{1,0:T(8,128)(2,1)S(1)}, u32[]{:S(2)}, u32[]{:S(2)}) collective-permute-start(bf16[256,1408]{1,0:T(8,128)(2,1)S(1)} %get-tuple-element.22.refs_8_), channel_id=1, source_target_pairs={{0,4},{4,0},{8,12},{12,8},{16,20},{20,16},{24,28},{28,24},{1,5},{5... | collective-permute-start | bytes 2162696 | tf_op jit(solution)/shard_map/ppermute | solution.py:33
  83.1 11.8 %collective-permute-start.18 = (bf16[256,1408]{1,0:T(8,128)(2,1)}, bf16[256,1408]{1,0:T(8,128)(2,1)S(1)}, u32[]{:S(2)}, u32[]{:S(2)}) collective-permute-start(bf16[256,1408]{1,0:T(8,128)(2,1)} %copy-done.20), channel_id=1, source_target_pairs={{0,8},{4,12},{8,0},{12,4},{16,24},{20,28},{24,16},{28,20},{1,9},{5... | collective-permute-start | bytes 2162696 | tf_op jit(solution)/shard_map/ppermute | solution.py:33
  96.4 4.4 %shard_map.110 = (f32[128,2048]{1,0:T(8,128)}, bf16[128,2048]{1,0:T(8,128)(2,1)}) custom-call(bf16[128,2048]{1,0:T(8,128)(2,1)} %resid_ref.1, f32[1,2048]{1,0:T(1,128)} %bitcast.26, bf16[128,256]{1,0:T(8,128)(2,1)} %get-tuple-element.52.refs_0_, bf16[128,256]{1,0:T(8,128)(2,1)} %copy-done.35, bf16[128,256]{1,0:T(8,128)(2,1)} %copy-done.36, ...), custom_call_target="tpu_custom_call" | custom-call | flops 536870912 | bytes 6291456 | tf_op jit(solution)/shard_map/pallas_call | solution.py:144
  100.8 2.0 collective-permute-start.29
  102.8 18.6 %collective-permute-done.26.refs_18_ = bf16[128,1408]{1,0:T(8,128)(2,1)} collective-permute-done((bf16[128,1408]{1,0:T(8,128)(2,1)}, bf16[128,1408]{1,0:T(8,128)(2,1)}, u32[]{:S(2)}, u32[]{:S(2)}) %collective-permute-start.26) | collective-permute-done | bytes 360480 | tf_op jit(solution)/shard_map/ppermute | solution.py:33
  121.5 16.0 %collective-permute-done.29.refs_2_ = bf16[704,256]{1,0:T(8,128)(2,1)S(1)} collective-permute-done((bf16[704,256]{1,0:T(8,128)(2,1)}, bf16[704,256]{1,0:T(8,128)(2,1)S(1)}, u32[]{:S(2)}, u32[]{:S(2)}) %collective-permute-start.29) | collective-permute-done | bytes 360480 | tf_op jit(solution)/shard_map/ppermute | solution.py:33
  143.5 5.3 %collective-permute-done.23.refs_15_ = bf16[128,1408]{1,0:T(8,128)(2,1)S(1)} collective-permute-done((bf16[128,1408]{1,0:T(8,128)(2,1)S(1)}, bf16[128,1408]{1,0:T(8,128)(2,1)S(1)}, u32[]{:S(2)}, u32[]{:S(2)}) %collective-permute-start.23) | collective-permute-done | bytes 360480 | tf_op jit(solution)/shard_map/ppermute | solution.py:33
  149.9 6.6 %collective-permute-done.25.refs_17_ = bf16[128,1408]{1,0:T(8,128)(2,1)S(1)} collective-permute-done((bf16[128,1408]{1,0:T(8,128)(2,1)}, bf16[128,1408]{1,0:T(8,128)(2,1)S(1)}, u32[]{:S(2)}, u32[]{:S(2)}) %collective-permute-start.25) | collective-permute-done | bytes 360480 | tf_op jit(solution)/shard_map/ppermute | solution.py:33
  157.8 6.4 %collective-permute-done.27.refs_19_ = bf16[128,1408]{1,0:T(8,128)(2,1)S(1)} collective-permute-done((bf16[128,1408]{1,0:T(8,128)(2,1)}, bf16[128,1408]{1,0:T(8,128)(2,1)S(1)}, u32[]{:S(2)}, u32[]{:S(2)}) %collective-permute-start.27) | collective-permute-done | bytes 360480 | tf_op jit(solution)/shard_map/ppermute | solution.py:33
  165.7 11.9 %collective-permute-done.19.refs_11_ = bf16[256,1408]{1,0:T(8,128)(2,1)S(1)} collective-permute-done((bf16[256,1408]{1,0:T(8,128)(2,1)S(1)}, bf16[256,1408]{1,0:T(8,128)(2,1)S(1)}, u32[]{:S(2)}, u32[]{:S(2)}) %collective-permute-start.19) | collective-permute-done | bytes 720928 | tf_op jit(solution)/shard_map/ppermute | solution.py:33
  188.6 11.9 %shard_map.111.hidden_ref = bf16[1024,704]{1,0:T(8,128)(2,1)S(1)} custom-call(s32[12]{0:T(128)S(1)} %stack.104.starts_ref, bf16[128,2048]{1,0:T(8,128)(2,1)S(1)} %copy-done, bf16[128,2048]{1,0:T(8,128)(2,1)} %collective-permute-done.10.refs_1_, bf16[128,2048]{1,0:T(8,128)(2,1)} %collective-permute-done.11.refs_2_, ...), custom_call_target="tpu_custom_call" | custom-call | flops 5905580032 | bytes 11534336 | tf_op jit(solution)/shard_map/pallas_call | solution.py:185
  200.6 2.1 shard_map.113
  202.8 2.1 collective-permute-start.43
  204.9 1.8 collective-permute-start.45
  206.7 12.3 %collective-permute-done.43.refs_0_ = bf16[704,128]{1,0:T(8,128)(2,1)} collective-permute-done((bf16[704,128]{1,0:T(8,128)(2,1)S(1)}, bf16[704,128]{1,0:T(8,128)(2,1)}, u32[]{:S(2)}, u32[]{:S(2)}) %collective-permute-start.43) | collective-permute-done | bytes 180256 | tf_op jit(solution)/shard_map/ppermute | solution.py:33
  223.5 3.7 %shard_map.112 = (bf16[512,1024]{1,0:T(8,128)(2,1)S(1)}, bf16[512,1024]{1,0:T(8,128)(2,1)S(1)}) custom-call(s32[4]{0:T(128)S(1)} %pad_add_fusion.1.starts_ref, bf16[1024,704]{1,0:T(8,128)(2,1)S(1)} %copy-done.18, bf16[704,256]{1,0:T(8,128)(2,1)S(1)} %get-tuple-element.28.refs_0_, bf16[704,256]{1,0:T(8,128)(2,1)} %collective-permute-done.28.refs_1_, ...), custom_call_target="tpu_custom_call" | custom-call | flops 1476395008 | bytes 4194304 | tf_op jit(solution)/shard_map/pallas_call | solution.py:226
  228.5 2.6 shard_map.114
  233.6 1.7 collective-permute-start.41
  240.7 1.7 collective-permute-start.33
  247.8 10.1 %collective-permute-done.49.refs_10_ = bf16[128,512]{1,0:T(8,128)(2,1)S(1)} collective-permute-done((bf16[128,512]{1,0:T(8,128)(2,1)}, bf16[128,512]{1,0:T(8,128)(2,1)S(1)}, u32[]{:S(2)}, u32[]{:S(2)}) %collective-permute-start.49) | collective-permute-done | bytes 131104 | tf_op jit(solution)/shard_map/ppermute | solution.py:33
  257.9 2.0 collective-permute-done.50.refs_11_
  260.8 3.0 %shard_map.115 = bf16[128,2048]{1,0:T(8,128)(2,1)} custom-call(s32[3]{0:T(128)} %pad_add_fusion.bases_ref, f32[128,2048]{1,0:T(8,128)} %get-tuple-element.13.middle_ref, bf16[128,1024]{1,0:T(8,128)(2,1)} %get-tuple-element.26.refs_0_, bf16[128,1024]{1,0:T(8,128)(2,1)} %copy-done.24, bf16[128,1024]{1,0:T(8,128)(2,1)} %copy-done.25, ...), custom_call_target="tpu_custom_call" | custom-call | flops 2097152 | bytes 2097152 | tf_op jit(solution)/shard_map/pallas_call | solution.py:257
  (182 shorter events, 59.6 us)
Async XLA Ops:
  0.0 83.1 %collective-permute-start.7 = (bf16[256,2048]{1,0:T(8,128)(2,1)}, bf16[256,2048]{1,0:T(8,128)(2,1)}, u32[]{:S(2)}, u32[]{:S(2)}) collective-permute-start(bf16[256,2048]{1,0:T(8,128)(2,1)} %refs_4_.1), channel_id=1, source_target_pairs={{0,1},{1,0},{2,3},{3,2},{4,5},{5,4},{6,7},{7,6},{8,9},{9,8},{10,11... | collective-permute-start | bytes 3145736 | tf_op jit(solution)/shard_map/ppermute | solution.py:33
  0.5 34.8 %collective-permute-start.8 = (bf16[256,2048]{1,0:T(8,128)(2,1)}, bf16[256,2048]{1,0:T(8,128)(2,1)}, u32[]{:S(2)}, u32[]{:S(2)}) collective-permute-start(bf16[256,2048]{1,0:T(8,128)(2,1)} %refs_4_.1), channel_id=1, source_target_pairs={{0,2},{1,3},{2,0},{3,1},{4,6},{5,7},{6,4},{7,5},{8,10},{9,11},{10,... | collective-permute-start | bytes 3145736 | tf_op jit(solution)/shard_map/ppermute | solution.py:33
  20.3 26.1 %collective-permute-start.35 = (bf16[704,128]{1,0:T(8,128)(2,1)S(1)}, bf16[704,128]{1,0:T(8,128)(2,1)S(1)}, u32[]{:S(2)}, u32[]{:S(2)}) collective-permute-start(bf16[704,128]{1,0:T(8,128)(2,1)S(1)} %get-tuple-element.48), channel_id=1, source_target_pairs={{0,16},{4,20},{8,24},{12,28},{16,0},{20,4},{24,8},{28,12},{1,17},{... | collective-permute-start | bytes 540680 | tf_op jit(solution)/shard_map/ppermute | solution.py:33
  35.2 59.6 %collective-permute-start.9 = (bf16[256,2048]{1,0:T(8,128)(2,1)}, bf16[256,2048]{1,0:T(8,128)(2,1)}, u32[]{:S(2)}, u32[]{:S(2)}) collective-permute-start(bf16[256,2048]{1,0:T(8,128)(2,1)} %collective-permute-done.8.refs_6_), channel_id=1, source_target_pairs={{0,1},{1,0},{2,3},{3,2},{4,5},{5,4},{6,7},{7,6},{8,9},{9,8},{10,11... | collective-permute-start | bytes 3145736 | tf_op jit(solution)/shard_map/ppermute | solution.py:33
  41.5 37.6 %collective-permute-start.20 = (bf16[128,1408]{1,0:T(8,128)(2,1)S(1)}, bf16[128,1408]{1,0:T(8,128)(2,1)S(1)}, u32[]{:S(2)}, u32[]{:S(2)}) collective-permute-start(bf16[128,1408]{1,0:T(8,128)(2,1)S(1)} %get-tuple-element.32), channel_id=1, source_target_pairs={{0,16},{4,20},{8,24},{12,28},{16,0},{20,4},{24,8},{28,12},{1,17},{... | collective-permute-start | bytes 1081352 | tf_op jit(solution)/shard_map/ppermute | solution.py:33
  46.4 54.4 %collective-permute-start.22 = (bf16[128,1408]{1,0:T(8,128)(2,1)}, bf16[128,1408]{1,0:T(8,128)(2,1)S(1)}, u32[]{:S(2)}, u32[]{:S(2)}) collective-permute-start(bf16[128,1408]{1,0:T(8,128)(2,1)} %get-tuple-element.31), channel_id=1, source_target_pairs={{0,16},{4,20},{8,24},{12,28},{16,0},{20,4},{24,8},{28,12},{1,17},{... | collective-permute-start | bytes 1081352 | tf_op jit(solution)/shard_map/ppermute | solution.py:33
  47.0 17.1 %collective-permute-start.37 = (bf16[704,128]{1,0:T(8,128)(2,1)S(1)}, bf16[704,128]{1,0:T(8,128)(2,1)S(1)}, u32[]{:S(2)}, u32[]{:S(2)}) collective-permute-start(bf16[704,128]{1,0:T(8,128)(2,1)S(1)} %get-tuple-element.46), channel_id=1, source_target_pairs={{0,24},{4,28},{8,16},{12,20},{16,8},{20,12},{24,0},{28,4},{1,25},{... | collective-permute-start | bytes 540680 | tf_op jit(solution)/shard_map/ppermute | solution.py:33
  64.1 36.7 %collective-permute-start.24 = (bf16[128,1408]{1,0:T(8,128)(2,1)}, bf16[128,1408]{1,0:T(8,128)(2,1)}, u32[]{:S(2)}, u32[]{:S(2)}) collective-permute-start(bf16[128,1408]{1,0:T(8,128)(2,1)} %get-tuple-element.30), channel_id=1, source_target_pairs={{0,24},{4,28},{8,16},{12,20},{16,8},{20,12},{24,0},{28,4},{1,25},{... | collective-permute-start | bytes 1081352 | tf_op jit(solution)/shard_map/ppermute | solution.py:33
  79.1 59.5 %collective-permute-start.17 = (bf16[256,1408]{1,0:T(8,128)(2,1)S(1)}, bf16[256,1408]{1,0:T(8,128)(2,1)S(1)}, u32[]{:S(2)}, u32[]{:S(2)}) collective-permute-start(bf16[256,1408]{1,0:T(8,128)(2,1)S(1)} %get-tuple-element.22.refs_8_), channel_id=1, source_target_pairs={{0,4},{4,0},{8,12},{12,8},{16,20},{20,16},{24,28},{28,24},{1,5},{5... | collective-permute-start | bytes 2162696 | tf_op jit(solution)/shard_map/ppermute | solution.py:33
  83.1 57.6 %collective-permute-start.18 = (bf16[256,1408]{1,0:T(8,128)(2,1)}, bf16[256,1408]{1,0:T(8,128)(2,1)S(1)}, u32[]{:S(2)}, u32[]{:S(2)}) collective-permute-start(bf16[256,1408]{1,0:T(8,128)(2,1)} %copy-done.20), channel_id=1, source_target_pairs={{0,8},{4,12},{8,0},{12,4},{16,24},{20,28},{24,16},{28,20},{1,9},{5... | collective-permute-start | bytes 2162696 | tf_op jit(solution)/shard_map/ppermute | solution.py:33
  94.9 26.5 %collective-permute-start.26 = (bf16[128,1408]{1,0:T(8,128)(2,1)}, bf16[128,1408]{1,0:T(8,128)(2,1)}, u32[]{:S(2)}, u32[]{:S(2)}) collective-permute-start(bf16[128,1408]{1,0:T(8,128)(2,1)} %get-tuple-element.29), channel_id=1, source_target_pairs={{0,24},{4,28},{8,16},{12,20},{16,8},{20,12},{24,0},{28,4},{1,25},{... | collective-permute-start | bytes 1081352 | tf_op jit(solution)/shard_map/ppermute | solution.py:33
  100.8 38.4 %collective-permute-start.11 = (bf16[128,2048]{1,0:T(8,128)(2,1)}, bf16[128,2048]{1,0:T(8,128)(2,1)}, u32[]{:S(2)}, u32[]{:S(2)}) collective-permute-start(bf16[128,2048]{1,0:T(8,128)(2,1)} %get-tuple-element.14.refs_0_), channel_id=1, source_target_pairs={{0,8},{4,12},{8,0},{12,4},{16,24},{20,28},{24,16},{28,20},{1,9},{5... | collective-permute-start | bytes 1572872 | tf_op jit(solution)/shard_map/ppermute | solution.py:33
  100.8 36.7 %collective-permute-start.29 = (bf16[704,256]{1,0:T(8,128)(2,1)}, bf16[704,256]{1,0:T(8,128)(2,1)S(1)}, u32[]{:S(2)}, u32[]{:S(2)}) collective-permute-start(bf16[704,256]{1,0:T(8,128)(2,1)} %copy-done.21), channel_id=1, source_target_pairs={{0,8},{4,12},{8,0},{12,4},{16,24},{20,28},{24,16},{28,20},{1,9},{5... | collective-permute-start | bytes 1081352 | tf_op jit(solution)/shard_map/ppermute | solution.py:33
  121.4 20.9 %collective-permute-start.21 = (bf16[128,1408]{1,0:T(8,128)(2,1)S(1)}, bf16[128,1408]{1,0:T(8,128)(2,1)S(1)}, u32[]{:S(2)}, u32[]{:S(2)}) collective-permute-start(bf16[128,1408]{1,0:T(8,128)(2,1)S(1)} %collective-permute-done.20.refs_12_), channel_id=1, source_target_pairs={{0,4},{4,0},{8,12},{12,8},{16,20},{20,16},{24,28},{28,24},{1,5},{5... | collective-permute-start | bytes 1081352 | tf_op jit(solution)/shard_map/ppermute | solution.py:33
  138.6 18.6 %collective-permute-start.10 = (bf16[128,2048]{1,0:T(8,128)(2,1)}, bf16[128,2048]{1,0:T(8,128)(2,1)}, u32[]{:S(2)}, u32[]{:S(2)}) collective-permute-start(bf16[128,2048]{1,0:T(8,128)(2,1)} %get-tuple-element.14.refs_0_), channel_id=1, source_target_pairs={{0,2},{1,3},{2,0},{3,1},{4,6},{5,7},{6,4},{7,5},{8,10},{9,11},{10,... | collective-permute-start | bytes 1572872 | tf_op jit(solution)/shard_map/ppermute | solution.py:33
  139.2 25.8 %collective-permute-start.12 = (bf16[128,2048]{1,0:T(8,128)(2,1)}, bf16[128,2048]{1,0:T(8,128)(2,1)}, u32[]{:S(2)}, u32[]{:S(2)}) collective-permute-start(bf16[128,2048]{1,0:T(8,128)(2,1)} %collective-permute-done.11.refs_2_), channel_id=1, source_target_pairs={{0,2},{1,3},{2,0},{3,1},{4,6},{5,7},{6,4},{7,5},{8,10},{9,11},{10,... | collective-permute-start | bytes 1572872 | tf_op jit(solution)/shard_map/ppermute | solution.py:33
  140.7 15.8 %collective-permute-start.25 = (bf16[128,1408]{1,0:T(8,128)(2,1)}, bf16[128,1408]{1,0:T(8,128)(2,1)S(1)}, u32[]{:S(2)}, u32[]{:S(2)}) collective-permute-start(bf16[128,1408]{1,0:T(8,128)(2,1)} %collective-permute-done.24.refs_16_), channel_id=1, source_target_pairs={{0,4},{4,0},{8,12},{12,8},{16,20},{20,16},{24,28},{28,24},{1,5},{5... | collective-permute-start | bytes 1081352 | tf_op jit(solution)/shard_map/ppermute | solution.py:33
  143.1 21.2 %collective-permute-start.27 = (bf16[128,1408]{1,0:T(8,128)(2,1)}, bf16[128,1408]{1,0:T(8,128)(2,1)S(1)}, u32[]{:S(2)}, u32[]{:S(2)}) collective-permute-start(bf16[128,1408]{1,0:T(8,128)(2,1)} %collective-permute-done.26.refs_18_), channel_id=1, source_target_pairs={{0,4},{4,0},{8,12},{12,8},{16,20},{20,16},{24,28},{28,24},{1,5},{5... | collective-permute-start | bytes 1081352 | tf_op jit(solution)/shard_map/ppermute | solution.py:33
  149.6 28.1 %collective-permute-start.19 = (bf16[256,1408]{1,0:T(8,128)(2,1)S(1)}, bf16[256,1408]{1,0:T(8,128)(2,1)S(1)}, u32[]{:S(2)}, u32[]{:S(2)}) collective-permute-start(bf16[256,1408]{1,0:T(8,128)(2,1)S(1)} %collective-permute-done.18.refs_10_), channel_id=1, source_target_pairs={{0,4},{4,0},{8,12},{12,8},{16,20},{20,16},{24,28},{28,24},{1,5},{5... | collective-permute-start | bytes 2162696 | tf_op jit(solution)/shard_map/ppermute | solution.py:33
  157.3 21.0 %collective-permute-start.13 = (bf16[128,2048]{1,0:T(8,128)(2,1)}, bf16[128,2048]{1,0:T(8,128)(2,1)}, u32[]{:S(2)}, u32[]{:S(2)}) collective-permute-start(bf16[128,2048]{1,0:T(8,128)(2,1)} %get-tuple-element.14.refs_0_), channel_id=1, source_target_pairs={{0,1},{1,0},{2,3},{3,2},{4,5},{5,4},{6,7},{7,6},{8,9},{9,8},{10,11... | collective-permute-start | bytes 1572872 | tf_op jit(solution)/shard_map/ppermute | solution.py:33
  157.3 22.4 %collective-permute-start.14 = (bf16[128,2048]{1,0:T(8,128)(2,1)}, bf16[128,2048]{1,0:T(8,128)(2,1)}, u32[]{:S(2)}, u32[]{:S(2)}) collective-permute-start(bf16[128,2048]{1,0:T(8,128)(2,1)} %collective-permute-done.10.refs_1_), channel_id=1, source_target_pairs={{0,1},{1,0},{2,3},{3,2},{4,5},{5,4},{6,7},{7,6},{8,9},{9,8},{10,11... | collective-permute-start | bytes 1572872 | tf_op jit(solution)/shard_map/ppermute | solution.py:33
  165.0 15.3 %collective-permute-start.15 = (bf16[128,2048]{1,0:T(8,128)(2,1)}, bf16[128,2048]{1,0:T(8,128)(2,1)}, u32[]{:S(2)}, u32[]{:S(2)}) collective-permute-start(bf16[128,2048]{1,0:T(8,128)(2,1)} %collective-permute-done.11.refs_2_), channel_id=1, source_target_pairs={{0,1},{1,0},{2,3},{3,2},{4,5},{5,4},{6,7},{7,6},{8,9},{9,8},{10,11... | collective-permute-start | bytes 1572872 | tf_op jit(solution)/shard_map/ppermute | solution.py:33
  165.0 16.7 %collective-permute-start.16 = (bf16[128,2048]{1,0:T(8,128)(2,1)}, bf16[128,2048]{1,0:T(8,128)(2,1)}, u32[]{:S(2)}, u32[]{:S(2)}) collective-permute-start(bf16[128,2048]{1,0:T(8,128)(2,1)} %collective-permute-done.12.refs_3_), channel_id=1, source_target_pairs={{0,1},{1,0},{2,3},{3,2},{4,5},{5,4},{6,7},{7,6},{8,9},{9,8},{10,11... | collective-permute-start | bytes 1572872 | tf_op jit(solution)/shard_map/ppermute | solution.py:33
  177.6 43.5 %collective-permute-start.28 = (bf16[704,256]{1,0:T(8,128)(2,1)S(1)}, bf16[704,256]{1,0:T(8,128)(2,1)}, u32[]{:S(2)}, u32[]{:S(2)}) collective-permute-start(bf16[704,256]{1,0:T(8,128)(2,1)S(1)} %get-tuple-element.28.refs_0_), channel_id=1, source_target_pairs={{0,4},{4,0},{8,12},{12,8},{16,20},{20,16},{24,28},{28,24},{1,5},{5... | collective-permute-start | bytes 1081352 | tf_op jit(solution)/shard_map/ppermute | solution.py:33
  178.3 22.3 %collective-permute-start.36 = (bf16[704,128]{1,0:T(8,128)(2,1)S(1)}, bf16[704,128]{1,0:T(8,128)(2,1)S(1)}, u32[]{:S(2)}, u32[]{:S(2)}) collective-permute-start(bf16[704,128]{1,0:T(8,128)(2,1)S(1)} %collective-permute-done.35.refs_0_), channel_id=1, source_target_pairs={{0,4},{4,0},{8,12},{12,8},{16,20},{20,16},{24,28},{28,24},{1,5},{5... | collective-permute-start | bytes 540680 | tf_op jit(solution)/shard_map/ppermute | solution.py:33
  179.6 20.9 %collective-permute-start.38 = (bf16[704,128]{1,0:T(8,128)(2,1)}, bf16[704,128]{1,0:T(8,128)(2,1)S(1)}, u32[]{:S(2)}, u32[]{:S(2)}) collective-permute-start(bf16[704,128]{1,0:T(8,128)(2,1)} %copy-done.15), channel_id=1, source_target_pairs={{0,4},{4,0},{8,12},{12,8},{16,20},{20,16},{24,28},{28,24},{1,5},{5... | collective-permute-start | bytes 540680 | tf_op jit(solution)/shard_map/ppermute | solution.py:33
  180.3 40.8 %collective-permute-start.30 = (bf16[704,256]{1,0:T(8,128)(2,1)}, bf16[704,256]{1,0:T(8,128)(2,1)}, u32[]{:S(2)}, u32[]{:S(2)}) collective-permute-start(bf16[704,256]{1,0:T(8,128)(2,1)} %copy-done.1), channel_id=1, source_target_pairs={{0,4},{4,0},{8,12},{12,8},{16,20},{20,16},{24,28},{28,24},{1,5},{5... | collective-permute-start | bytes 1081352 | tf_op jit(solution)/shard_map/ppermute | solution.py:33
  202.7 28.5 %collective-permute-start.39 = (bf16[512,512]{1,0:T(8,128)(2,1)}, bf16[512,512]{1,0:T(8,128)(2,1)}, u32[]{:S(2)}, u32[]{:S(2)}) collective-permute-start(bf16[512,512]{1,0:T(8,128)(2,1)} %get-tuple-element.18), channel_id=1, source_target_pairs={{0,1},{1,0},{2,3},{3,2},{4,5},{5,4},{6,7},{7,6},{8,9},{9,8},{10,11... | collective-permute-start | bytes 1572872 | tf_op jit(solution)/shard_map/ppermute | solution.py:33
  202.8 16.2 %collective-permute-start.43 = (bf16[704,128]{1,0:T(8,128)(2,1)S(1)}, bf16[704,128]{1,0:T(8,128)(2,1)}, u32[]{:S(2)}, u32[]{:S(2)}) collective-permute-start(bf16[704,128]{1,0:T(8,128)(2,1)S(1)} %copy-done.27), channel_id=1, source_target_pairs={{0,16},{4,20},{8,24},{12,28},{16,0},{20,4},{24,8},{28,12},{1,17},{... | collective-permute-start | bytes 540680 | tf_op jit(solution)/shard_map/ppermute | solution.py:33
  239.2 20.7 %collective-permute-start.32 = (bf16[128,1024]{1,0:T(8,128)(2,1)S(1)}, bf16[128,1024]{1,0:T(8,128)(2,1)S(1)}, u32[]{:S(2)}, u32[]{:S(2)}) collective-permute-start(bf16[128,1024]{1,0:T(8,128)(2,1)S(1)} %get-tuple-element.25), channel_id=1, source_target_pairs={{0,2},{1,3},{2,0},{3,1},{4,6},{5,7},{6,4},{7,5},{8,10},{9,11},{10,... | collective-permute-start | bytes 786440 | tf_op jit(solution)/shard_map/ppermute | solution.py:33
  240.7 19.2 %collective-permute-start.33 = (bf16[128,1024]{1,0:T(8,128)(2,1)S(1)}, bf16[128,1024]{1,0:T(8,128)(2,1)S(1)}, u32[]{:S(2)}, u32[]{:S(2)}) collective-permute-start(bf16[128,1024]{1,0:T(8,128)(2,1)S(1)} %get-tuple-element.24), channel_id=1, source_target_pairs={{0,8},{4,12},{8,0},{12,4},{16,24},{20,28},{24,16},{28,20},{1,9},{5... | collective-permute-start | bytes 786440 | tf_op jit(solution)/shard_map/ppermute | solution.py:33
  242.4 17.5 %collective-permute-start.34 = (bf16[128,1024]{1,0:T(8,128)(2,1)S(1)}, bf16[128,1024]{1,0:T(8,128)(2,1)S(1)}, u32[]{:S(2)}, u32[]{:S(2)}) collective-permute-start(bf16[128,1024]{1,0:T(8,128)(2,1)S(1)} %get-tuple-element.23), channel_id=1, source_target_pairs={{0,10},{1,11},{2,8},{3,9},{4,14},{5,15},{6,12},{7,13},{8,2},{9,3},... | collective-permute-start | bytes 786440 | tf_op jit(solution)/shard_map/ppermute | solution.py:33
  (60 other events, 536.1 us)
where the time goes:
time: 265 us; the launch traced here: 264 us
  waiting for transfers between devices  123 us (46%)
  starting transfers between devices  74.7 us (28%)
  Pallas kernels  35.3 us (13%)
  local copies, waits for them, and re-layouts  25.7 us (10%)
  other arithmetic  4.85 us (2%)
    ppermute x47, waiting for transfers between devices, swap(): return lax.ppermute(block, axis, pairs)  122 us
    ppermute x47, starting transfers between devices, swap(): return lax.ppermute(block, axis, pairs)  63.3 us
    unnamed x83, local copies, waits for them, and re-layouts  16.3 us
    pallas_call x1, Pallas kernels, hidden_units(): pl.pallas_call(functools.partial(hidden_kernel, len(row_blocks), len(part...  11.9 us
    ppermute x2, starting transfers between devices, edges(): low = lax.ppermute(block[block.shape[0] - width:], 'sp', forward)  8.88 us
    pallas_call x3, Pallas kernels, down_rows(): pl.pallas_call(functools.partial(down_kernel, len(parts)), out_shape=(sha...  8.35 us
    pallas_call x1, Pallas kernels, attention(): pl.pallas_call(attention_kernel, out_shape=jax.ShapeDtypeStruct(q_proj.sh...  7.7 us
  transfers between devices with their start and end apart: 51, of which 16 were waited for; matrix products, arithmetic and copies ran while one was open for 6% of the time, Pallas kernels for 12%

commit v1 on v0

--- a/solution.py
+++ b/solution.py
@@ -33,34 +33,29 @@
     return lax.ppermute(block, axis, pairs)
 
 
-def edges(block, width):
-    count = lax.axis_size("sp")
-    forward = [(i, i + 1) for i in range(count - 1)]
-    backward = [(b, a) for a, b in forward]
-    low = lax.ppermute(block[block.shape[0] - width :], "sp", forward)
-    high = lax.ppermute(block[:width], "sp", backward)
-    return low, high
-
-
-def attention_kernel(sinks_ref, docs_ref, q_ref, k_ref, v_ref, low_ref, high_ref, out_ref):
+def attention_kernel(n_out, info_ref, sinks_ref, docs_ref, q_ref, k_ref, v_ref, first_ref, second_ref, *refs):
+    out_refs, attended = refs[:n_out], refs[n_out]
     kv_cols = k_ref.shape[1]
     kv_heads = kv_cols // HEAD
     groups = q_ref.shape[1] // kv_cols
     count = q_ref.shape[0] // WINDOW
     span = 3 * WINDOW
     shape = (WINDOW, span)
+    even = info_ref[1] == 0
     offset = lax.broadcasted_iota(jnp.int32, shape, 1) - lax.broadcasted_iota(jnp.int32, shape, 0)
     near = (offset >= 0) & (offset <= 2 * WINDOW)
+    ones = jnp.ones((span, HEAD), jnp.bfloat16)
 
     def band(own_ref, column, block):
+        cols = slice(column, column + kv_cols)
         pieces = []
         for i in range(block - 1, block + 2):
-            if i < 0:
-                pieces.append(low_ref[:, column : column + kv_cols])
-            elif i == count:
-                pieces.append(high_ref[:, column : column + kv_cols])
+            if 0 <= i < count:
+                pieces.append(own_ref[i * WINDOW : (i + 1) * WINDOW, :])
+            elif i < 0:
+                pieces.append(jnp.where(even, second_ref[:, cols], first_ref[:, cols]))
             else:
-                pieces.append(own_ref[i * WINDOW : (i + 1) * WINDOW, :])
+                pieces.append(jnp.where(even, first_ref[:, cols], second_ref[:, cols]))
         return jnp.concatenate(pieces, axis=0)
 
     for block in range(count):
@@ -70,54 +65,160 @@
         band_docs = docs_ref[:, block * WINDOW : block * WINDOW + span]
         valid = near & (jnp.concatenate([query_docs] * 3, axis=1) == band_docs)
         keys, values = band(k_ref, 0, block), band(v_ref, kv_cols, block)
+        queries = q_ref[rows, :] * HEAD ** (-0.5)
         outs = []
         for head in range(kv_heads):
             cols = slice(head * HEAD, (head + 1) * HEAD)
+            key = keys[:, cols]
+            value = jnp.concatenate([values[:, cols], ones], axis=1)
             for group in range(groups):
                 index = head * groups + group
-                query = q_ref[rows, index * HEAD : (index + 1) * HEAD]
                 scores = lax.dot_general(
-                    query, keys[:, cols], (((1,), (1,)), ((), ())), preferred_element_type=jnp.float32
-                ) * HEAD ** (-0.5)
+                    queries[:, index * HEAD : (index + 1) * HEAD],
+                    key,
+                    (((1,), (1,)), ((), ())),
+                    preferred_element_type=jnp.float32,
+                )
                 scores = jnp.where(valid, scores, masked)
                 sink = sinks_ref[index]
                 top = jnp.maximum(jnp.max(scores, axis=-1, keepdims=True), sink)
-                expd = jnp.exp(scores - top)
-                total = jnp.sum(expd, axis=-1, keepdims=True) + jnp.exp(sink - top)
-                probs = (expd * (1.0 / total)).astype(jnp.bfloat16)
-                outs.append(jnp.dot(probs, values[:, cols], preferred_element_type=jnp.float32))
-        out_ref[rows, :] = jnp.concatenate(outs, axis=1).astype(jnp.bfloat16)
+                expd = jnp.exp(scores - top).astype(jnp.bfloat16)
+                both = jnp.dot(expd, value, preferred_element_type=jnp.float32)
+                outs.append(both[:, :HEAD] / (both[:, HEAD:] + jnp.exp(sink - top)))
+        attended[rows, :] = jnp.concatenate(outs, axis=1).astype(jnp.bfloat16)
+    height = out_refs[0].shape[0]
+    for i, out_ref in enumerate(out_refs):
+        out_ref[...] = attended[pl.ds(pl.multiple_of((info_ref[0] ^ i) * height, height), height), :]
 
 
 def attention(q_proj, k_proj, v_proj, doc_ids, sinks):
     tok_rows = q_proj.shape[0]
+    n_tp, sp = lax.axis_size("tp"), lax.axis_index("sp")
     kv = jnp.concatenate([k_proj, v_proj], axis=1)
-    kv_low, kv_high = edges(kv, WINDOW)
-    doc_low, doc_high = edges(doc_ids, WINDOW)
-    docs = jnp.concatenate([doc_low, doc_ids, doc_high], axis=0)
-    positions = (
-        lax.axis_index("sp") * tok_rows
-        - WINDOW
-        + jnp.arange(tok_rows + 2 * WINDOW, dtype=jnp.int32)
-    )
-    inside = (positions >= 0) & (positions < tok_rows * lax.axis_size("sp"))
-    docs = jnp.where(inside, docs, -1)[None, :]
-    return pl.pallas_call(
-        attention_kernel,
-        out_shape=jax.ShapeDtypeStruct(q_proj.shape, jnp.bfloat16),
-        in_specs=[SMEM] + [VMEM] * 6,
-        out_specs=VMEM,
+    count = lax.axis_size("sp")
+    even = sp % 2 == 0
+    up = [(i, i + 1) for i in range(0, count - 1, 2)]
+    down = [(i, i + 1) for i in range(1, count - 1, 2)]
+    tail, head = slice(tok_rows - WINDOW, tok_rows), slice(0, WINDOW)
+
+    def trade(pairs, block, up_first):
+        sent = jnp.where(even == up_first, block[tail], block[head])
+        return lax.ppermute(sent, "sp", pairs + [(b, a) for a, b in pairs])
+
+    doc_first, doc_second = (trade(up, doc_ids, True), trade(down, doc_ids, False))
+    kv_first, kv_second = trade(up, kv, True), trade(down, kv, False)
+    docs = jnp.concatenate(
+        [
+            jnp.where(sp == 0, -1, jnp.where(even, doc_second, doc_first)),
+            doc_ids,
+            jnp.where(sp == count - 1, -1, jnp.where(even, doc_first, doc_second)),
+        ]
+    )[None, :]
+    info = jnp.stack([lax.axis_index("tp"), sp % 2]).astype(jnp.int32)
+    own = jax.ShapeDtypeStruct((tok_rows // n_tp, q_proj.shape[1]), jnp.bfloat16)
+    return pl.pallas_call(
+        functools.partial(attention_kernel, n_tp),
+        out_shape=(own,) * n_tp,
+        in_specs=[SMEM] * 2 + [VMEM] * 6,
+        out_specs=(VMEM,) * n_tp,
+        scratch_shapes=[pltpu.VMEM(q_proj.shape, jnp.bfloat16)],
         cost_estimate=pl.CostEstimate(
             flops=12 * tok_rows * WINDOW * q_proj.shape[1],
             bytes_accessed=1 << 20,
             transcendentals=0,
         ),
-    )(sinks, docs, q_proj, k_proj, v_proj, kv_low, kv_high)
+    )(info, sinks, docs, q_proj, k_proj, v_proj, kv_first, kv_second)
 
 
 SMEM = pl.BlockSpec(memory_space=pltpu.SMEM)
 VMEM = pl.BlockSpec(memory_space=pltpu.VMEM)
 ANY = pl.BlockSpec(memory_space=pl.ANY)
+
+
+def pack_kernel(half, far_cuts, info_ref, gate_ref, up_ref, *refs):
+    whole, step = half // 128 * 128, gate_ref.shape[0] // far_cuts
+
+    def fill(source, target_of):
+        lower = source * half
+        for start in range(0, whole, 128):
+            for ref, shift in ((gate_ref, 0), (up_ref, 128)):
+                target_of(2 * start + shift, ref[:, lower + start : lower + start + 128])
+        if half > whole:
+            rest = [ref[:, lower + whole : lower + half] for ref in (gate_ref, up_ref)]
+            target_of(2 * whole, jnp.concatenate(rest, axis=1))
+
+    for source in (0, 1):
+        for parity in (0, 1):
+            targets = refs[parity * (1 + far_cuts) : (parity + 1) * (1 + far_cuts)]
+
+            def store(start, value):
+                cols = slice(start, start + value.shape[1])
+                targets[0][:, cols] = value
+                for cut in range(far_cuts):
+                    targets[1 + cut][:, cols] = value[cut * step : (cut + 1) * step]
+
+            @pl.when(info_ref[0] == source ^ parity)
+            def _():
+                fill(source, store)
+
+
+def pack_gate_up(info, w_gate, w_up, far_cuts):
+    depth, width = w_gate.shape
+    near = jax.ShapeDtypeStruct((depth, width), jnp.bfloat16)
+    far = jax.ShapeDtypeStruct((depth // far_cuts, width), jnp.bfloat16)
+    packed = pl.pallas_call(
+        functools.partial(pack_kernel, width // 2, far_cuts),
+        out_shape=((near,) + (far,) * far_cuts) * 2,
+        in_specs=[SMEM, VMEM, VMEM],
+        out_specs=(VMEM,) * (2 * (1 + far_cuts)),
+        cost_estimate=pl.CostEstimate(flops=4 * depth * width, bytes_accessed=6 * w_gate.size, transcendentals=0),
+    )(info, w_gate, w_up)
+    return packed[: 1 + far_cuts], packed[1 + far_cuts :]
+
+
+def split_kernel(far_cuts, info_ref, down_ref, *refs):
+    half = refs[0].shape[0]
+    for parity in (0, 1):
+        targets = refs[parity * (1 + far_cuts) : (parity + 1) * (1 + far_cuts)]
+        rows = pl.ds(pl.multiple_of((info_ref[0] ^ parity) * half, half), half)
+        value = down_ref[rows, :]
+        width = value.shape[1] // far_cuts
+        targets[0][...] = value
+        for cut in range(far_cuts):
+            targets[1 + cut][...] = value[:, cut * width : (cut + 1) * width]
+
+
+def split_down(info, w_down, far_cuts):
+    depth, width = w_down.shape
+    near = jax.ShapeDtypeStruct((depth // 2, width), jnp.bfloat16)
+    far = jax.ShapeDtypeStruct((depth // 2, width // far_cuts), jnp.bfloat16)
+    halves = pl.pallas_call(
+        functools.partial(split_kernel, far_cuts),
+        out_shape=((near,) + (far,) * far_cuts) * 2,
+        in_specs=[SMEM, VMEM],
+        out_specs=(VMEM,) * (2 * (1 + far_cuts)),
+        cost_estimate=pl.CostEstimate(flops=depth * width, bytes_accessed=8 * depth * width, transcendentals=0),
+    )(info, w_down)
+    return halves[: 1 + far_cuts], halves[1 + far_cuts :]
+
+
+def merge_kernel(keep_ref, other_ref, *out_refs):
+    height = out_refs[0].shape[0]
+    for i, out_ref in enumerate(out_refs):
+        rows = pl.ds(i * height, height)
+        total = keep_ref[rows, :].astype(jnp.float32) + other_ref[rows, :].astype(jnp.float32)
+        out_ref[...] = total.astype(jnp.bfloat16)
+
+
+def merge(keep, other, count):
+    part = jax.ShapeDtypeStruct((keep.shape[0] // count, keep.shape[1]), jnp.bfloat16)
+    return pl.pallas_call(
+        merge_kernel,
+        out_shape=(part,) * count,
+        in_specs=[VMEM] * 2,
+        out_specs=(VMEM,) * count,
+        cost_estimate=pl.CostEstimate(flops=keep.size, bytes_accessed=6 * keep.size, transcendentals=0),
+    )(keep, other)
 
 
 def project_kernel(count, resid_ref, gain_ref, *refs):
@@ -170,13 +271,18 @@
     for copy in copies[n_rows:]:
         copy.wait()
     half = hidden_ref.shape[1]
-    tile = min(256, rows.shape[0])
+    tile = min(512, rows.shape[0])
     for lower in range(0, rows.shape[0], tile):
+        part = pl.ds(lower, tile)
         for i in range(lower // height, (lower + tile) // height):
             copies[i].wait()
-        both = jnp.dot(rows[pl.ds(lower, tile), :], weight[...], preferred_element_type=jnp.float32)
-        gate, up = both[:, :half], both[:, half:]
-        hidden_ref[pl.ds(lower, tile), :] = (gate / (1.0 + jnp.exp(-gate)) * up).astype(jnp.bfloat16)
+        for start in range(0, half, 128):
+            size = min(128, half - start)
+            both = jnp.dot(
+                rows[part, :], weight[:, 2 * start : 2 * (start + size)], preferred_element_type=jnp.float32
+            )
+            gate, up = both[:, :size], both[:, size:]
+            hidden_ref[part, start : start + size] = (gate / (1.0 + jnp.exp(-gate)) * up).astype(jnp.bfloat16)
 
 
 def hidden_units(starts, row_blocks, parts):
@@ -283,36 +389,30 @@
     n_sp, n_tp = lax.axis_size("sp"), lax.axis_size("tp")
     n_y = y_count(n_sp)
     n_z = n_sp // n_y
-    sp, tp = lax.axis_index("sp"), lax.axis_index("tp")
+    sp = lax.axis_index("sp")
     z = sp // n_y
-    half = w_gate.shape[1] // 2
-    depth = w_gate.shape[0]
-    piece = w_down.shape[1]
-
-    lower = jnp.concatenate([w_gate[:, :half], w_up[:, :half]], axis=1)
-    upper = jnp.concatenate([w_gate[:, half:], w_up[:, half:]], axis=1)
-    first = z % 2 == 0
-    gu_half = (jnp.where(first, lower, upper), jnp.where(first, upper, lower))
-    down_half = (
-        jnp.where(first, w_down[:half], w_down[half:]),
-        jnp.where(first, w_down[half:], w_down[:half]),
-    )
+    depth, piece = w_gate.shape[0], w_down.shape[1]
+
+    info = (z % 2).astype(jnp.int32)[None]
+    gu_cuts = 2 if depth % 32 == 0 else 1
+    down_cuts = 2 if piece % 256 == 0 else 1
+    gu_half = pack_gate_up(info, w_gate, w_up, gu_cuts)
+    down_half = split_down(info, w_down, down_cuts)
 
     gu_parts, gu_starts = [], []
     for dz in range(n_z):
-        cuts = 1 if dz < 2 else 2
+        cuts = 1 if dz < 2 else gu_cuts
         height = depth // cuts
         for cut in range(cuts):
-            held = swap(gu_half[dz % 2][cut * height : (cut + 1) * height], dz * n_y)
+            held = swap(gu_half[dz % 2][cut + 1 if dz >= 2 else 0], dz * n_y)
             for dy in range(n_y):
                 gu_parts.append(swap(held, dy))
                 gu_starts.append((sp ^ (dz * n_y + dy)) * depth + cut * height)
     down, cuts_of = {}, {}
     for dz in range(n_z):
-        cuts = cuts_of[dz // 2] = 2 if dz >= 2 and piece % 256 == 0 else 1
-        width = piece // cuts
+        cuts = cuts_of[dz // 2] = 1 if dz < 2 else down_cuts
         for cut in range(cuts):
-            held = swap(down_half[dz % 2][:, cut * width : (cut + 1) * width], dz * n_y)
+            held = swap(down_half[dz % 2][cut + 1 if dz >= 2 else 0], dz * n_y)
             for dy in range(n_y):
                 down[dz, cut, dy] = swap(held, dy)
 
@@ -322,8 +422,7 @@
     for t in range(0, n_tp, 2):
         out_blocks[t] = swap(w_out, 0, t)
         out_blocks[t + 1] = swap(out_blocks[t], 0, 1)
-    own_rows = q_proj.shape[0] // n_tp
-    heads = [swap(lax.dynamic_slice_in_dim(attended, (tp ^ t) * own_rows, own_rows, 0), 0, t) for t in range(n_tp)]
+    heads = [swap(attended[t], 0, t) for t in range(n_tp)]
     middle, normed = project(
         resid, norm_gain[None, :], heads, [out_blocks[t] for t in range(n_tp)]
     )
@@ -352,15 +451,10 @@
                 parts, starts = [lay_out(parts, starts, 1)], [sp * 0]
             keep, send = down_rows(jnp.stack(starts).astype(jnp.int32), hidden, parts)
             other = swap(send, 0, 1)
-            total = (keep.astype(jnp.float32) + other.astype(jnp.float32)).astype(jnp.bfloat16)
+            totals = merge(keep, other, len(order) // 2)
             plan.append((1, span, 0) if cuts == 1 else (2 * n_y, piece, cut * width))
             bases.append((z // 2 ^ pair) * span)
-            chunks.append(
-                [
-                    swap(total[i * own_rows : (i + 1) * own_rows], a * n_y, t)
-                    for i, (a, t) in enumerate(order[: len(order) // 2])
-                ]
-            )
+            chunks.append([swap(totals[i], a * n_y, t) for i, (a, t) in enumerate(order[: len(order) // 2])])
     return finish(tuple(plan), jnp.stack(bases).astype(jnp.int32), middle, chunks)
 
 

time: 265 us -> 255 us (0.962)
  Pallas kernels: 35.3 us -> 44.5 us
  starting transfers between devices: 74.7 us -> 66.2 us
  local copies, waits for them, and re-layouts: 25.7 us -> 21.2 us
  waiting for transfers between devices: 123 us -> 120 us
  other arithmetic: 4.85 us -> 2.1 us
    pallas_call x1 -> x6, Pallas kernels: 7.7 us -> 19 us  [the longest x3 6.68 us: merge(): pl.pallas_call(merge_kernel, out_shape=(part,) * count, in_specs=[VMEM] *...]
    slice x10 -> x0, local copies, waits for them, and re-layouts: 6.71 us -> none  [the longest x3 2.24 us: shards(): total[i * own_rows:(i + 1) * own_rows]]
    ppermute x47, starting transfers between devices: 63.3 us -> 58.7 us  [swap(): return lax.ppermute(block, axis, pairs)]
    ppermute x4, starting transfers between devices: 11.4 us -> 7.49 us  [trade(): return lax.ppermute(sent, 'sp', pairs + [(b, a) for a, b in pairs])]
    unnamed x83 -> x89, local copies, waits for them, and re-layouts: 16.3 us -> 19.6 us
  transfers between devices with their start and end apart: 51 -> 51, of which waited for: 16 -> 14; matrix products, arithmetic and copies ran while one was open for 6% -> 2% of each run, Pallas kernels for 12% -> 16%
where the time goes in v1:
time: 255 us; the launch traced here: 254 us
  waiting for transfers between devices  120 us (47%)
  starting transfers between devices  66.2 us (26%)
  Pallas kernels  44.5 us (17%)
  local copies, waits for them, and re-layouts  21.2 us (8%)
    ppermute x47, waiting for transfers between devices, swap(): return lax.ppermute(block, axis, pairs)  120 us
    ppermute x47, starting transfers between devices, swap(): return lax.ppermute(block, axis, pairs)  58.7 us
    unnamed x89, local copies, waits for them, and re-layouts  19.6 us
    pallas_call x1, Pallas kernels, hidden_units(): pl.pallas_call(functools.partial(hidden_kernel, len(row_blocks), len(part...  11.3 us
    ppermute x4, starting transfers between devices, trade(): return lax.ppermute(sent, 'sp', pairs + [(b, a) for a, b in pairs])  7.49 us
    pallas_call x3, Pallas kernels, down_rows(): pl.pallas_call(functools.partial(down_kernel, len(parts)), out_shape=(sha...  6.87 us
    pallas_call x3, Pallas kernels, merge(): pl.pallas_call(merge_kernel, out_shape=(part,) * count, in_specs=[VMEM] *...  6.68 us
    pallas_call x1, Pallas kernels, attention(): pl.pallas_call(functools.partial(attention_kernel, n_tp), out_shape=(own,...  6.43 us
  transfers between devices with their start and end apart: 51, of which 14 were waited for; matrix products, arithmetic and copies ran while one was open for 2% of the time, Pallas kernels for 16%

profile of v1, /device:TPU:0, one launch (start us, length us, event | category | flops | bytes accessed | tf_op | source)
XLA Modules:
  0.0 254.4 jit_solution(6702506717943784232)
XLA Ops:
  0.0 3.0 %collective-permute-start.8 = (bf16[256,2048]{1,0:T(8,128)(2,1)}, bf16[256,2048]{1,0:T(8,128)(2,1)S(1)}, u32[]{:S(2)}, u32[]{:S(2)}) collective-permute-start(bf16[256,2048]{1,0:T(8,128)(2,1)} %refs_4_.1), channel_id=1, source_target_pairs={{0,2},{1,3},{2,0},{3,1},{4,6},{5,7},{6,4},{7,5},{8,10},{9,11},{10,... | collective-permute-start | bytes 3145736 | tf_op jit(solution)/shard_map/ppermute | solution.py:33
  4.4 4.4 %collective-permute-start.1 = (s32[128]{0:T(128)S(1)}, s32[128]{0:T(128)S(1)}, u32[]{:S(2)}, u32[]{:S(2)}) collective-permute-start(s32[128]{0:T(128)S(1)} %get-tuple-element.80), channel_id=1, source_target_pairs={{0,4},{8,12},{16,20},{24,28},{4,0},{12,8},{20,16},{28,24},{1,5},{9... | collective-permute-start | bytes 1544 | tf_op jit(solution)/shard_map/ppermute | solution.py:106
  10.6 15.7 %collective-permute-done.8.refs_6_ = bf16[256,2048]{1,0:T(8,128)(2,1)S(1)} collective-permute-done((bf16[256,2048]{1,0:T(8,128)(2,1)}, bf16[256,2048]{1,0:T(8,128)(2,1)S(1)}, u32[]{:S(2)}, u32[]{:S(2)}) %collective-permute-start.8) | collective-permute-done | bytes 1048608 | tf_op jit(solution)/shard_map/ppermute | solution.py:33
  28.8 3.5 %shard_map.111 = (bf16[256,1408]{1,0:T(8,128)(2,1)}, bf16[128,1408]{1,0:T(8,128)(2,1)}, bf16[128,1408]{1,0:T(8,128)(2,1)}, bf16[256,1408]{1,0:T(8,128)(2,1)}, bf...) custom-call(s32[1]{0:T(128)} %bitcast.21.info_ref, bf16[256,1408]{1,0:T(8,128)(2,1)} %gate_ref.1, bf16[256,1408]{1,0:T(8,128)(2,1)} %up_ref.1), custom_call_target="tpu_custom_call" | custom-call | flops 1441792 | bytes 2162688 | tf_op jit(solution)/shard_map/pallas_call | solution.py:169
  33.0 4.3 %collective-permute-start.20 = (bf16[128,1408]{1,0:T(8,128)(2,1)}, bf16[128,1408]{1,0:T(8,128)(2,1)S(1)}, u32[]{:S(2)}, u32[]{:S(2)}) collective-permute-start(bf16[128,1408]{1,0:T(8,128)(2,1)} %get-tuple-element.49), channel_id=1, source_target_pairs={{0,16},{4,20},{8,24},{12,28},{16,0},{20,4},{24,8},{28,12},{1,17},{... | collective-permute-start | bytes 1081352 | tf_op jit(solution)/shard_map/ppermute | solution.py:33
  39.1 6.4 %shard_map.109 = (bf16[128,256]{1,0:T(8,128)(2,1)}, bf16[128,256]{1,0:T(8,128)(2,1)}, bf16[128,256]{1,0:T(8,128)(2,1)}, bf16[128,256]{1,0:T(8,128)(2,1)}) custom-call(s32[2]{0:T(128)} %pad_add_fusion.2.info_ref, f32[4]{0:T(128)} %sinks_ref.1, s32[1,768]{1,0:T(1,128)} %broadcast_in_dim.16.docs_ref, bf16[512,256]{1,0:T(8,128)(2,1)} %q_ref.1, ...), custom_call_target="tpu_custom_call" | custom-call | flops 201326592 | bytes 1048576 | tf_op jit(solution)/shard_map/pallas_call | solution.py:119
  47.1 4.1 %collective-permute-start.22 = (bf16[128,1408]{1,0:T(8,128)(2,1)}, bf16[128,1408]{1,0:T(8,128)(2,1)S(1)}, u32[]{:S(2)}, u32[]{:S(2)}) collective-permute-start(bf16[128,1408]{1,0:T(8,128)(2,1)} %get-tuple-element.50), channel_id=1, source_target_pairs={{0,16},{4,20},{8,24},{12,28},{16,0},{20,4},{24,8},{28,12},{1,17},{... | collective-permute-start | bytes 1081352 | tf_op jit(solution)/shard_map/ppermute | solution.py:33
  52.1 3.6 %collective-permute-done.6.refs_3_ = bf16[128,256]{1,0:T(8,128)(2,1)S(1)} collective-permute-done((bf16[128,256]{1,0:T(8,128)(2,1)}, bf16[128,256]{1,0:T(8,128)(2,1)S(1)}, u32[]{:S(2)}, u32[]{:S(2)}) %collective-permute-start.6) | collective-permute-done | bytes 65568 | tf_op jit(solution)/shard_map/ppermute | solution.py:33
  55.8 4.7 %collective-permute-start.24 = (bf16[128,1408]{1,0:T(8,128)(2,1)}, bf16[128,1408]{1,0:T(8,128)(2,1)}, u32[]{:S(2)}, u32[]{:S(2)}) collective-permute-start(bf16[128,1408]{1,0:T(8,128)(2,1)} %get-tuple-element.51), channel_id=1, source_target_pairs={{0,24},{4,28},{8,16},{12,20},{16,8},{20,12},{24,0},{28,4},{1,25},{... | collective-permute-start | bytes 1081352 | tf_op jit(solution)/shard_map/ppermute | solution.py:33
  60.4 10.5 %collective-permute-done.20.refs_12_ = bf16[128,1408]{1,0:T(8,128)(2,1)S(1)} collective-permute-done((bf16[128,1408]{1,0:T(8,128)(2,1)}, bf16[128,1408]{1,0:T(8,128)(2,1)S(1)}, u32[]{:S(2)}, u32[]{:S(2)}) %collective-permute-start.20) | collective-permute-done | bytes 360480 | tf_op jit(solution)/shard_map/ppermute | solution.py:33
  72.9 2.2 collective-permute-start.26
  75.1 4.4 %shard_map.110 = (f32[128,2048]{1,0:T(8,128)}, bf16[128,2048]{1,0:T(8,128)(2,1)}) custom-call(bf16[128,2048]{1,0:T(8,128)(2,1)} %resid_ref.1, f32[1,2048]{1,0:T(1,128)} %bitcast.26, bf16[128,256]{1,0:T(8,128)(2,1)} %get-tuple-element.41.refs_0_, bf16[128,256]{1,0:T(8,128)(2,1)} %copy-done.34, bf16[128,256]{1,0:T(8,128)(2,1)} %copy-done.35, ...), custom_call_target="tpu_custom_call" | custom-call | flops 536870912 | bytes 6291456 | tf_op jit(solution)/shard_map/pallas_call | solution.py:245
  80.7 2.3 shard_map.113
  83.0 4.2 %collective-permute-start.29 = (bf16[704,256]{1,0:T(8,128)(2,1)}, bf16[704,256]{1,0:T(8,128)(2,1)S(1)}, u32[]{:S(2)}, u32[]{:S(2)}) collective-permute-start(bf16[704,256]{1,0:T(8,128)(2,1)} %get-tuple-element.54), channel_id=1, source_target_pairs={{0,8},{4,12},{8,0},{12,4},{16,24},{20,28},{24,16},{28,20},{1,9},{5... | collective-permute-start | bytes 1081352 | tf_op jit(solution)/shard_map/ppermute | solution.py:33
  87.1 12.9 %collective-permute-done.26.refs_18_ = bf16[128,1408]{1,0:T(8,128)(2,1)} collective-permute-done((bf16[128,1408]{1,0:T(8,128)(2,1)}, bf16[128,1408]{1,0:T(8,128)(2,1)}, u32[]{:S(2)}, u32[]{:S(2)}) %collective-permute-start.26) | collective-permute-done | bytes 360480 | tf_op jit(solution)/shard_map/ppermute | solution.py:33
  100.1 20.0 %collective-permute-done.29.refs_2_ = bf16[704,256]{1,0:T(8,128)(2,1)S(1)} collective-permute-done((bf16[704,256]{1,0:T(8,128)(2,1)}, bf16[704,256]{1,0:T(8,128)(2,1)S(1)}, u32[]{:S(2)}, u32[]{:S(2)}) %collective-permute-start.29) | collective-permute-done | bytes 360480 | tf_op jit(solution)/shard_map/ppermute | solution.py:33
  126.5 4.9 %collective-permute-done.23.refs_15_ = bf16[128,1408]{1,0:T(8,128)(2,1)S(1)} collective-permute-done((bf16[128,1408]{1,0:T(8,128)(2,1)S(1)}, bf16[128,1408]{1,0:T(8,128)(2,1)S(1)}, u32[]{:S(2)}, u32[]{:S(2)}) %collective-permute-start.23) | collective-permute-done | bytes 360480 | tf_op jit(solution)/shard_map/ppermute | solution.py:33
  133.7 5.4 %collective-permute-done.25.refs_17_ = bf16[128,1408]{1,0:T(8,128)(2,1)S(1)} collective-permute-done((bf16[128,1408]{1,0:T(8,128)(2,1)}, bf16[128,1408]{1,0:T(8,128)(2,1)S(1)}, u32[]{:S(2)}, u32[]{:S(2)}) %collective-permute-start.25) | collective-permute-done | bytes 360480 | tf_op jit(solution)/shard_map/ppermute | solution.py:33
  140.4 6.5 %collective-permute-done.27.refs_19_ = bf16[128,1408]{1,0:T(8,128)(2,1)S(1)} collective-permute-done((bf16[128,1408]{1,0:T(8,128)(2,1)}, bf16[128,1408]{1,0:T(8,128)(2,1)S(1)}, u32[]{:S(2)}, u32[]{:S(2)}) %collective-permute-start.27) | collective-permute-done | bytes 360480 | tf_op jit(solution)/shard_map/ppermute | solution.py:33
  148.3 13.1 %collective-permute-done.19.refs_11_ = bf16[256,1408]{1,0:T(8,128)(2,1)S(1)} collective-permute-done((bf16[256,1408]{1,0:T(8,128)(2,1)S(1)}, bf16[256,1408]{1,0:T(8,128)(2,1)S(1)}, u32[]{:S(2)}, u32[]{:S(2)}) %collective-permute-start.19) | collective-permute-done | bytes 720928 | tf_op jit(solution)/shard_map/ppermute | solution.py:33
  172.8 11.3 %shard_map.112.hidden_ref = bf16[1024,704]{1,0:T(8,128)(2,1)S(1)} custom-call(s32[12]{0:T(128)S(1)} %stack.116.starts_ref, bf16[128,2048]{1,0:T(8,128)(2,1)S(1)} %copy-done.4, bf16[128,2048]{1,0:T(8,128)(2,1)} %collective-permute-done.10.refs_1_, bf16[128,2048]{1,0:T(8,128)(2,1)S(1)} %collective-permute-done.11.refs_2_, ...), custom_call_target="tpu_custom_call" | custom-call | flops 5905580032 | bytes 11534336 | tf_op jit(solution)/shard_map/pallas_call | solution.py:291
  184.2 2.6 %shard_map.114 = (bf16[512,1024]{1,0:T(8,128)(2,1)S(1)}, bf16[512,1024]{1,0:T(8,128)(2,1)S(1)}) custom-call(s32[4]{0:T(128)S(1)} %pad_add_fusion.3.starts_ref, bf16[1024,704]{1,0:T(8,128)(2,1)S(1)} %shard_map.112.hidden_ref, bf16[704,256]{1,0:T(8,128)(2,1)S(1)} %copy-done.9, bf16[704,256]{1,0:T(8,128)(2,1)S(1)} %collective-permute-done.28.refs_1_, ...), custom_call_target="tpu_custom_call" | custom-call | flops 1476395008 | bytes 4194304 | tf_op jit(solution)/shard_map/pallas_call | solution.py:332
  187.9 2.0 collective-permute-start.43
  193.2 10.7 %collective-permute-done.43.refs_0_ = bf16[704,128]{1,0:T(8,128)(2,1)S(1)} collective-permute-done((bf16[704,128]{1,0:T(8,128)(2,1)S(1)}, bf16[704,128]{1,0:T(8,128)(2,1)S(1)}, u32[]{:S(2)}, u32[]{:S(2)}) %collective-permute-start.43) | collective-permute-done | bytes 180256 | tf_op jit(solution)/shard_map/ppermute | solution.py:33
  207.4 2.6 %shard_map.116 = (bf16[512,512]{1,0:T(8,128)(2,1)S(1)}, bf16[512,512]{1,0:T(8,128)(2,1)S(1)}) custom-call(s32[4]{0:T(128)S(1)} %pad_add_fusion.4.starts_ref, bf16[1024,704]{1,0:T(8,128)(2,1)S(1)} %copy-done.21, bf16[704,128]{1,0:T(8,128)(2,1)} %collective-permute-done.35.refs_0_, bf16[704,128]{1,0:T(8,128)(2,1)S(1)} %collective-permute-done.36.refs_1_, ...), custom_call_target="tpu_custom_call" | custom-call | flops 738197504 | bytes 4194304 | tf_op jit(solution)/shard_map/pallas_call | solution.py:332
  211.3 2.1 collective-permute-done.46.refs_3_
  216.8 2.0 shard_map.117
  223.1 2.1 shard_map.119
  227.7 2.6 %shard_map.115 = (bf16[128,1024]{1,0:T(8,128)(2,1)}, bf16[128,1024]{1,0:T(8,128)(2,1)}, bf16[128,1024]{1,0:T(8,128)(2,1)}, bf16[128,1024]{1,0:T(8,128)(2,1)}) custom-call(bf16[512,1024]{1,0:T(8,128)(2,1)} %copy-done, bf16[512,1024]{1,0:T(8,128)(2,1)} %copy-done.23), custom_call_target="tpu_custom_call" | custom-call | flops 524288 | bytes 3145728 | tf_op jit(solution)/shard_map/pallas_call | solution.py:215
  236.4 11.7 %collective-permute-done.49.refs_10_ = bf16[128,512]{1,0:T(8,128)(2,1)S(1)} collective-permute-done((bf16[128,512]{1,0:T(8,128)(2,1)S(1)}, bf16[128,512]{1,0:T(8,128)(2,1)S(1)}, u32[]{:S(2)}, u32[]{:S(2)}) %collective-permute-start.49) | collective-permute-done | bytes 131104 | tf_op jit(solution)/shard_map/ppermute | solution.py:33
  248.2 2.3 collective-permute-done.50.refs_11_
  251.4 3.0 %shard_map.120 = bf16[128,2048]{1,0:T(8,128)(2,1)} custom-call(s32[3]{0:T(128)} %pad_add_fusion.1.bases_ref, f32[128,2048]{1,0:T(8,128)} %get-tuple-element.45.middle_ref, bf16[128,1024]{1,0:T(8,128)(2,1)} %get-tuple-element.57.refs_0_, bf16[128,1024]{1,0:T(8,128)(2,1)} %copy-done.26, bf16[128,1024]{1,0:T(8,128)(2,1)} %copy-done.27, ...), custom_call_target="tpu_custom_call" | custom-call | flops 2097152 | bytes 2097152 | tf_op jit(solution)/shard_map/pallas_call | solution.py:363
  (182 shorter events, 63.1 us)
Async XLA Ops:
  0.0 26.3 %collective-permute-start.8 = (bf16[256,2048]{1,0:T(8,128)(2,1)}, bf16[256,2048]{1,0:T(8,128)(2,1)S(1)}, u32[]{:S(2)}, u32[]{:S(2)}) collective-permute-start(bf16[256,2048]{1,0:T(8,128)(2,1)} %refs_4_.1), channel_id=1, source_target_pairs={{0,2},{1,3},{2,0},{3,1},{4,6},{5,7},{6,4},{7,5},{8,10},{9,11},{10,... | collective-permute-start | bytes 3145736 | tf_op jit(solution)/shard_map/ppermute | solution.py:33
  3.0 69.9 %collective-permute-start.7 = (bf16[256,2048]{1,0:T(8,128)(2,1)}, bf16[256,2048]{1,0:T(8,128)(2,1)}, u32[]{:S(2)}, u32[]{:S(2)}) collective-permute-start(bf16[256,2048]{1,0:T(8,128)(2,1)} %refs_4_.1), channel_id=1, source_target_pairs={{0,1},{1,0},{2,3},{3,2},{4,5},{5,4},{6,7},{7,6},{8,9},{9,8},{10,11... | collective-permute-start | bytes 3145736 | tf_op jit(solution)/shard_map/ppermute | solution.py:33
  3.7 28.6 %collective-permute-start = (s32[128]{0:T(128)S(1)}, s32[128]{0:T(128)S(1)}, u32[]{:S(2)}, u32[]{:S(2)}) collective-permute-start(s32[128]{0:T(128)S(1)} %get-tuple-element.79), channel_id=1, source_target_pairs={{4,8},{12,16},{20,24},{8,4},{16,12},{24,20},{5,9},{13,17},{21,25},... | collective-permute-start | bytes 1544 | tf_op jit(solution)/shard_map/ppermute | solution.py:106
  4.4 28.6 %collective-permute-start.1 = (s32[128]{0:T(128)S(1)}, s32[128]{0:T(128)S(1)}, u32[]{:S(2)}, u32[]{:S(2)}) collective-permute-start(s32[128]{0:T(128)S(1)} %get-tuple-element.80), channel_id=1, source_target_pairs={{0,4},{8,12},{16,20},{24,28},{4,0},{12,8},{20,16},{28,24},{1,5},{9... | collective-permute-start | bytes 1544 | tf_op jit(solution)/shard_map/ppermute | solution.py:106
  26.3 46.5 %collective-permute-start.9 = (bf16[256,2048]{1,0:T(8,128)(2,1)S(1)}, bf16[256,2048]{1,0:T(8,128)(2,1)}, u32[]{:S(2)}, u32[]{:S(2)}) collective-permute-start(bf16[256,2048]{1,0:T(8,128)(2,1)S(1)} %collective-permute-done.8.refs_6_), channel_id=1, source_target_pairs={{0,1},{1,0},{2,3},{3,2},{4,5},{5,4},{6,7},{7,6},{8,9},{9,8},{10,11... | collective-permute-start | bytes 3145736 | tf_op jit(solution)/shard_map/ppermute | solution.py:33
  33.0 38.0 %collective-permute-start.20 = (bf16[128,1408]{1,0:T(8,128)(2,1)}, bf16[128,1408]{1,0:T(8,128)(2,1)S(1)}, u32[]{:S(2)}, u32[]{:S(2)}) collective-permute-start(bf16[128,1408]{1,0:T(8,128)(2,1)} %get-tuple-element.49), channel_id=1, source_target_pairs={{0,16},{4,20},{8,24},{12,28},{16,0},{20,4},{24,8},{28,12},{1,17},{... | collective-permute-start | bytes 1081352 | tf_op jit(solution)/shard_map/ppermute | solution.py:33
  47.1 32.4 %collective-permute-start.22 = (bf16[128,1408]{1,0:T(8,128)(2,1)}, bf16[128,1408]{1,0:T(8,128)(2,1)S(1)}, u32[]{:S(2)}, u32[]{:S(2)}) collective-permute-start(bf16[128,1408]{1,0:T(8,128)(2,1)} %get-tuple-element.50), channel_id=1, source_target_pairs={{0,16},{4,20},{8,24},{12,28},{16,0},{20,4},{24,8},{28,12},{1,17},{... | collective-permute-start | bytes 1081352 | tf_op jit(solution)/shard_map/ppermute | solution.py:33
  55.8 27.2 %collective-permute-start.24 = (bf16[128,1408]{1,0:T(8,128)(2,1)}, bf16[128,1408]{1,0:T(8,128)(2,1)}, u32[]{:S(2)}, u32[]{:S(2)}) collective-permute-start(bf16[128,1408]{1,0:T(8,128)(2,1)} %get-tuple-element.51), channel_id=1, source_target_pairs={{0,24},{4,28},{8,16},{12,20},{16,8},{20,12},{24,0},{28,4},{1,25},{... | collective-permute-start | bytes 1081352 | tf_op jit(solution)/shard_map/ppermute | solution.py:33
  71.0 50.7 %collective-permute-start.17 = (bf16[256,1408]{1,0:T(8,128)(2,1)}, bf16[256,1408]{1,0:T(8,128)(2,1)S(1)}, u32[]{:S(2)}, u32[]{:S(2)}) collective-permute-start(bf16[256,1408]{1,0:T(8,128)(2,1)} %get-tuple-element.47.refs_8_), channel_id=1, source_target_pairs={{0,4},{4,0},{8,12},{12,8},{16,20},{20,16},{24,28},{28,24},{1,5},{5... | collective-permute-start | bytes 2162696 | tf_op jit(solution)/shard_map/ppermute | solution.py:33
  72.9 50.9 %collective-permute-start.18 = (bf16[256,1408]{1,0:T(8,128)(2,1)}, bf16[256,1408]{1,0:T(8,128)(2,1)S(1)}, u32[]{:S(2)}, u32[]{:S(2)}) collective-permute-start(bf16[256,1408]{1,0:T(8,128)(2,1)} %get-tuple-element.48), channel_id=1, source_target_pairs={{0,8},{4,12},{8,0},{12,4},{16,24},{20,28},{24,16},{28,20},{1,9},{5... | collective-permute-start | bytes 2162696 | tf_op jit(solution)/shard_map/ppermute | solution.py:33
  72.9 27.2 %collective-permute-start.26 = (bf16[128,1408]{1,0:T(8,128)(2,1)}, bf16[128,1408]{1,0:T(8,128)(2,1)}, u32[]{:S(2)}, u32[]{:S(2)}) collective-permute-start(bf16[128,1408]{1,0:T(8,128)(2,1)} %get-tuple-element.52), channel_id=1, source_target_pairs={{0,24},{4,28},{8,16},{12,20},{16,8},{20,12},{24,0},{28,4},{1,25},{... | collective-permute-start | bytes 1081352 | tf_op jit(solution)/shard_map/ppermute | solution.py:33
  79.5 43.7 %collective-permute-start.11 = (bf16[128,2048]{1,0:T(8,128)(2,1)}, bf16[128,2048]{1,0:T(8,128)(2,1)S(1)}, u32[]{:S(2)}, u32[]{:S(2)}) collective-permute-start(bf16[128,2048]{1,0:T(8,128)(2,1)} %get-tuple-element.46.refs_0_), channel_id=1, source_target_pairs={{0,8},{4,12},{8,0},{12,4},{16,24},{20,28},{24,16},{28,20},{1,9},{5... | collective-permute-start | bytes 1572872 | tf_op jit(solution)/shard_map/ppermute | solution.py:33
  83.0 37.1 %collective-permute-start.29 = (bf16[704,256]{1,0:T(8,128)(2,1)}, bf16[704,256]{1,0:T(8,128)(2,1)S(1)}, u32[]{:S(2)}, u32[]{:S(2)}) collective-permute-start(bf16[704,256]{1,0:T(8,128)(2,1)} %get-tuple-element.54), channel_id=1, source_target_pairs={{0,8},{4,12},{8,0},{12,4},{16,24},{20,28},{24,16},{28,20},{1,9},{5... | collective-permute-start | bytes 1081352 | tf_op jit(solution)/shard_map/ppermute | solution.py:33
  100.1 24.1 %collective-permute-start.21 = (bf16[128,1408]{1,0:T(8,128)(2,1)S(1)}, bf16[128,1408]{1,0:T(8,128)(2,1)S(1)}, u32[]{:S(2)}, u32[]{:S(2)}) collective-permute-start(bf16[128,1408]{1,0:T(8,128)(2,1)S(1)} %collective-permute-done.20.refs_12_), channel_id=1, source_target_pairs={{0,4},{4,0},{8,12},{12,8},{16,20},{20,16},{24,28},{28,24},{1,5},{5... | collective-permute-start | bytes 1081352 | tf_op jit(solution)/shard_map/ppermute | solution.py:33
  121.7 18.1 %collective-permute-start.10 = (bf16[128,2048]{1,0:T(8,128)(2,1)}, bf16[128,2048]{1,0:T(8,128)(2,1)}, u32[]{:S(2)}, u32[]{:S(2)}) collective-permute-start(bf16[128,2048]{1,0:T(8,128)(2,1)} %get-tuple-element.46.refs_0_), channel_id=1, source_target_pairs={{0,2},{1,3},{2,0},{3,1},{4,6},{5,7},{6,4},{7,5},{8,10},{9,11},{10,... | collective-permute-start | bytes 1572872 | tf_op jit(solution)/shard_map/ppermute | solution.py:33
  123.2 24.4 %collective-permute-start.12 = (bf16[128,2048]{1,0:T(8,128)(2,1)S(1)}, bf16[128,2048]{1,0:T(8,128)(2,1)}, u32[]{:S(2)}, u32[]{:S(2)}) collective-permute-start(bf16[128,2048]{1,0:T(8,128)(2,1)S(1)} %collective-permute-done.11.refs_2_), channel_id=1, source_target_pairs={{0,2},{1,3},{2,0},{3,1},{4,6},{5,7},{6,4},{7,5},{8,10},{9,11},{10,... | collective-permute-start | bytes 1572872 | tf_op jit(solution)/shard_map/ppermute | solution.py:33
  124.9 21.9 %collective-permute-start.27 = (bf16[128,1408]{1,0:T(8,128)(2,1)}, bf16[128,1408]{1,0:T(8,128)(2,1)S(1)}, u32[]{:S(2)}, u32[]{:S(2)}) collective-permute-start(bf16[128,1408]{1,0:T(8,128)(2,1)} %collective-permute-done.26.refs_18_), channel_id=1, source_target_pairs={{0,4},{4,0},{8,12},{12,8},{16,20},{20,16},{24,28},{28,24},{1,5},{5... | collective-permute-start | bytes 1081352 | tf_op jit(solution)/shard_map/ppermute | solution.py:33
  132.1 29.2 %collective-permute-start.19 = (bf16[256,1408]{1,0:T(8,128)(2,1)S(1)}, bf16[256,1408]{1,0:T(8,128)(2,1)S(1)}, u32[]{:S(2)}, u32[]{:S(2)}) collective-permute-start(bf16[256,1408]{1,0:T(8,128)(2,1)S(1)} %collective-permute-done.18.refs_10_), channel_id=1, source_target_pairs={{0,4},{4,0},{8,12},{12,8},{16,20},{20,16},{24,28},{28,24},{1,5},{5... | collective-permute-start | bytes 2162696 | tf_op jit(solution)/shard_map/ppermute | solution.py:33
  139.8 23.1 %collective-permute-start.13 = (bf16[128,2048]{1,0:T(8,128)(2,1)}, bf16[128,2048]{1,0:T(8,128)(2,1)}, u32[]{:S(2)}, u32[]{:S(2)}) collective-permute-start(bf16[128,2048]{1,0:T(8,128)(2,1)} %get-tuple-element.46.refs_0_), channel_id=1, source_target_pairs={{0,1},{1,0},{2,3},{3,2},{4,5},{5,4},{6,7},{7,6},{8,9},{9,8},{10,11... | collective-permute-start | bytes 1572872 | tf_op jit(solution)/shard_map/ppermute | solution.py:33
  139.8 23.7 %collective-permute-start.14 = (bf16[128,2048]{1,0:T(8,128)(2,1)}, bf16[128,2048]{1,0:T(8,128)(2,1)}, u32[]{:S(2)}, u32[]{:S(2)}) collective-permute-start(bf16[128,2048]{1,0:T(8,128)(2,1)} %collective-permute-done.10.refs_1_), channel_id=1, source_target_pairs={{0,1},{1,0},{2,3},{3,2},{4,5},{5,4},{6,7},{7,6},{8,9},{9,8},{10,11... | collective-permute-start | bytes 1572872 | tf_op jit(solution)/shard_map/ppermute | solution.py:33
  147.6 17.8 %collective-permute-start.15 = (bf16[128,2048]{1,0:T(8,128)(2,1)S(1)}, bf16[128,2048]{1,0:T(8,128)(2,1)}, u32[]{:S(2)}, u32[]{:S(2)}) collective-permute-start(bf16[128,2048]{1,0:T(8,128)(2,1)S(1)} %collective-permute-done.11.refs_2_), channel_id=1, source_target_pairs={{0,1},{1,0},{2,3},{3,2},{4,5},{5,4},{6,7},{7,6},{8,9},{9,8},{10,11... | collective-permute-start | bytes 1572872 | tf_op jit(solution)/shard_map/ppermute | solution.py:33
  147.6 18.3 %collective-permute-start.16 = (bf16[128,2048]{1,0:T(8,128)(2,1)}, bf16[128,2048]{1,0:T(8,128)(2,1)}, u32[]{:S(2)}, u32[]{:S(2)}) collective-permute-start(bf16[128,2048]{1,0:T(8,128)(2,1)} %collective-permute-done.12.refs_3_), channel_id=1, source_target_pairs={{0,1},{1,0},{2,3},{3,2},{4,5},{5,4},{6,7},{7,6},{8,9},{9,8},{10,11... | collective-permute-start | bytes 1572872 | tf_op jit(solution)/shard_map/ppermute | solution.py:33
  161.3 22.9 %collective-permute-start.28 = (bf16[704,256]{1,0:T(8,128)(2,1)}, bf16[704,256]{1,0:T(8,128)(2,1)S(1)}, u32[]{:S(2)}, u32[]{:S(2)}) collective-permute-start(bf16[704,256]{1,0:T(8,128)(2,1)} %get-tuple-element.53.refs_0_), channel_id=1, source_target_pairs={{0,4},{4,0},{8,12},{12,8},{16,20},{20,16},{24,28},{28,24},{1,5},{5... | collective-permute-start | bytes 1081352 | tf_op jit(solution)/shard_map/ppermute | solution.py:33
  162.9 28.3 %collective-permute-start.35 = (bf16[704,128]{1,0:T(8,128)(2,1)}, bf16[704,128]{1,0:T(8,128)(2,1)}, u32[]{:S(2)}, u32[]{:S(2)}) collective-permute-start(bf16[704,128]{1,0:T(8,128)(2,1)} %get-tuple-element.61), channel_id=1, source_target_pairs={{0,16},{4,20},{8,24},{12,28},{16,0},{20,4},{24,8},{28,12},{1,17},{... | collective-permute-start | bytes 540680 | tf_op jit(solution)/shard_map/ppermute | solution.py:33
  163.5 29.3 %collective-permute-start.37 = (bf16[704,128]{1,0:T(8,128)(2,1)}, bf16[704,128]{1,0:T(8,128)(2,1)}, u32[]{:S(2)}, u32[]{:S(2)}) collective-permute-start(bf16[704,128]{1,0:T(8,128)(2,1)} %get-tuple-element.62), channel_id=1, source_target_pairs={{0,24},{4,28},{8,16},{12,20},{16,8},{20,12},{24,0},{28,4},{1,25},{... | collective-permute-start | bytes 540680 | tf_op jit(solution)/shard_map/ppermute | solution.py:33
  165.4 18.8 %collective-permute-start.30 = (bf16[704,256]{1,0:T(8,128)(2,1)}, bf16[704,256]{1,0:T(8,128)(2,1)S(1)}, u32[]{:S(2)}, u32[]{:S(2)}) collective-permute-start(bf16[704,256]{1,0:T(8,128)(2,1)} %copy-done.10), channel_id=1, source_target_pairs={{0,4},{4,0},{8,12},{12,8},{16,20},{20,16},{24,28},{28,24},{1,5},{5... | collective-permute-start | bytes 1081352 | tf_op jit(solution)/shard_map/ppermute | solution.py:33
  187.9 38.8 %collective-permute-start.31 = (bf16[512,1024]{1,0:T(8,128)(2,1)S(1)}, bf16[512,1024]{1,0:T(8,128)(2,1)S(1)}, u32[]{:S(2)}, u32[]{:S(2)}) collective-permute-start(bf16[512,1024]{1,0:T(8,128)(2,1)S(1)} %get-tuple-element.56), channel_id=1, source_target_pairs={{0,1},{1,0},{2,3},{3,2},{4,5},{5,4},{6,7},{7,6},{8,9},{9,8},{10,11... | collective-permute-start | bytes 3145736 | tf_op jit(solution)/shard_map/ppermute | solution.py:33
  187.9 16.0 %collective-permute-start.43 = (bf16[704,128]{1,0:T(8,128)(2,1)S(1)}, bf16[704,128]{1,0:T(8,128)(2,1)S(1)}, u32[]{:S(2)}, u32[]{:S(2)}) collective-permute-start(bf16[704,128]{1,0:T(8,128)(2,1)S(1)} %copy-done.39), channel_id=1, source_target_pairs={{0,16},{4,20},{8,24},{12,28},{16,0},{20,4},{24,8},{28,12},{1,17},{... | collective-permute-start | bytes 540680 | tf_op jit(solution)/shard_map/ppermute | solution.py:33
  189.8 15.6 %collective-permute-start.45 = (bf16[704,128]{1,0:T(8,128)(2,1)S(1)}, bf16[704,128]{1,0:T(8,128)(2,1)S(1)}, u32[]{:S(2)}, u32[]{:S(2)}) collective-permute-start(bf16[704,128]{1,0:T(8,128)(2,1)S(1)} %copy-done.38), channel_id=1, source_target_pairs={{0,24},{4,28},{8,16},{12,20},{16,8},{20,12},{24,0},{28,4},{1,25},{... | collective-permute-start | bytes 540680 | tf_op jit(solution)/shard_map/ppermute | solution.py:33
  230.3 20.2 %collective-permute-start.32 = (bf16[128,1024]{1,0:T(8,128)(2,1)}, bf16[128,1024]{1,0:T(8,128)(2,1)S(1)}, u32[]{:S(2)}, u32[]{:S(2)}) collective-permute-start(bf16[128,1024]{1,0:T(8,128)(2,1)} %get-tuple-element.58), channel_id=1, source_target_pairs={{0,2},{1,3},{2,0},{3,1},{4,6},{5,7},{6,4},{7,5},{8,10},{9,11},{10,... | collective-permute-start | bytes 786440 | tf_op jit(solution)/shard_map/ppermute | solution.py:33
  230.8 19.7 %collective-permute-start.33 = (bf16[128,1024]{1,0:T(8,128)(2,1)}, bf16[128,1024]{1,0:T(8,128)(2,1)S(1)}, u32[]{:S(2)}, u32[]{:S(2)}) collective-permute-start(bf16[128,1024]{1,0:T(8,128)(2,1)} %get-tuple-element.59), channel_id=1, source_target_pairs={{0,8},{4,12},{8,0},{12,4},{16,24},{20,28},{24,16},{28,20},{1,9},{5... | collective-permute-start | bytes 786440 | tf_op jit(solution)/shard_map/ppermute | solution.py:33
  232.2 18.3 %collective-permute-start.34 = (bf16[128,1024]{1,0:T(8,128)(2,1)}, bf16[128,1024]{1,0:T(8,128)(2,1)S(1)}, u32[]{:S(2)}, u32[]{:S(2)}) collective-permute-start(bf16[128,1024]{1,0:T(8,128)(2,1)} %get-tuple-element.60), channel_id=1, source_target_pairs={{0,10},{1,11},{2,8},{3,9},{4,14},{5,15},{6,12},{7,13},{8,2},{9,3},... | collective-permute-start | bytes 786440 | tf_op jit(solution)/shard_map/ppermute | solution.py:33
  (63 other events, 667.7 us)

commit v2 on v1

v2 whole, which is shorter than its diff:
```python
import functools

import jax
import jax.numpy as jnp
from jax import lax
from jax.experimental import pallas as pl
from jax.experimental.pallas import tpu as pltpu
from jax.sharding import PartitionSpec as P


HEAD = 64
WINDOW = 128

norm_eps = 1e-06
masked = -1e30


def swap(block, sp_mask=0, tp_mask=0):
    n_sp, n_tp = lax.axis_size("sp"), lax.axis_size("tp")
    if sp_mask and tp_mask:
        axis = ("sp", "tp")
        pairs = [
            (s * n_tp + t, (s ^ sp_mask) * n_tp + (t ^ tp_mask))
            for s in range(n_sp)
            for t in range(n_tp)
        ]
    elif sp_mask:
        axis, pairs = "sp", [(s, s ^ sp_mask) for s in range(n_sp)]
    elif tp_mask:
        axis, pairs = "tp", [(t, t ^ tp_mask) for t in range(n_tp)]
    else:
        return block
    return lax.ppermute(block, axis, pairs)


def edge_kernel(place_ref, docs_ref, k_ref, v_ref, kv_first_ref, kv_second_ref, doc_first_ref, doc_second_ref):
    even = place_ref[0] & 1 == 0
    last = k_ref.shape[0] - WINDOW
    kv_cols = k_ref.shape[1]
    for ref, cols in ((k_ref, slice(0, kv_cols)), (v_ref, slice(kv_cols, 2 * kv_cols))):
        head, tail = ref[:WINDOW, :], ref[last:, :]
        kv_first_ref[:, cols] = jnp.where(even, tail, head)
        kv_second_ref[:, cols] = jnp.where(even, head, tail)
    head, tail = docs_ref[:, :WINDOW], docs_ref[:, last:]
    doc_first_ref[...] = jnp.where(even, tail, head)
    doc_second_ref[...] = jnp.where(even, head, tail)


def attention_kernel(n_sp, n_out, place_ref, sinks_ref, docs_ref, q_ref, k_ref, v_ref, *refs):
    first_ref, second_ref, doc_first_ref, doc_second_ref = refs[:4]
    out_refs, attended = refs[4 : 4 + n_out], refs[4 + n_out]
    sp = place_ref[0]
    kv_cols = k_ref.shape[1]
    kv_heads = kv_cols // HEAD
    groups = q_ref.shape[1] // kv_cols
    count = q_ref.shape[0] // WINDOW
    span = 3 * WINDOW
    shape = (WINDOW, span)
    even = sp & 1 == 0
    offset = lax.broadcasted_iota(jnp.int32, shape, 1) - lax.broadcasted_iota(jnp.int32, shape, 0)
    near = (offset >= 0) & (offset <= 2 * WINDOW)
    ones = jnp.ones((span, HEAD), jnp.bfloat16)
    doc_first, doc_second = doc_first_ref[...], doc_second_ref[...]
    docs = jnp.concatenate(
        [
            jnp.where(sp == 0, -1, jnp.where(even, doc_second, doc_first)),
            docs_ref[...],
            jnp.where(sp == n_sp - 1, -1, jnp.where(even, doc_first, doc_second)),
        ],
        axis=1,
    )

    def band(own_ref, column, block):
        cols = slice(column, column + kv_cols)
        pieces = []
        for i in range(block - 1, block + 2):
            if 0 <= i < count:
                pieces.append(own_ref[i * WINDOW : (i + 1) * WINDOW, :])
            elif i < 0:
                pieces.append(jnp.where(even, second_ref[:, cols], first_ref[:, cols]))
            else:
                pieces.append(jnp.where(even, first_ref[:, cols], second_ref[:, cols]))
        return jnp.concatenate(pieces, axis=0)

    for block in range(count):
        rows = slice(block * WINDOW, (block + 1) * WINDOW)
        own_docs = docs[:, (block + 1) * WINDOW : (block + 2) * WINDOW]
        query_docs = jnp.broadcast_to(own_docs, (WINDOW, WINDOW)).T
        band_docs = docs[:, block * WINDOW : block * WINDOW + span]
        valid = near & (jnp.concatenate([query_docs] * 3, axis=1) == band_docs)
        keys, values = band(k_ref, 0, block), band(v_ref, kv_cols, block)
        queries = q_ref[rows, :] * HEAD ** (-0.5)
        outs = []
        for head in range(kv_heads):
            cols = slice(head * HEAD, (head + 1) * HEAD)
            key = keys[:, cols]
            value = jnp.concatenate([values[:, cols], ones], axis=1)
            for group in range(groups):
                index = head * groups + group
                scores = lax.dot_general(
                    queries[:, index * HEAD : (index + 1) * HEAD],
                    key,
                    (((1,), (1,)), ((), ())),
                    preferred_element_type=jnp.float32,
                )
                scores = jnp.where(valid, scores, masked)
                sink = sinks_ref[index]
                top = jnp.maximum(jnp.max(scores, axis=-1, keepdims=True), sink)
                expd = jnp.exp(scores - top).astype(jnp.bfloat16)
                both = jnp.dot(expd, value, preferred_element_type=jnp.float32)
                outs.append(both[:, :HEAD] / (both[:, HEAD:] + jnp.exp(sink - top)))
        attended[rows, :] = jnp.concatenate(outs, axis=1).astype(jnp.bfloat16)
    height = out_refs[0].shape[0]
    for i, out_ref in enumerate(out_refs):
        out_ref[...] = attended[pl.ds(pl.multiple_of((place_ref[1] ^ i) * height, height), height), :]


def attention(place, q_proj, k_proj, v_proj, doc_ids, sinks):
    tok_rows, kv_cols = k_proj.shape
    n_tp, n_sp = lax.axis_size("tp"), lax.axis_size("sp")
    doc_ids = doc_ids[None, :]
    kv_edge = jax.ShapeDtypeStruct((WINDOW, 2 * kv_cols), jnp.bfloat16)
    doc_edge = jax.ShapeDtypeStruct((1, WINDOW), jnp.int32)
    kv_first, kv_second, doc_first, doc_second = pl.pallas_call(
        edge_kernel,
        out_shape=(kv_edge, kv_edge, doc_edge, doc_edge),
        in_specs=[SMEM] + [VMEM] * 3,
        out_specs=(VMEM,) * 4,
        compiler_params=room(4),
    )(place, doc_ids, k_proj, v_proj)

    def trade(name, block):
        low = int(name.endswith("second"))
        pairs = [(i, i + 1) for i in range(low, n_sp - 1, 2)]
        return lax.ppermute(block, "sp", pairs + [(b, a) for a, b in pairs])

    edges = [trade("kv_first", kv_first), trade("kv_second", kv_second)]
    edges += [trade("doc_first", doc_first), trade("doc_second", doc_second)]
    own = jax.ShapeDtypeStruct((tok_rows // n_tp, q_proj.shape[1]), jnp.bfloat16)
    return pl.pallas_call(
        functools.partial(attention_kernel, n_sp, n_tp),
        out_shape=(own,) * n_tp,
        in_specs=[SMEM] * 2 + [VMEM] * 8,
        out_specs=(VMEM,) * n_tp,
        scratch_shapes=[pltpu.VMEM(q_proj.shape, jnp.bfloat16)],
        compiler_params=room(8),
        cost_estimate=pl.CostEstimate(
            flops=12 * tok_rows * WINDOW * q_proj.shape[1],
            bytes_accessed=1 << 20,
            transcendentals=0,
        ),
    )(place, sinks, doc_ids, q_proj, k_proj, v_proj, *edges)


SMEM = pl.BlockSpec(memory_space=pltpu.SMEM)
VMEM = pl.BlockSpec(memory_space=pltpu.VMEM)
ANY = pl.BlockSpec(memory_space=pl.ANY)
HBM = pl.BlockSpec(memory_space=pltpu.HBM)


def room(mebibytes):
    return pltpu.CompilerParams(vmem_limit_bytes=mebibytes << 20)


def pack_kernel(half, y_bits, wanted, place_ref, gate_ref, up_ref, *refs):
    whole = half // 128 * 128

    def fill(source, chosen):
        lower = source * half

        def store(start, value):
            for (_, low, high), ref in chosen:
                ref[:, start : start + value.shape[1]] = value[low:high]

        for start in range(0, whole, 128):
            for ref, shift in ((gate_ref, 0), (up_ref, 128)):
                store(2 * start + shift, ref[:, lower + start : lower + start + 128])
        if half > whole:
            rest = [ref[:, lower + whole : lower + half] for ref in (gate_ref, up_ref)]
            store(2 * whole, jnp.concatenate(rest, axis=1))

    for source in (0, 1):
        for parity in (0, 1):
            chosen = [(want, ref) for want, ref in zip(wanted, refs) if want[0] == parity]

            @pl.when((place_ref[0] >> y_bits) & 1 == source ^ parity)
            def _():
                fill(source, chosen)


def pack_gate_up(place, y_bits, w_gate, w_up, wanted):
    depth, width = w_gate.shape
    return pl.pallas_call(
        functools.partial(pack_kernel, width // 2, y_bits, wanted),
        out_shape=tuple(
            jax.ShapeDtypeStruct((high - low, width), jnp.bfloat16) for _, low, high in wanted
        ),
        in_specs=[SMEM, VMEM, VMEM],
        out_specs=(VMEM,) * len(wanted),
        compiler_params=room(8),
        cost_estimate=pl.CostEstimate(flops=4 * depth * width, bytes_accessed=6 * w_gate.size, transcendentals=0),
    )(place, w_gate, w_up)


def split_kernel(far_cuts, y_bits, place_ref, down_ref, *refs):
    half = refs[0].shape[0]
    for parity in (0, 1):
        targets = refs[parity * (1 + far_cuts) : (parity + 1) * (1 + far_cuts)]
        rows = pl.ds(pl.multiple_of(((place_ref[0] >> y_bits) & 1 ^ parity) * half, half), half)
        value = down_ref[rows, :]
        width = value.shape[1] // far_cuts
        targets[0][...] = value
        for cut in range(far_cuts):
            targets[1 + cut][...] = value[:, cut * width : (cut + 1) * width]


def split_down(place, y_bits, w_down, far_cuts):
    depth, width = w_down.shape
    near = jax.ShapeDtypeStruct((depth // 2, width), jnp.bfloat16)
    far = jax.ShapeDtypeStruct((depth // 2, width // far_cuts), jnp.bfloat16)
    halves = pl.pallas_call(
        functools.partial(split_kernel, far_cuts, y_bits),
        out_shape=((near,) + (far,) * far_cuts) * 2,
        in_specs=[SMEM, VMEM],
        out_specs=(VMEM,) * (2 * (1 + far_cuts)),
        compiler_params=room(8),
        cost_estimate=pl.CostEstimate(flops=depth * width, bytes_accessed=8 * depth * width, transcendentals=0),
    )(place, w_down)
    return halves[: 1 + far_cuts], halves[1 + far_cuts :]


def merge_kernel(keep_ref, other_ref, *out_refs):
    height = out_refs[0].shape[0]
    for i, out_ref in enumerate(out_refs):
        rows = pl.ds(i * height, height)
        total = keep_ref[rows, :].astype(jnp.float32) + other_ref[rows, :].astype(jnp.float32)
        out_ref[...] = total.astype(jnp.bfloat16)


def merge(keep, other, count):
    part = jax.ShapeDtypeStruct((keep.shape[0] // count, keep.shape[1]), jnp.bfloat16)
    return pl.pallas_call(
        merge_kernel,
        out_shape=(part,) * count,
        in_specs=[VMEM] * 2,
        out_specs=(VMEM,) * count,
        compiler_params=room(8),
        cost_estimate=pl.CostEstimate(flops=keep.size, bytes_accessed=6 * keep.size, transcendentals=0),
    )(keep, other)


def project_kernel(count, resid_ref, gain_ref, *refs):
    heads, weights, (middle_ref, normed_ref) = refs[:count], refs[count : 2 * count], refs[2 * count :]
    width = middle_ref.shape[1]
    tile = min(512, width)
    squares = jnp.zeros((middle_ref.shape[0], 1), jnp.float32)
    for lower in range(0, width, tile):
        cols = pl.ds(lower, tile)
        total = resid_ref[:, cols].astype(jnp.float32)
        for head, weight in zip(heads, weights):
            total += jnp.dot(head[...], weight[:, cols], preferred_element_type=jnp.float32)
        middle_ref[:, cols] = total
        squares += jnp.sum(total * total, axis=-1, keepdims=True)
    factor = lax.rsqrt(squares / width + norm_eps)
    for lower in range(0, width, tile):
        cols = pl.ds(lower, tile)
        normed_ref[:, cols] = (middle_ref[:, cols] * factor * gain_ref[:, cols]).astype(jnp.bfloat16)


def project(resid, gain, heads, weights):
    rows, width = resid.shape
    count = len(heads)
    return pl.pallas_call(
        functools.partial(project_kernel, count),
        out_shape=(
            jax.ShapeDtypeStruct((rows, width), jnp.float32),
            jax.ShapeDtypeStruct((rows, width), jnp.bfloat16),
        ),
        in_specs=[VMEM] * (2 + 2 * count),
        out_specs=(VMEM, VMEM),
        compiler_params=room(12),
        cost_estimate=pl.CostEstimate(
            flops=2 * rows * width * count * heads[0].shape[1], bytes_accessed=6 << 20, transcendentals=0
        ),
    )(resid, gain, *heads, *weights)


def hidden_kernel(n_rows, pair_bits, groups, with_total, last, place_ref, *refs):
    counts = [len(starts) for _, starts in groups]
    row_refs, refs = refs[:n_rows], refs[n_rows:]
    part_refs, refs = refs[: sum(counts)], refs[sum(counts) :]
    if with_total:
        total_ref, refs = refs[0], refs[1:]
    out_ref, rows, weight, row_sems, part_sems = refs
    pairs, span = len(counts), weight.shape[1]
    height = row_refs[0].shape[0]
    row_copies, part_copies = [], []
    index = 0
    for pair, count in enumerate(counts):
        columns = pl.ds(pl.multiple_of(((place_ref[0] >> pair_bits) ^ groups[pair][0]) * span, span), span)
        for i, ref in enumerate(row_refs):
            row_copies.append(
                pltpu.make_async_copy(
                    ref.at[:, columns], rows.at[pair, pl.ds(i * height, height)], row_sems.at[pair, i]
                )
            )
        for (mask, scale, shift), ref in zip(groups[pair][1], part_refs[index : index + count]):
            within = (place_ref[0] ^ mask) & ((1 << pair_bits) - 1)
            start = pl.multiple_of(within * scale + shift, ref.shape[0])
            part_copies.append(
                pltpu.make_async_copy(ref, weight.at[pair, pl.ds(start, ref.shape[0])], part_sems.at[index])
            )
            index += 1
    for copy in part_copies + row_copies:
        copy.start()
    for copy in part_copies:
        copy.wait()
    total_rows, width = rows.shape[1], weight.shape[2]
    tile = min(512, total_rows)
    for lower in range(0, total_rows, tile):
        part = pl.ds(lower, tile)
        for i in range(lower // height, (lower + tile) // height):
            for pair in range(pairs):
                row_copies[pair * n_rows + i].wait()
        for start in range(0, width, 256):
            size = min(256, width - start)
            cols = slice(start, start + size)
            both = total_ref[part, cols] if with_total else 0.0
            for pair in range(pairs):
                both += jnp.dot(rows[pair, part, :], weight[pair, :, cols], preferred_element_type=jnp.float32)
            if last:
                gate, up = both[:, : size // 2], both[:, size // 2 :]
                out_ref[part, start // 2 : (start + size) // 2] = (gate / (1.0 + jnp.exp(-gate)) * up).astype(
                    jnp.bfloat16
                )
            else:
                out_ref[part, cols] = both


def hidden_units(place, pair_bits, groups, row_blocks, parts, total, last):
    rows = sum(block.shape[0] for block in row_blocks)
    width = parts[0][0].shape[1]
    span = sum(part.shape[0] for part in parts[0])
    flat = [part for group in parts for part in group]
    out = jax.ShapeDtypeStruct((rows, width // 2), jnp.bfloat16)
    if not last:
        out = jax.ShapeDtypeStruct((rows, width), jnp.float32)
    return pl.pallas_call(
        functools.partial(
            hidden_kernel, len(row_blocks), pair_bits, groups, total is not None, last
        ),
        out_shape=out,
        in_specs=[SMEM]
        + [HBM] * (len(row_blocks) + len(flat))
        + ([VMEM] if total is not None else []),
        out_specs=VMEM,
        scratch_shapes=[
            pltpu.VMEM((len(parts), rows, span), jnp.bfloat16),
            pltpu.VMEM((len(parts), span, width), jnp.bfloat16),
            pltpu.SemaphoreType.DMA((len(parts), len(row_blocks))),
            pltpu.SemaphoreType.DMA((len(flat),)),
        ],
        cost_estimate=pl.CostEstimate(
            flops=2 * rows * width * span * len(parts),
            bytes_accessed=8 << 20,
            transcendentals=0,
        ),
        compiler_params=room(12),
    )(place, *row_blocks, *flat, *([total] if total is not None else []))


def down_kernel(pair_bits, masks, place_ref, hidden_ref, *refs):
    n_parts = len(masks)
    part_refs, (keep_ref, send_ref, weight, sems) = refs[:n_parts], refs[n_parts:]
    copies = []
    for i, ref in enumerate(part_refs):
        start = 0
        if n_parts > 1:
            within = (place_ref[0] ^ masks[i]) & ((1 << pair_bits) - 1)
            start = pl.multiple_of(within * ref.shape[1], ref.shape[1])
        copies.append(pltpu.make_async_copy(ref, weight.at[:, pl.ds(start, ref.shape[1])], sems.at[i]))
    for copy in copies:
        copy.start()
    for copy in copies:
        copy.wait()
    keep = keep_ref.shape[0]
    tile = min(256, keep)
    for target, base in ((send_ref, keep), (keep_ref, 0)):
        for lower in range(0, keep, tile):
            target[pl.ds(lower, tile), :] = jnp.dot(
                hidden_ref[pl.ds(base + lower, tile), :], weight[...], preferred_element_type=jnp.float32
            ).astype(jnp.bfloat16)


def down_rows(place, pair_bits, masks, hidden, parts):
    rows, depth = hidden.shape
    width = sum(part.shape[1] for part in parts)
    shape = jax.ShapeDtypeStruct((rows // 2, width), jnp.bfloat16)
    return pl.pallas_call(
        functools.partial(down_kernel, pair_bits, masks),
        out_shape=(shape, shape),
        in_specs=[SMEM, VMEM] + [HBM] * len(parts),
        out_specs=(VMEM, VMEM),
        scratch_shapes=[
            pltpu.VMEM((depth, width), jnp.bfloat16),
            pltpu.SemaphoreType.DMA((len(parts),)),
        ],
        cost_estimate=pl.CostEstimate(
            flops=2 * rows * width * depth, bytes_accessed=4 << 20, transcendentals=0
        ),
        compiler_params=room(8),
    )(place, hidden, *parts)


def finish_kernel(pair_bits, plan, per_chunk, place_ref, middle_ref, *refs):
    out_ref = refs[-1]
    for chunk, (pair, span, strips, pitch, shift) in enumerate(plan):
        base = ((place_ref[0] >> pair_bits) ^ pair) * span
        totals = refs[chunk * per_chunk : (chunk + 1) * per_chunk]
        width = totals[0].shape[1] // strips
        for strip in range(strips):
            start = base + (strip * pitch + shift)
            cols = pl.ds(pl.multiple_of(start, width), width)
            total = middle_ref[:, cols]
            for ref in totals:
                total += ref[:, strip * width : (strip + 1) * width].astype(jnp.float32)
            out_ref[:, cols] = total.astype(jnp.bfloat16)


def finish(place, pair_bits, plan, middle, chunks):
    count = len(chunks) * len(chunks[0])
    return pl.pallas_call(
        functools.partial(finish_kernel, pair_bits, plan, len(chunks[0])),
        out_shape=jax.ShapeDtypeStruct(middle.shape, jnp.bfloat16),
        in_specs=[SMEM] + [VMEM] * (1 + count),
        out_specs=VMEM,
        compiler_params=room(8),
        cost_estimate=pl.CostEstimate(
            flops=8 * middle.size, bytes_accessed=8 * middle.size, transcendentals=0
        ),
    )(place, middle, *[block for chunk in chunks for block in chunk])


def lay_out(parts, starts, axis):
    total = sum(part.shape[axis] for part in parts)
    shape = list(parts[0].shape)
    shape[axis] = total
    whole = jnp.zeros(shape, parts[0].dtype)
    for part, start in zip(parts, starts):
        whole = lax.dynamic_update_slice_in_dim(whole, part, start, axis)
    return whole


def y_count(n_sp):
    return 1 << ((n_sp.bit_length() - 1) // 2)


def shards(q_proj, k_proj, v_proj, doc_ids, sinks, resid, w_out, norm_gain, w_gate, w_up, w_down):
    n_sp, n_tp = lax.axis_size("sp"), lax.axis_size("tp")
    n_y = y_count(n_sp)
    n_z = n_sp // n_y
    y_bits = n_y.bit_length() - 1
    place = jnp.stack([lax.axis_index("sp"), lax.axis_index("tp")]).astype(jnp.int32)
    depth, piece = w_gate.shape[0], w_down.shape[1]

    gu_cuts = 2 if depth % 32 == 0 else 1
    down_cuts = 2 if piece % 256 == 0 else 1
    step = depth // gu_cuts
    cuts = [(cut * step, (cut + 1) * step) for cut in range(gu_cuts)]
    wanted = [[(1, 0, depth), (0, *cuts[0]), (1, *cuts[0])], [(0, 0, depth)]]
    wanted[1] += [(parity, *cut) for cut in cuts[1:] for parity in (0, 1)]
    gu_half = {}
    for group in wanted:
        packed = pack_gate_up(place, y_bits, w_gate, w_up, tuple(group))
        for (parity, low, high), value in zip(group, packed):
            gu_half[parity, low, high] = value
    down_half = split_down(place, y_bits, w_down, down_cuts)

    gu = {}
    for dz in range(n_z):
        cuts = 1 if dz < 2 else gu_cuts
        height = depth // cuts
        for cut in range(cuts):
            held = swap(gu_half[dz % 2, cut * height, (cut + 1) * height], dz * n_y)
            for dy in range(n_y):
                start = (dz * n_y + dy, depth, cut * height)
                gu.setdefault(dz // 2, []).append((swap(held, dy), start))
    down, cuts_of = {}, {}
    for dz in range(n_z):
        cuts = cuts_of[dz // 2] = 1 if dz < 2 else down_cuts
        for cut in range(cuts):
            held = swap(down_half[dz % 2][cut + 1 if dz >= 2 else 0], dz * n_y)
            for dy in range(n_y):
                down[dz, cut, dy] = swap(held, dy)

    attended = attention(place, q_proj, k_proj, v_proj, doc_ids, sinks)

    out_blocks = {}
    for t in range(0, n_tp, 2):
        out_blocks[t] = swap(w_out, 0, t)
        out_blocks[t + 1] = swap(out_blocks[t], 0, 1)
    heads = [swap(attended[t], 0, t) for t in range(n_tp)]
    middle, normed = project(
        resid, norm_gain[None, :], heads, [out_blocks[t] for t in range(n_tp)]
    )

    rows = {(0, 0): normed, (1, 0): swap(normed, n_y)}
    for t in range(2, n_tp, 2):
        for a in (0, 1):
            rows[a, t] = swap(rows[a, 0], 0, t)
    for (a, t), block in list(rows.items()):
        rows[a, t + 1] = swap(block, 0, 1)
    order = [(a, t + c) for c in (0, 1) for a in (0, 1) for t in range(0, n_tp, 2)]

    blocks = [rows[key] for key in order]
    hidden = None
    for pairs in ([0], list(range(1, n_z // 2))):
        hidden = hidden_units(
            place,
            y_bits + 1,
            [(pair, [start for _, start in gu[pair]]) for pair in pairs],
            blocks,
            [[part for part, _ in gu[pair]] for pair in pairs],
            hidden,
            pairs[0] > 0,
        )

    span = 2 * n_y * piece
    plan, chunks = [], []
    for pair, cuts in cuts_of.items():
        width = piece // cuts
        for cut in range(cuts):
            keys = [(2 * pair + b, dy) for b in (0, 1) for dy in range(n_y)]
            masks = [dz * n_y + dy for dz, dy in keys]
            parts = [down[dz, cut, dy] for dz, dy in keys]
            if width % 128:
                starts = [((place[0] ^ mask) % (2 * n_y)) * width for mask in masks]
                parts, masks = [lay_out(parts, starts, 1)], [0]
            keep, send = down_rows(place, y_bits + 1, masks, hidden, parts)
            other = swap(send, 0, 1)
            totals = merge(keep, other, len(order) // 2)
            plan.append((pair, span) + ((1, span, 0) if cuts == 1 else (2 * n_y, piece, cut * width)))
            chunks.append([swap(totals[i], a * n_y, t) for i, (a, t) in enumerate(order[: len(order) // 2])])
    return finish(place, y_bits + 1, plan, middle, chunks)


def solution(mesh):
    placed = (
        P("sp", "tp"),
        P("sp", "tp"),
        P("sp", "tp"),
        P("sp"),
        P("tp"),
        P(("sp", "tp"), None),
        P("tp", None),
        P(),
        P("sp", "tp"),
        P("sp", "tp"),
        P("tp", "sp"),
    )

    return jax.shard_map(shards, mesh=mesh, in_specs=placed, out_specs=P(("sp", "tp"), None), check_vma=False)
```

time: 255 us -> 261 us (1.024)
  waiting for transfers between devices: 120 us -> 150 us
  Pallas kernels: 44.5 us -> 29.4 us
  local copies, waits for them, and re-layouts: 21.2 us -> 14 us
    ppermute x47, waiting for transfers between devices: 120 us -> 147 us  [swap(): return lax.ppermute(block, axis, pairs)]
    pallas_call x3, Pallas kernels: 6.68 us -> 0.48 us  [merge(): pl.pallas_call(merge_kernel, out_shape=(part,) * count, in_specs=[VMEM] *...]
    unnamed x89 -> x32, local copies, waits for them, and re-layouts: 19.6 us -> 14 us
    pallas_call x8 -> x11, Pallas kernels: 33.4 us -> 28 us  [the longest x2 11.9 us: hidden_units(): pl.pallas_call(functools.partial(hidden_kernel, len(row_blocks), pair_bit...]
    pallas_call x1, Pallas kernels: 4.43 us -> 0.91 us  [project(): pl.pallas_call(functools.partial(project_kernel, count), out_shape=(jax.S...]
    ppermute x4, waiting for transfers between devices: 0.01 us -> 2.98 us  [trade(): return lax.ppermute(block, 'sp', pairs + [(b, a) for a, b in pairs])]
    ppermute x47, starting transfers between devices: 58.7 us -> 61.3 us  [swap(): return lax.ppermute(block, axis, pairs)]
  transfers between devices with their start and end apart: 51 -> 51, of which waited for: 14 -> 23; matrix products, arithmetic and copies ran while one was open for 2% -> 0% of each run, Pallas kernels for 16% -> 11%
where the time goes in v2:
time: 261 us
  waiting for transfers between devices  150 us (57%)
  starting transfers between devices  67.1 us (26%)
  Pallas kernels  29.4 us (11%)
  local copies, waits for them, and re-layouts  14 us (5%)
    ppermute x47, waiting for transfers between devices, swap(): return lax.ppermute(block, axis, pairs)  147 us
    ppermute x47, starting transfers between devices, swap(): return lax.ppermute(block, axis, pairs)  61.3 us
    unnamed x32, local copies, waits for them, and re-layouts  14 us
    pallas_call x2, Pallas kernels, hidden_units(): pl.pallas_call(functools.partial(hidden_kernel, len(row_blocks), pair_bit...  11.9 us
    pallas_call x3, Pallas kernels, down_rows(): pl.pallas_call(functools.partial(down_kernel, pair_bits, masks), out_shap...  5.99 us
    ppermute x4, starting transfers between devices, trade(): return lax.ppermute(block, 'sp', pairs + [(b, a) for a, b in pairs])  5.77 us
  transfers between devices with their start and end apart: 51, of which 23 were waited for; matrix products, arithmetic and copies ran while one was open for 0% of the time, Pallas kernels for 11%

profile of v2, /device:TPU:0, one launch (start us, length us, event | category | flops | bytes accessed | tf_op | source)
XLA Modules:
  0.0 260.7 jit_solution(4154213466556892930)
XLA Ops:
  0.0 3.0 %collective-permute-start.8 = (bf16[256,2048]{1,0:T(8,128)(2,1)}, bf16[256,2048]{1,0:T(8,128)(2,1)S(1)}, u32[]{:S(2)}, u32[]{:S(2)}) collective-permute-start(bf16[256,2048]{1,0:T(8,128)(2,1)} %refs_4_.1), channel_id=1, source_target_pairs={{0,2},{1,3},{2,0},{3,1},{4,6},{5,7},{6,4},{7,5},{8,10},{9,11},{10,... | collective-permute-start | bytes 3145736 | tf_op jit(solution)/shard_map/ppermute | solution.py:33
  3.0 23.4 %collective-permute-done.8.refs_6_ = bf16[256,2048]{1,0:T(8,128)(2,1)S(1)} collective-permute-done((bf16[256,2048]{1,0:T(8,128)(2,1)}, bf16[256,2048]{1,0:T(8,128)(2,1)S(1)}, u32[]{:S(2)}, u32[]{:S(2)}) %collective-permute-start.8) | collective-permute-done | bytes 1048608 | tf_op jit(solution)/shard_map/ppermute | solution.py:33
  29.7 2.9 %collective-permute-start.17 = (bf16[128,1408]{1,0:T(8,128)(2,1)S(1)}, bf16[128,1408]{1,0:T(8,128)(2,1)S(1)}, u32[]{:S(2)}, u32[]{:S(2)}) collective-permute-start(bf16[128,1408]{1,0:T(8,128)(2,1)S(1)} %get-tuple-element.55), channel_id=1, source_target_pairs={{0,16},{4,20},{8,24},{12,28},{16,0},{20,4},{24,8},{28,12},{1,17},{... | collective-permute-start | bytes 1081352 | tf_op jit(solution)/shard_map/ppermute | solution.py:33
  39.3 2.9 %collective-permute-start = (bf16[128,256]{1,0:T(8,128)(2,1)S(1)}, bf16[128,256]{1,0:T(8,128)(2,1)S(1)}, u32[]{:S(2)}, u32[]{:S(2)}) collective-permute-start(bf16[128,256]{1,0:T(8,128)(2,1)S(1)} %get-tuple-element.45), channel_id=1, source_target_pairs={{0,4},{8,12},{16,20},{24,28},{4,0},{12,8},{20,16},{28,24},{1,5},{9... | collective-permute-start | bytes 196616 | tf_op jit(solution)/shard_map/ppermute | solution.py:135
  48.5 5.2 %shard_map.110 = (bf16[128,256]{1,0:T(8,128)(2,1)S(1)}, bf16[128,256]{1,0:T(8,128)(2,1)S(1)}, bf16[128,256]{1,0:T(8,128)(2,1)S(1)}, bf16[128,256]{1,0:T(8,128)(2,1)S(1)}) custom-call(s32[2]{0:T(128)S(1)} %pad_add_fusion.place_ref, f32[4]{0:T(128)S(1)} %copy-done.15, s32[1,512]{1,0:T(1,128)S(1)} %bitcast.6, bf16[512,256]{1,0:T(8,128)(2,1)S(1)} %copy-done.14, ...), custom_call_target="tpu_custom_call" | custom-call | flops 201326592 | bytes 1048576 | tf_op jit(solution)/shard_map/pallas_call | solution.py:140
  58.9 15.7 %collective-permute-start.19 = (bf16[128,1408]{1,0:T(8,128)(2,1)S(1)}, bf16[128,1408]{1,0:T(8,128)(2,1)S(1)}, u32[]{:S(2)}, u32[]{:S(2)}) collective-permute-start(bf16[128,1408]{1,0:T(8,128)(2,1)S(1)} %get-tuple-element.56), channel_id=1, source_target_pairs={{0,16},{4,20},{8,24},{12,28},{16,0},{20,4},{24,8},{28,12},{1,17},{... | collective-permute-start | bytes 1081352 | tf_op jit(solution)/shard_map/ppermute | solution.py:33
  78.5 4.4 %collective-permute-start.11 = (bf16[128,2048]{1,0:T(8,128)(2,1)S(1)}, bf16[128,2048]{1,0:T(8,128)(2,1)S(1)}, u32[]{:S(2)}, u32[]{:S(2)}) collective-permute-start(bf16[128,2048]{1,0:T(8,128)(2,1)S(1)} %get-tuple-element.54.refs_0_), channel_id=1, source_target_pairs={{0,8},{4,12},{8,0},{12,4},{16,24},{20,28},{24,16},{28,20},{1,9},{5... | collective-permute-start | bytes 1572872 | tf_op jit(solution)/shard_map/ppermute | solution.py:33
  84.4 10.0 %collective-permute-done.19.refs_10_ = bf16[128,1408]{1,0:T(8,128)(2,1)S(1)} collective-permute-done((bf16[128,1408]{1,0:T(8,128)(2,1)S(1)}, bf16[128,1408]{1,0:T(8,128)(2,1)S(1)}, u32[]{:S(2)}, u32[]{:S(2)}) %collective-permute-start.19) | collective-permute-done | bytes 360480 | tf_op jit(solution)/shard_map/ppermute | solution.py:33
  95.2 7.5 %collective-permute-start.29 = (bf16[704,256]{1,0:T(8,128)(2,1)S(1)}, bf16[704,256]{1,0:T(8,128)(2,1)S(1)}, u32[]{:S(2)}, u32[]{:S(2)}) collective-permute-start(bf16[704,256]{1,0:T(8,128)(2,1)S(1)} %get-tuple-element.62), channel_id=1, source_target_pairs={{0,8},{4,12},{8,0},{12,4},{16,24},{20,28},{24,16},{28,20},{1,9},{5... | collective-permute-start | bytes 1081352 | tf_op jit(solution)/shard_map/ppermute | solution.py:33
  102.6 23.0 %collective-permute-done.23.refs_14_ = bf16[128,1408]{1,0:T(8,128)(2,1)S(1)} collective-permute-done((bf16[128,1408]{1,0:T(8,128)(2,1)S(1)}, bf16[128,1408]{1,0:T(8,128)(2,1)S(1)}, u32[]{:S(2)}, u32[]{:S(2)}) %collective-permute-start.23) | collective-permute-done | bytes 360480 | tf_op jit(solution)/shard_map/ppermute | solution.py:33
  127.7 8.8 %collective-permute-done.29.refs_2_ = bf16[704,256]{1,0:T(8,128)(2,1)S(1)} collective-permute-done((bf16[704,256]{1,0:T(8,128)(2,1)S(1)}, bf16[704,256]{1,0:T(8,128)(2,1)S(1)}, u32[]{:S(2)}, u32[]{:S(2)}) %collective-permute-start.29) | collective-permute-done | bytes 360480 | tf_op jit(solution)/shard_map/ppermute | solution.py:33
  136.4 2.0 collective-permute-start.27
  138.4 2.0 collective-permute-done.10.refs_1_
  140.4 7.3 %collective-permute-done.18.refs_9_ = bf16[128,1408]{1,0:T(8,128)(2,1)S(1)} collective-permute-done((bf16[128,1408]{1,0:T(8,128)(2,1)S(1)}, bf16[128,1408]{1,0:T(8,128)(2,1)S(1)}, u32[]{:S(2)}, u32[]{:S(2)}) %collective-permute-start.18) | collective-permute-done | bytes 360480 | tf_op jit(solution)/shard_map/ppermute | solution.py:33
  147.7 1.9 collective-permute-done.12.refs_3_
  149.6 12.6 %collective-permute-done.27.refs_11_ = bf16[256,1408]{1,0:T(8,128)(2,1)S(1)} collective-permute-done((bf16[256,1408]{1,0:T(8,128)(2,1)S(1)}, bf16[256,1408]{1,0:T(8,128)(2,1)S(1)}, u32[]{:S(2)}, u32[]{:S(2)}) %collective-permute-start.27) | collective-permute-done | bytes 720928 | tf_op jit(solution)/shard_map/ppermute | solution.py:33
  162.5 1.7 collective-permute-start.22
  164.5 1.7 collective-permute-start.28
  166.6 5.8 %shard_map.114.refs_16_ = f32[1024,1408]{1,0:T(8,128)S(1)} custom-call(s32[2]{0:T(128)S(1)} %pad_add_fusion.place_ref, bf16[128,2048]{1,0:T(8,128)(2,1)S(1)} %get-tuple-element.54.refs_0_, bf16[128,2048]{1,0:T(8,128)(2,1)S(1)} %collective-permute-done.10.refs_1_, bf16[128,2048]{1,0:T(8,128)(2,1)S(1)} %collective-permute-done.11.refs_2_, ...), custom_call_target="tpu_custom_call" | custom-call | flops 2952790016 | bytes 8388608 | tf_op jit(solution)/shard_map/pallas_call | solution.py:348
  173.5 7.7 %collective-permute-done.22.refs_13_ = bf16[128,1408]{1,0:T(8,128)(2,1)S(1)} collective-permute-done((bf16[128,1408]{1,0:T(8,128)(2,1)S(1)}, bf16[128,1408]{1,0:T(8,128)(2,1)S(1)}, u32[]{:S(2)}, u32[]{:S(2)}) %collective-permute-start.22) | collective-permute-done | bytes 360480 | tf_op jit(solution)/shard_map/ppermute | solution.py:33
  181.6 7.4 %collective-permute-done.24.refs_15_ = bf16[128,1408]{1,0:T(8,128)(2,1)S(1)} collective-permute-done((bf16[128,1408]{1,0:T(8,128)(2,1)S(1)}, bf16[128,1408]{1,0:T(8,128)(2,1)S(1)}, u32[]{:S(2)}, u32[]{:S(2)}) %collective-permute-start.24) | collective-permute-done | bytes 360480 | tf_op jit(solution)/shard_map/ppermute | solution.py:33
  189.0 6.2 %shard_map.115.hidden_ref = bf16[1024,704]{1,0:T(8,128)(2,1)S(1)} custom-call(s32[2]{0:T(128)S(1)} %pad_add_fusion.place_ref, bf16[128,2048]{1,0:T(8,128)(2,1)S(1)} %get-tuple-element.54.refs_0_, bf16[128,2048]{1,0:T(8,128)(2,1)S(1)} %collective-permute-done.10.refs_1_, bf16[128,2048]{1,0:T(8,128)(2,1)S(1)} %collective-permute-done.11.refs_2_, ...), custom_call_target="tpu_custom_call" | custom-call | flops 2952790016 | bytes 8388608 | tf_op jit(solution)/shard_map/pallas_call | solution.py:348
  196.7 5.9 %collective-permute-done.30.refs_3_ = bf16[704,256]{1,0:T(8,128)(2,1)S(1)} collective-permute-done((bf16[704,256]{1,0:T(8,128)(2,1)S(1)}, bf16[704,256]{1,0:T(8,128)(2,1)S(1)}, u32[]{:S(2)}, u32[]{:S(2)}) %collective-permute-start.30) | collective-permute-done | bytes 360480 | tf_op jit(solution)/shard_map/ppermute | solution.py:33
  202.6 2.6 %shard_map.117 = (bf16[512,1024]{1,0:T(8,128)(2,1)S(1)}, bf16[512,1024]{1,0:T(8,128)(2,1)S(1)}) custom-call(s32[2]{0:T(128)S(1)} %pad_add_fusion.place_ref, bf16[1024,704]{1,0:T(8,128)(2,1)S(1)} %shard_map.115.hidden_ref, bf16[704,256]{1,0:T(8,128)(2,1)S(1)} %get-tuple-element.61.refs_0_, bf16[704,256]{1,0:T(8,128)(2,1)S(1)} %collective-permute-done.28.refs_1_, ...), custom_call_target="tpu_custom_call" | custom-call | flops 1476395008 | bytes 4194304 | tf_op jit(solution)/shard_map/pallas_call | solution.py:399
  205.4 1.9 collective-permute-start.37
  209.3 10.6 %collective-permute-done.35.refs_0_ = bf16[704,128]{1,0:T(8,128)(2,1)S(1)} collective-permute-done((bf16[704,128]{1,0:T(8,128)(2,1)S(1)}, bf16[704,128]{1,0:T(8,128)(2,1)S(1)}, u32[]{:S(2)}, u32[]{:S(2)}) %collective-permute-start.35) | collective-permute-done | bytes 180256 | tf_op jit(solution)/shard_map/ppermute | solution.py:33
  221.9 1.7 shard_map.121
  223.7 3.6 %collective-permute-done.36.refs_1_ = bf16[704,128]{1,0:T(8,128)(2,1)S(1)} collective-permute-done((bf16[704,128]{1,0:T(8,128)(2,1)S(1)}, bf16[704,128]{1,0:T(8,128)(2,1)S(1)}, u32[]{:S(2)}, u32[]{:S(2)}) %collective-permute-start.36) | collective-permute-done | bytes 180256 | tf_op jit(solution)/shard_map/ppermute | solution.py:33
  227.3 2.9 %collective-permute-done.38.refs_3_ = bf16[704,128]{1,0:T(8,128)(2,1)S(1)} collective-permute-done((bf16[704,128]{1,0:T(8,128)(2,1)S(1)}, bf16[704,128]{1,0:T(8,128)(2,1)S(1)}, u32[]{:S(2)}, u32[]{:S(2)}) %collective-permute-start.38) | collective-permute-done | bytes 180256 | tf_op jit(solution)/shard_map/ppermute | solution.py:33
  241.2 1.7 collective-permute-done.50.refs_11_
  246.1 10.9 %collective-permute-done.41.refs_6_ = bf16[128,512]{1,0:T(8,128)(2,1)S(1)} collective-permute-done((bf16[128,512]{1,0:T(8,128)(2,1)S(1)}, bf16[128,512]{1,0:T(8,128)(2,1)S(1)}, u32[]{:S(2)}, u32[]{:S(2)}) %collective-permute-start.41) | collective-permute-done | bytes 131104 | tf_op jit(solution)/shard_map/ppermute | solution.py:33
  257.0 2.0 collective-permute-done.42.refs_7_
  (118 shorter events, 53.8 us)
Async XLA Ops:
  0.0 26.3 %collective-permute-start.8 = (bf16[256,2048]{1,0:T(8,128)(2,1)}, bf16[256,2048]{1,0:T(8,128)(2,1)S(1)}, u32[]{:S(2)}, u32[]{:S(2)}) collective-permute-start(bf16[256,2048]{1,0:T(8,128)(2,1)} %refs_4_.1), channel_id=1, source_target_pairs={{0,2},{1,3},{2,0},{3,1},{4,6},{5,7},{6,4},{7,5},{8,10},{9,11},{10,... | collective-permute-start | bytes 3145736 | tf_op jit(solution)/shard_map/ppermute | solution.py:33
  3.0 71.6 %collective-permute-start.7 = (bf16[256,2048]{1,0:T(8,128)(2,1)}, bf16[256,2048]{1,0:T(8,128)(2,1)S(1)}, u32[]{:S(2)}, u32[]{:S(2)}) collective-permute-start(bf16[256,2048]{1,0:T(8,128)(2,1)} %refs_4_.1), channel_id=1, source_target_pairs={{0,1},{1,0},{2,3},{3,2},{4,5},{5,4},{6,7},{7,6},{8,9},{9,8},{10,11... | collective-permute-start | bytes 3145736 | tf_op jit(solution)/shard_map/ppermute | solution.py:33
  26.3 48.3 %collective-permute-start.9 = (bf16[256,2048]{1,0:T(8,128)(2,1)S(1)}, bf16[256,2048]{1,0:T(8,128)(2,1)S(1)}, u32[]{:S(2)}, u32[]{:S(2)}) collective-permute-start(bf16[256,2048]{1,0:T(8,128)(2,1)S(1)} %collective-permute-done.8.refs_6_), channel_id=1, source_target_pairs={{0,1},{1,0},{2,3},{3,2},{4,5},{5,4},{6,7},{7,6},{8,9},{9,8},{10,11... | collective-permute-start | bytes 3145736 | tf_op jit(solution)/shard_map/ppermute | solution.py:33
  29.7 53.3 %collective-permute-start.17 = (bf16[128,1408]{1,0:T(8,128)(2,1)S(1)}, bf16[128,1408]{1,0:T(8,128)(2,1)S(1)}, u32[]{:S(2)}, u32[]{:S(2)}) collective-permute-start(bf16[128,1408]{1,0:T(8,128)(2,1)S(1)} %get-tuple-element.55), channel_id=1, source_target_pairs={{0,16},{4,20},{8,24},{12,28},{16,0},{20,4},{24,8},{28,12},{1,17},{... | collective-permute-start | bytes 1081352 | tf_op jit(solution)/shard_map/ppermute | solution.py:33
  58.6 16.0 %collective-permute-start.6 = (bf16[128,256]{1,0:T(8,128)(2,1)S(1)}, bf16[128,256]{1,0:T(8,128)(2,1)S(1)}, u32[]{:S(2)}, u32[]{:S(2)}) collective-permute-start(bf16[128,256]{1,0:T(8,128)(2,1)S(1)} %get-tuple-element.52), channel_id=1, source_target_pairs={{0,3},{1,2},{2,1},{3,0},{4,7},{5,6},{6,5},{7,4},{8,11},{9,10},{10,... | collective-permute-start | bytes 196616 | tf_op jit(solution)/shard_map/ppermute | solution.py:33
  58.9 35.5 %collective-permute-start.19 = (bf16[128,1408]{1,0:T(8,128)(2,1)S(1)}, bf16[128,1408]{1,0:T(8,128)(2,1)S(1)}, u32[]{:S(2)}, u32[]{:S(2)}) collective-permute-start(bf16[128,1408]{1,0:T(8,128)(2,1)S(1)} %get-tuple-element.56), channel_id=1, source_target_pairs={{0,16},{4,20},{8,24},{12,28},{16,0},{20,4},{24,8},{28,12},{1,17},{... | collective-permute-start | bytes 1081352 | tf_op jit(solution)/shard_map/ppermute | solution.py:33
  74.6 20.5 %collective-permute-start.21 = (bf16[128,1408]{1,0:T(8,128)(2,1)S(1)}, bf16[128,1408]{1,0:T(8,128)(2,1)S(1)}, u32[]{:S(2)}, u32[]{:S(2)}) collective-permute-start(bf16[128,1408]{1,0:T(8,128)(2,1)S(1)} %get-tuple-element.57), channel_id=1, source_target_pairs={{0,24},{4,28},{8,16},{12,20},{16,8},{20,12},{24,0},{28,4},{1,25},{... | collective-permute-start | bytes 1081352 | tf_op jit(solution)/shard_map/ppermute | solution.py:33
  78.5 48.6 %collective-permute-start.11 = (bf16[128,2048]{1,0:T(8,128)(2,1)S(1)}, bf16[128,2048]{1,0:T(8,128)(2,1)S(1)}, u32[]{:S(2)}, u32[]{:S(2)}) collective-permute-start(bf16[128,2048]{1,0:T(8,128)(2,1)S(1)} %get-tuple-element.54.refs_0_), channel_id=1, source_target_pairs={{0,8},{4,12},{8,0},{12,4},{16,24},{20,28},{24,16},{28,20},{1,9},{5... | collective-permute-start | bytes 1572872 | tf_op jit(solution)/shard_map/ppermute | solution.py:33
  82.9 53.5 %collective-permute-start.26 = (bf16[256,1408]{1,0:T(8,128)(2,1)S(1)}, bf16[256,1408]{1,0:T(8,128)(2,1)S(1)}, u32[]{:S(2)}, u32[]{:S(2)}) collective-permute-start(bf16[256,1408]{1,0:T(8,128)(2,1)S(1)} %get-tuple-element.60), channel_id=1, source_target_pairs={{0,8},{4,12},{8,0},{12,4},{16,24},{20,28},{24,16},{28,20},{1,9},{5... | collective-permute-start | bytes 2162696 | tf_op jit(solution)/shard_map/ppermute | solution.py:33
  83.0 42.7 %collective-permute-start.23 = (bf16[128,1408]{1,0:T(8,128)(2,1)S(1)}, bf16[128,1408]{1,0:T(8,128)(2,1)S(1)}, u32[]{:S(2)}, u32[]{:S(2)}) collective-permute-start(bf16[128,1408]{1,0:T(8,128)(2,1)S(1)} %get-tuple-element.58), channel_id=1, source_target_pairs={{0,24},{4,28},{8,16},{12,20},{16,8},{20,12},{24,0},{28,4},{1,25},{... | collective-permute-start | bytes 1081352 | tf_op jit(solution)/shard_map/ppermute | solution.py:33
  94.4 44.1 %collective-permute-start.25 = (bf16[256,1408]{1,0:T(8,128)(2,1)S(1)}, bf16[256,1408]{1,0:T(8,128)(2,1)S(1)}, u32[]{:S(2)}, u32[]{:S(2)}) collective-permute-start(bf16[256,1408]{1,0:T(8,128)(2,1)S(1)} %get-tuple-element.59.refs_8_), channel_id=1, source_target_pairs={{0,4},{4,0},{8,12},{12,8},{16,20},{20,16},{24,28},{28,24},{1,5},{5... | collective-permute-start | bytes 2162696 | tf_op jit(solution)/shard_map/ppermute | solution.py:33
  95.2 41.2 %collective-permute-start.29 = (bf16[704,256]{1,0:T(8,128)(2,1)S(1)}, bf16[704,256]{1,0:T(8,128)(2,1)S(1)}, u32[]{:S(2)}, u32[]{:S(2)}) collective-permute-start(bf16[704,256]{1,0:T(8,128)(2,1)S(1)} %get-tuple-element.62), channel_id=1, source_target_pairs={{0,8},{4,12},{8,0},{12,4},{16,24},{20,28},{24,16},{28,20},{1,9},{5... | collective-permute-start | bytes 1081352 | tf_op jit(solution)/shard_map/ppermute | solution.py:33
  125.6 14.8 %collective-permute-start.10 = (bf16[128,2048]{1,0:T(8,128)(2,1)S(1)}, bf16[128,2048]{1,0:T(8,128)(2,1)S(1)}, u32[]{:S(2)}, u32[]{:S(2)}) collective-permute-start(bf16[128,2048]{1,0:T(8,128)(2,1)S(1)} %get-tuple-element.54.refs_0_), channel_id=1, source_target_pairs={{0,2},{1,3},{2,0},{3,1},{4,6},{5,7},{6,4},{7,5},{8,10},{9,11},{10,... | collective-permute-start | bytes 1572872 | tf_op jit(solution)/shard_map/ppermute | solution.py:33
  127.1 22.5 %collective-permute-start.12 = (bf16[128,2048]{1,0:T(8,128)(2,1)S(1)}, bf16[128,2048]{1,0:T(8,128)(2,1)S(1)}, u32[]{:S(2)}, u32[]{:S(2)}) collective-permute-start(bf16[128,2048]{1,0:T(8,128)(2,1)S(1)} %collective-permute-done.11.refs_2_), channel_id=1, source_target_pairs={{0,2},{1,3},{2,0},{3,1},{4,6},{5,7},{6,4},{7,5},{8,10},{9,11},{10,... | collective-permute-start | bytes 1572872 | tf_op jit(solution)/shard_map/ppermute | solution.py:33
  136.4 25.8 %collective-permute-start.27 = (bf16[256,1408]{1,0:T(8,128)(2,1)S(1)}, bf16[256,1408]{1,0:T(8,128)(2,1)S(1)}, u32[]{:S(2)}, u32[]{:S(2)}) collective-permute-start(bf16[256,1408]{1,0:T(8,128)(2,1)S(1)} %collective-permute-done.26.refs_10_), channel_id=1, source_target_pairs={{0,4},{4,0},{8,12},{12,8},{16,20},{20,16},{24,28},{28,24},{1,5},{5... | collective-permute-start | bytes 2162696 | tf_op jit(solution)/shard_map/ppermute | solution.py:33
  138.4 24.1 %collective-permute-start.13 = (bf16[128,2048]{1,0:T(8,128)(2,1)S(1)}, bf16[128,2048]{1,0:T(8,128)(2,1)S(1)}, u32[]{:S(2)}, u32[]{:S(2)}) collective-permute-start(bf16[128,2048]{1,0:T(8,128)(2,1)S(1)} %get-tuple-element.54.refs_0_), channel_id=1, source_target_pairs={{0,1},{1,0},{2,3},{3,2},{4,5},{5,4},{6,7},{7,6},{8,9},{9,8},{10,11... | collective-permute-start | bytes 1572872 | tf_op jit(solution)/shard_map/ppermute | solution.py:33
  140.4 23.8 %collective-permute-start.14 = (bf16[128,2048]{1,0:T(8,128)(2,1)S(1)}, bf16[128,2048]{1,0:T(8,128)(2,1)S(1)}, u32[]{:S(2)}, u32[]{:S(2)}) collective-permute-start(bf16[128,2048]{1,0:T(8,128)(2,1)S(1)} %collective-permute-done.10.refs_1_), channel_id=1, source_target_pairs={{0,1},{1,0},{2,3},{3,2},{4,5},{5,4},{6,7},{7,6},{8,9},{9,8},{10,11... | collective-permute-start | bytes 1572872 | tf_op jit(solution)/shard_map/ppermute | solution.py:33
  147.7 16.8 %collective-permute-start.15 = (bf16[128,2048]{1,0:T(8,128)(2,1)S(1)}, bf16[128,2048]{1,0:T(8,128)(2,1)S(1)}, u32[]{:S(2)}, u32[]{:S(2)}) collective-permute-start(bf16[128,2048]{1,0:T(8,128)(2,1)S(1)} %collective-permute-done.11.refs_2_), channel_id=1, source_target_pairs={{0,1},{1,0},{2,3},{3,2},{4,5},{5,4},{6,7},{7,6},{8,9},{9,8},{10,11... | collective-permute-start | bytes 1572872 | tf_op jit(solution)/shard_map/ppermute | solution.py:33
  149.6 16.7 %collective-permute-start.16 = (bf16[128,2048]{1,0:T(8,128)(2,1)S(1)}, bf16[128,2048]{1,0:T(8,128)(2,1)S(1)}, u32[]{:S(2)}, u32[]{:S(2)}) collective-permute-start(bf16[128,2048]{1,0:T(8,128)(2,1)S(1)} %collective-permute-done.12.refs_3_), channel_id=1, source_target_pairs={{0,1},{1,0},{2,3},{3,2},{4,5},{5,4},{6,7},{7,6},{8,9},{9,8},{10,11... | collective-permute-start | bytes 1572872 | tf_op jit(solution)/shard_map/ppermute | solution.py:33
  162.5 18.7 %collective-permute-start.22 = (bf16[128,1408]{1,0:T(8,128)(2,1)S(1)}, bf16[128,1408]{1,0:T(8,128)(2,1)S(1)}, u32[]{:S(2)}, u32[]{:S(2)}) collective-permute-start(bf16[128,1408]{1,0:T(8,128)(2,1)S(1)} %collective-permute-done.21.refs_12_), channel_id=1, source_target_pairs={{0,4},{4,0},{8,12},{12,8},{16,20},{20,16},{24,28},{28,24},{1,5},{5... | collective-permute-start | bytes 1081352 | tf_op jit(solution)/shard_map/ppermute | solution.py:33
  164.3 24.7 %collective-permute-start.24 = (bf16[128,1408]{1,0:T(8,128)(2,1)S(1)}, bf16[128,1408]{1,0:T(8,128)(2,1)S(1)}, u32[]{:S(2)}, u32[]{:S(2)}) collective-permute-start(bf16[128,1408]{1,0:T(8,128)(2,1)S(1)} %collective-permute-done.23.refs_14_), channel_id=1, source_target_pairs={{0,4},{4,0},{8,12},{12,8},{16,20},{20,16},{24,28},{28,24},{1,5},{5... | collective-permute-start | bytes 1081352 | tf_op jit(solution)/shard_map/ppermute | solution.py:33
  164.5 32.1 %collective-permute-start.28 = (bf16[704,256]{1,0:T(8,128)(2,1)S(1)}, bf16[704,256]{1,0:T(8,128)(2,1)S(1)}, u32[]{:S(2)}, u32[]{:S(2)}) collective-permute-start(bf16[704,256]{1,0:T(8,128)(2,1)S(1)} %get-tuple-element.61.refs_0_), channel_id=1, source_target_pairs={{0,4},{4,0},{8,12},{12,8},{16,20},{20,16},{24,28},{28,24},{1,5},{5... | collective-permute-start | bytes 1081352 | tf_op jit(solution)/shard_map/ppermute | solution.py:33
  166.3 36.3 %collective-permute-start.30 = (bf16[704,256]{1,0:T(8,128)(2,1)S(1)}, bf16[704,256]{1,0:T(8,128)(2,1)S(1)}, u32[]{:S(2)}, u32[]{:S(2)}) collective-permute-start(bf16[704,256]{1,0:T(8,128)(2,1)S(1)} %collective-permute-done.29.refs_2_), channel_id=1, source_target_pairs={{0,4},{4,0},{8,12},{12,8},{16,20},{20,16},{24,28},{28,24},{1,5},{5... | collective-permute-start | bytes 1081352 | tf_op jit(solution)/shard_map/ppermute | solution.py:33
  173.5 33.8 %collective-permute-start.43 = (bf16[704,128]{1,0:T(8,128)(2,1)S(1)}, bf16[704,128]{1,0:T(8,128)(2,1)S(1)}, u32[]{:S(2)}, u32[]{:S(2)}) collective-permute-start(bf16[704,128]{1,0:T(8,128)(2,1)S(1)} %get-tuple-element.77), channel_id=1, source_target_pairs={{0,16},{4,20},{8,24},{12,28},{16,0},{20,4},{24,8},{28,12},{1,17},{... | collective-permute-start | bytes 540680 | tf_op jit(solution)/shard_map/ppermute | solution.py:33
  181.2 26.6 %collective-permute-start.45 = (bf16[704,128]{1,0:T(8,128)(2,1)S(1)}, bf16[704,128]{1,0:T(8,128)(2,1)S(1)}, u32[]{:S(2)}, u32[]{:S(2)}) collective-permute-start(bf16[704,128]{1,0:T(8,128)(2,1)S(1)} %get-tuple-element.78), channel_id=1, source_target_pairs={{0,24},{4,28},{8,16},{12,20},{16,8},{20,12},{24,0},{28,4},{1,25},{... | collective-permute-start | bytes 540680 | tf_op jit(solution)/shard_map/ppermute | solution.py:33
  205.2 32.2 %collective-permute-start.31 = (bf16[512,1024]{1,0:T(8,128)(2,1)S(1)}, bf16[512,1024]{1,0:T(8,128)(2,1)S(1)}, u32[]{:S(2)}, u32[]{:S(2)}) collective-permute-start(bf16[512,1024]{1,0:T(8,128)(2,1)S(1)} %get-tuple-element.64), channel_id=1, source_target_pairs={{0,1},{1,0},{2,3},{3,2},{4,5},{5,4},{6,7},{7,6},{8,9},{9,8},{10,11... | collective-permute-start | bytes 3145736 | tf_op jit(solution)/shard_map/ppermute | solution.py:33
  205.3 14.6 %collective-permute-start.35 = (bf16[704,128]{1,0:T(8,128)(2,1)S(1)}, bf16[704,128]{1,0:T(8,128)(2,1)S(1)}, u32[]{:S(2)}, u32[]{:S(2)}) collective-permute-start(bf16[704,128]{1,0:T(8,128)(2,1)S(1)} %get-tuple-element.69), channel_id=1, source_target_pairs={{0,16},{4,20},{8,24},{12,28},{16,0},{20,4},{24,8},{28,12},{1,17},{... | collective-permute-start | bytes 540680 | tf_op jit(solution)/shard_map/ppermute | solution.py:33
  205.4 15.1 %collective-permute-start.37 = (bf16[704,128]{1,0:T(8,128)(2,1)S(1)}, bf16[704,128]{1,0:T(8,128)(2,1)S(1)}, u32[]{:S(2)}, u32[]{:S(2)}) collective-permute-start(bf16[704,128]{1,0:T(8,128)(2,1)S(1)} %get-tuple-element.70), channel_id=1, source_target_pairs={{0,24},{4,28},{8,16},{12,20},{16,8},{20,12},{24,0},{28,4},{1,25},{... | collective-permute-start | bytes 540680 | tf_op jit(solution)/shard_map/ppermute | solution.py:33
  207.3 14.7 %collective-permute-start.44 = (bf16[704,128]{1,0:T(8,128)(2,1)S(1)}, bf16[704,128]{1,0:T(8,128)(2,1)S(1)}, u32[]{:S(2)}, u32[]{:S(2)}) collective-permute-start(bf16[704,128]{1,0:T(8,128)(2,1)S(1)} %collective-permute-done.43.refs_0_), channel_id=1, source_target_pairs={{0,4},{4,0},{8,12},{12,8},{16,20},{20,16},{24,28},{28,24},{1,5},{5... | collective-permute-start | bytes 540680 | tf_op jit(solution)/shard_map/ppermute | solution.py:33
  237.6 21.4 %collective-permute-start.32 = (bf16[128,1024]{1,0:T(8,128)(2,1)S(1)}, bf16[128,1024]{1,0:T(8,128)(2,1)S(1)}, u32[]{:S(2)}, u32[]{:S(2)}) collective-permute-start(bf16[128,1024]{1,0:T(8,128)(2,1)S(1)} %get-tuple-element.66), channel_id=1, source_target_pairs={{0,2},{1,3},{2,0},{3,1},{4,6},{5,7},{6,4},{7,5},{8,10},{9,11},{10,... | collective-permute-start | bytes 786440 | tf_op jit(solution)/shard_map/ppermute | solution.py:33
  238.2 20.8 %collective-permute-start.33 = (bf16[128,1024]{1,0:T(8,128)(2,1)S(1)}, bf16[128,1024]{1,0:T(8,128)(2,1)S(1)}, u32[]{:S(2)}, u32[]{:S(2)}) collective-permute-start(bf16[128,1024]{1,0:T(8,128)(2,1)S(1)} %get-tuple-element.67), channel_id=1, source_target_pairs={{0,8},{4,12},{8,0},{12,4},{16,24},{20,28},{24,16},{28,20},{1,9},{5... | collective-permute-start | bytes 786440 | tf_op jit(solution)/shard_map/ppermute | solution.py:33
  240.1 19.0 %collective-permute-start.34 = (bf16[128,1024]{1,0:T(8,128)(2,1)S(1)}, bf16[128,1024]{1,0:T(8,128)(2,1)S(1)}, u32[]{:S(2)}, u32[]{:S(2)}) collective-permute-start(bf16[128,1024]{1,0:T(8,128)(2,1)S(1)} %get-tuple-element.68), channel_id=1, source_target_pairs={{0,10},{1,11},{2,8},{3,9},{4,14},{5,15},{6,12},{7,13},{8,2},{9,3},... | collective-permute-start | bytes 786440 | tf_op jit(solution)/shard_map/ppermute | solution.py:33
  (35 other events, 230.1 us)

commit v3 on v2

--- a/solution.py
+++ b/solution.py
@@ -33,7 +33,10 @@
     return lax.ppermute(block, axis, pairs)
 
 
-def edge_kernel(place_ref, docs_ref, k_ref, v_ref, kv_first_ref, kv_second_ref, doc_first_ref, doc_second_ref):
+def edge_kernel(place_ref, docs_ref, k_ref, v_ref, *refs):
+    kv_first_ref, kv_second_ref, doc_first_ref, doc_second_ref = refs[:4]
+    for source, target in zip((docs_ref, k_ref, v_ref), refs[4:]):
+        target[...] = source[...]
     even = place_ref[0] & 1 == 0
     last = k_ref.shape[0] - WINDOW
     kv_cols = k_ref.shape[1]
@@ -121,11 +124,12 @@
     doc_ids = doc_ids[None, :]
     kv_edge = jax.ShapeDtypeStruct((WINDOW, 2 * kv_cols), jnp.bfloat16)
     doc_edge = jax.ShapeDtypeStruct((1, WINDOW), jnp.int32)
-    kv_first, kv_second, doc_first, doc_second = pl.pallas_call(
+    same = [jax.ShapeDtypeStruct(array.shape, array.dtype) for array in (doc_ids, k_proj, v_proj)]
+    kv_first, kv_second, doc_first, doc_second, doc_ids, k_proj, v_proj = pl.pallas_call(
         edge_kernel,
-        out_shape=(kv_edge, kv_edge, doc_edge, doc_edge),
+        out_shape=(kv_edge, kv_edge, doc_edge, doc_edge, *same),
         in_specs=[SMEM] + [VMEM] * 3,
-        out_specs=(VMEM,) * 4,
+        out_specs=(VMEM,) * 7,
         compiler_params=room(4),
     )(place, doc_ids, k_proj, v_proj)
 
@@ -227,26 +231,6 @@
         cost_estimate=pl.CostEstimate(flops=depth * width, bytes_accessed=8 * depth * width, transcendentals=0),
     )(place, w_down)
     return halves[: 1 + far_cuts], halves[1 + far_cuts :]
-
-
-def merge_kernel(keep_ref, other_ref, *out_refs):
-    height = out_refs[0].shape[0]
-    for i, out_ref in enumerate(out_refs):
-        rows = pl.ds(i * height, height)
-        total = keep_ref[rows, :].astype(jnp.float32) + other_ref[rows, :].astype(jnp.float32)
-        out_ref[...] = total.astype(jnp.bfloat16)
-
-
-def merge(keep, other, count):
-    part = jax.ShapeDtypeStruct((keep.shape[0] // count, keep.shape[1]), jnp.bfloat16)
-    return pl.pallas_call(
-        merge_kernel,
-        out_shape=(part,) * count,
-        in_specs=[VMEM] * 2,
-        out_specs=(VMEM,) * count,
-        compiler_params=room(8),
-        cost_estimate=pl.CostEstimate(flops=keep.size, bytes_accessed=6 * keep.size, transcendentals=0),
-    )(keep, other)
 
 
 def project_kernel(count, resid_ref, gain_ref, *refs):
@@ -369,13 +353,14 @@
     )(place, *row_blocks, *flat, *([total] if total is not None else []))
 
 
-def down_kernel(pair_bits, masks, place_ref, hidden_ref, *refs):
-    n_parts = len(masks)
-    part_refs, (keep_ref, send_ref, weight, sems) = refs[:n_parts], refs[n_parts:]
+def down_kernel(pair_bits, masks, base, n_out, place_ref, hidden_ref, *refs):
+    part_refs, refs = refs[: len(masks)], refs[len(masks) :]
+    other_ref, refs = (refs[0], refs[1:]) if n_out > 1 else (None, refs)
+    out_refs, (weight, sems) = refs[:n_out], refs[n_out:]
     copies = []
     for i, ref in enumerate(part_refs):
         start = 0
-        if n_parts > 1:
+        if len(masks) > 1:
             within = (place_ref[0] ^ masks[i]) & ((1 << pair_bits) - 1)
             start = pl.multiple_of(within * ref.shape[1], ref.shape[1])
         copies.append(pltpu.make_async_copy(ref, weight.at[:, pl.ds(start, ref.shape[1])], sems.at[i]))
@@ -383,33 +368,36 @@
         copy.start()
     for copy in copies:
         copy.wait()
-    keep = keep_ref.shape[0]
-    tile = min(256, keep)
-    for target, base in ((send_ref, keep), (keep_ref, 0)):
-        for lower in range(0, keep, tile):
-            target[pl.ds(lower, tile), :] = jnp.dot(
-                hidden_ref[pl.ds(base + lower, tile), :], weight[...], preferred_element_type=jnp.float32
-            ).astype(jnp.bfloat16)
-
-
-def down_rows(place, pair_bits, masks, hidden, parts):
+    rows = hidden_ref.shape[0] // 2
+    height = rows // n_out
+    tile = min(256, rows)
+    for lower in range(0, rows, tile):
+        total = jnp.dot(
+            hidden_ref[pl.ds(base * rows + lower, tile), :], weight[...], preferred_element_type=jnp.float32
+        )
+        if n_out == 1:
+            out_refs[0][pl.ds(lower, tile), :] = total.astype(jnp.bfloat16)
+            continue
+        total = (total + other_ref[pl.ds(lower, tile), :].astype(jnp.float32)).astype(jnp.bfloat16)
+        for start in range(lower, lower + tile, height):
+            out_refs[start // height][...] = total[start - lower : start - lower + height]
+
+
+def down_rows(place, pair_bits, masks, hidden, parts, other, n_out):
     rows, depth = hidden.shape
     width = sum(part.shape[1] for part in parts)
-    shape = jax.ShapeDtypeStruct((rows // 2, width), jnp.bfloat16)
     return pl.pallas_call(
-        functools.partial(down_kernel, pair_bits, masks),
-        out_shape=(shape, shape),
-        in_specs=[SMEM, VMEM] + [HBM] * len(parts),
-        out_specs=(VMEM, VMEM),
+        functools.partial(down_kernel, pair_bits, masks, 1 if other is None else 0, n_out),
+        out_shape=(jax.ShapeDtypeStruct((rows // 2 // n_out, width), jnp.bfloat16),) * n_out,
+        in_specs=[SMEM, VMEM] + [HBM] * len(parts) + ([] if other is None else [VMEM]),
+        out_specs=(VMEM,) * n_out,
         scratch_shapes=[
             pltpu.VMEM((depth, width), jnp.bfloat16),
             pltpu.SemaphoreType.DMA((len(parts),)),
         ],
-        cost_estimate=pl.CostEstimate(
-            flops=2 * rows * width * depth, bytes_accessed=4 << 20, transcendentals=0
-        ),
         compiler_params=room(8),
-    )(place, hidden, *parts)
+        cost_estimate=pl.CostEstimate(flops=rows * width * depth, bytes_accessed=2 << 20, transcendentals=0),
+    )(place, hidden, *parts, *([] if other is None else [other]))
 
 
 def finish_kernel(pair_bits, plan, per_chunk, place_ref, middle_ref, *refs):
@@ -536,9 +524,9 @@
             if width % 128:
                 starts = [((place[0] ^ mask) % (2 * n_y)) * width for mask in masks]
                 parts, masks = [lay_out(parts, starts, 1)], [0]
-            keep, send = down_rows(place, y_bits + 1, masks, hidden, parts)
-            other = swap(send, 0, 1)
-            totals = merge(keep, other, len(order) // 2)
+            (sent,) = down_rows(place, y_bits + 1, masks, hidden, parts, None, 1)
+            other = swap(sent, 0, 1)
+            totals = down_rows(place, y_bits + 1, masks, hidden, parts, other, len(order) // 2)
             plan.append((pair, span) + ((1, span, 0) if cuts == 1 else (2 * n_y, piece, cut * width)))
             chunks.append([swap(totals[i], a * n_y, t) for i, (a, t) in enumerate(order[: len(order) // 2])])
     return finish(place, y_bits + 1, plan, middle, chunks)

time: 261 us -> 275 us (1.054)
  waiting for transfers between devices: 150 us -> 161 us
  starting transfers between devices: 67.1 us -> 70.3 us
    ppermute x47, waiting for transfers between devices: 147 us -> 158 us  [swap(): return lax.ppermute(block, axis, pairs)]
    ppermute x47, starting transfers between devices: 61.3 us -> 64.5 us  [swap(): return lax.ppermute(block, axis, pairs)]
    unnamed x32 -> x26, local copies, waits for them, and re-layouts: 14 us -> 11.5 us
  transfers between devices with their start and end apart: 51 -> 51, of which waited for: 23 -> 24; matrix products, arithmetic and copies ran while one was open for 0% -> 0% of each run, Pallas kernels for 11% -> 10%
where the time goes in v3:
time: 275 us
  waiting for transfers between devices  161 us (59%)
  starting transfers between devices  70.3 us (26%)
  Pallas kernels  31.7 us (12%)
  local copies, waits for them, and re-layouts  11.5 us (4%)
    ppermute x47, waiting for transfers between devices, swap(): return lax.ppermute(block, axis, pairs)  158 us
    ppermute x47, starting transfers between devices, swap(): return lax.ppermute(block, axis, pairs)  64.5 us
    pallas_call x2, Pallas kernels, hidden_units(): pl.pallas_call(functools.partial(hidden_kernel, len(row_blocks), pair_bit...  11.9 us
    unnamed x26, local copies, waits for them, and re-layouts  11.5 us
    pallas_call x6, Pallas kernels, down_rows(): pl.pallas_call(functools.partial(down_kernel, pair_bits, masks, 1 if othe...  8.73 us
    ppermute x4, starting transfers between devices, trade(): return lax.ppermute(block, 'sp', pairs + [(b, a) for a, b in pairs])  5.77 us
  transfers between devices with their start and end apart: 51, of which 24 were waited for; matrix products, arithmetic and copies ran while one was open for 0% of the time, Pallas kernels for 10%

profile of v3, /device:TPU:0, one launch (start us, length us, event | category | flops | bytes accessed | tf_op | source)
XLA Modules:
  0.0 274.6 jit_solution(10952104826729778423)
XLA Ops:
  0.0 3.0 %collective-permute-start.8 = (bf16[256,2048]{1,0:T(8,128)(2,1)}, bf16[256,2048]{1,0:T(8,128)(2,1)S(1)}, u32[]{:S(2)}, u32[]{:S(2)}) collective-permute-start(bf16[256,2048]{1,0:T(8,128)(2,1)} %refs_4_.1), channel_id=1, source_target_pairs={{0,2},{1,3},{2,0},{3,1},{4,6},{5,7},{6,4},{7,5},{8,10},{9,11},{10,... | collective-permute-start | bytes 3145736 | tf_op jit(solution)/shard_map/ppermute | solution.py:33
  3.0 23.4 %collective-permute-done.8.refs_6_ = bf16[256,2048]{1,0:T(8,128)(2,1)S(1)} collective-permute-done((bf16[256,2048]{1,0:T(8,128)(2,1)}, bf16[256,2048]{1,0:T(8,128)(2,1)S(1)}, u32[]{:S(2)}, u32[]{:S(2)}) %collective-permute-start.8) | collective-permute-done | bytes 1048608 | tf_op jit(solution)/shard_map/ppermute | solution.py:33
  29.7 2.9 %collective-permute-start.17 = (bf16[128,1408]{1,0:T(8,128)(2,1)S(1)}, bf16[128,1408]{1,0:T(8,128)(2,1)S(1)}, u32[]{:S(2)}, u32[]{:S(2)}) collective-permute-start(bf16[128,1408]{1,0:T(8,128)(2,1)S(1)} %get-tuple-element.55), channel_id=1, source_target_pairs={{0,16},{4,20},{8,24},{12,28},{16,0},{20,4},{24,8},{28,12},{1,17},{... | collective-permute-start | bytes 1081352 | tf_op jit(solution)/shard_map/ppermute | solution.py:33
  39.3 2.9 %collective-permute-start = (bf16[128,256]{1,0:T(8,128)(2,1)S(1)}, bf16[128,256]{1,0:T(8,128)(2,1)S(1)}, u32[]{:S(2)}, u32[]{:S(2)}) collective-permute-start(bf16[128,256]{1,0:T(8,128)(2,1)S(1)} %get-tuple-element.45), channel_id=1, source_target_pairs={{0,4},{8,12},{16,20},{24,28},{4,0},{12,8},{20,16},{28,24},{1,5},{9... | collective-permute-start | bytes 196616 | tf_op jit(solution)/shard_map/ppermute | solution.py:139
  46.1 5.2 %shard_map.110 = (bf16[128,256]{1,0:T(8,128)(2,1)S(1)}, bf16[128,256]{1,0:T(8,128)(2,1)S(1)}, bf16[128,256]{1,0:T(8,128)(2,1)S(1)}, bf16[128,256]{1,0:T(8,128)(2,1)S(1)}) custom-call(s32[2]{0:T(128)S(1)} %pad_add_fusion.place_ref, f32[4]{0:T(128)S(1)} %copy-done.12, s32[1,512]{1,0:T(1,128)S(1)} %get-tuple-element.42.docs_ref, ...), custom_call_target="tpu_custom_call" | custom-call | flops 201326592 | bytes 1048576 | tf_op jit(solution)/shard_map/pallas_call | solution.py:144
  56.1 15.7 %collective-permute-start.19 = (bf16[128,1408]{1,0:T(8,128)(2,1)S(1)}, bf16[128,1408]{1,0:T(8,128)(2,1)S(1)}, u32[]{:S(2)}, u32[]{:S(2)}) collective-permute-start(bf16[128,1408]{1,0:T(8,128)(2,1)S(1)} %get-tuple-element.56), channel_id=1, source_target_pairs={{0,16},{4,20},{8,24},{12,28},{16,0},{20,4},{24,8},{28,12},{1,17},{... | collective-permute-start | bytes 1081352 | tf_op jit(solution)/shard_map/ppermute | solution.py:33
  71.8 4.3 %collective-permute-done.6.refs_3_ = bf16[128,256]{1,0:T(8,128)(2,1)S(1)} collective-permute-done((bf16[128,256]{1,0:T(8,128)(2,1)S(1)}, bf16[128,256]{1,0:T(8,128)(2,1)S(1)}, u32[]{:S(2)}, u32[]{:S(2)}) %collective-permute-start.6) | collective-permute-done | bytes 65568 | tf_op jit(solution)/shard_map/ppermute | solution.py:33
  82.2 3.8 %collective-permute-start.23 = (bf16[128,1408]{1,0:T(8,128)(2,1)S(1)}, bf16[128,1408]{1,0:T(8,128)(2,1)S(1)}, u32[]{:S(2)}, u32[]{:S(2)}) collective-permute-start(bf16[128,1408]{1,0:T(8,128)(2,1)S(1)} %get-tuple-element.58), channel_id=1, source_target_pairs={{0,24},{4,28},{8,16},{12,20},{16,8},{20,12},{24,0},{28,4},{1,25},{... | collective-permute-start | bytes 1081352 | tf_op jit(solution)/shard_map/ppermute | solution.py:33
  86.0 5.4 %collective-permute-done.19.refs_10_ = bf16[128,1408]{1,0:T(8,128)(2,1)S(1)} collective-permute-done((bf16[128,1408]{1,0:T(8,128)(2,1)S(1)}, bf16[128,1408]{1,0:T(8,128)(2,1)S(1)}, u32[]{:S(2)}, u32[]{:S(2)}) %collective-permute-start.19) | collective-permute-done | bytes 360480 | tf_op jit(solution)/shard_map/ppermute | solution.py:33
  92.4 7.3 %collective-permute-start.29 = (bf16[704,256]{1,0:T(8,128)(2,1)S(1)}, bf16[704,256]{1,0:T(8,128)(2,1)S(1)}, u32[]{:S(2)}, u32[]{:S(2)}) collective-permute-start(bf16[704,256]{1,0:T(8,128)(2,1)S(1)} %get-tuple-element.62), channel_id=1, source_target_pairs={{0,8},{4,12},{8,0},{12,4},{16,24},{20,28},{24,16},{28,20},{1,9},{5... | collective-permute-start | bytes 1081352 | tf_op jit(solution)/shard_map/ppermute | solution.py:33
  99.7 24.0 %collective-permute-done.23.refs_14_ = bf16[128,1408]{1,0:T(8,128)(2,1)S(1)} collective-permute-done((bf16[128,1408]{1,0:T(8,128)(2,1)S(1)}, bf16[128,1408]{1,0:T(8,128)(2,1)S(1)}, u32[]{:S(2)}, u32[]{:S(2)}) %collective-permute-start.23) | collective-permute-done | bytes 360480 | tf_op jit(solution)/shard_map/ppermute | solution.py:33
  125.8 7.7 %collective-permute-done.29.refs_2_ = bf16[704,256]{1,0:T(8,128)(2,1)S(1)} collective-permute-done((bf16[704,256]{1,0:T(8,128)(2,1)S(1)}, bf16[704,256]{1,0:T(8,128)(2,1)S(1)}, u32[]{:S(2)}, u32[]{:S(2)}) %collective-permute-start.29) | collective-permute-done | bytes 360480 | tf_op jit(solution)/shard_map/ppermute | solution.py:33
  133.4 2.0 collective-permute-start.27
  135.5 3.1 %collective-permute-done.10.refs_1_ = bf16[128,2048]{1,0:T(8,128)(2,1)S(1)} collective-permute-done((bf16[128,2048]{1,0:T(8,128)(2,1)S(1)}, bf16[128,2048]{1,0:T(8,128)(2,1)S(1)}, u32[]{:S(2)}, u32[]{:S(2)}) %collective-permute-start.10) | collective-permute-done | bytes 524320 | tf_op jit(solution)/shard_map/ppermute | solution.py:33
  138.5 6.2 %collective-permute-done.18.refs_9_ = bf16[128,1408]{1,0:T(8,128)(2,1)S(1)} collective-permute-done((bf16[128,1408]{1,0:T(8,128)(2,1)S(1)}, bf16[128,1408]{1,0:T(8,128)(2,1)S(1)}, u32[]{:S(2)}, u32[]{:S(2)}) %collective-permute-start.18) | collective-permute-done | bytes 360480 | tf_op jit(solution)/shard_map/ppermute | solution.py:33
  144.7 2.6 collective-permute-done.12.refs_3_
  147.3 11.9 %collective-permute-done.27.refs_11_ = bf16[256,1408]{1,0:T(8,128)(2,1)S(1)} collective-permute-done((bf16[256,1408]{1,0:T(8,128)(2,1)S(1)}, bf16[256,1408]{1,0:T(8,128)(2,1)S(1)}, u32[]{:S(2)}, u32[]{:S(2)}) %collective-permute-start.27) | collective-permute-done | bytes 720928 | tf_op jit(solution)/shard_map/ppermute | solution.py:33
  163.6 5.8 %shard_map.114.refs_16_ = f32[1024,1408]{1,0:T(8,128)S(1)} custom-call(s32[2]{0:T(128)S(1)} %pad_add_fusion.place_ref, bf16[128,2048]{1,0:T(8,128)(2,1)S(1)} %get-tuple-element.54.refs_0_, bf16[128,2048]{1,0:T(8,128)(2,1)S(1)} %collective-permute-done.10.refs_1_, bf16[128,2048]{1,0:T(8,128)(2,1)S(1)} %collective-permute-done.11.refs_2_, ...), custom_call_target="tpu_custom_call" | custom-call | flops 2952790016 | bytes 8388608 | tf_op jit(solution)/shard_map/pallas_call | solution.py:332
  170.5 7.7 %collective-permute-done.22.refs_13_ = bf16[128,1408]{1,0:T(8,128)(2,1)S(1)} collective-permute-done((bf16[128,1408]{1,0:T(8,128)(2,1)S(1)}, bf16[128,1408]{1,0:T(8,128)(2,1)S(1)}, u32[]{:S(2)}, u32[]{:S(2)}) %collective-permute-start.22) | collective-permute-done | bytes 360480 | tf_op jit(solution)/shard_map/ppermute | solution.py:33
  178.2 7.7 %collective-permute-done.24.refs_15_ = bf16[128,1408]{1,0:T(8,128)(2,1)S(1)} collective-permute-done((bf16[128,1408]{1,0:T(8,128)(2,1)S(1)}, bf16[128,1408]{1,0:T(8,128)(2,1)S(1)}, u32[]{:S(2)}, u32[]{:S(2)}) %collective-permute-start.24) | collective-permute-done | bytes 360480 | tf_op jit(solution)/shard_map/ppermute | solution.py:33
  186.0 6.2 %shard_map.115.hidden_ref = bf16[1024,704]{1,0:T(8,128)(2,1)S(1)} custom-call(s32[2]{0:T(128)S(1)} %pad_add_fusion.place_ref, bf16[128,2048]{1,0:T(8,128)(2,1)S(1)} %get-tuple-element.54.refs_0_, bf16[128,2048]{1,0:T(8,128)(2,1)S(1)} %collective-permute-done.10.refs_1_, bf16[128,2048]{1,0:T(8,128)(2,1)S(1)} %collective-permute-done.11.refs_2_, ...), custom_call_target="tpu_custom_call" | custom-call | flops 2952790016 | bytes 8388608 | tf_op jit(solution)/shard_map/pallas_call | solution.py:332
  193.7 5.9 %collective-permute-done.30.refs_3_ = bf16[704,256]{1,0:T(8,128)(2,1)S(1)} collective-permute-done((bf16[704,256]{1,0:T(8,128)(2,1)S(1)}, bf16[704,256]{1,0:T(8,128)(2,1)S(1)}, u32[]{:S(2)}, u32[]{:S(2)}) %collective-permute-start.30) | collective-permute-done | bytes 360480 | tf_op jit(solution)/shard_map/ppermute | solution.py:33
  199.6 1.8 shard_map.117
  202.2 2.0 collective-permute-start.45
  204.2 1.9 collective-permute-start.35
  207.4 17.4 %collective-permute-done.43.refs_0_ = bf16[704,128]{1,0:T(8,128)(2,1)S(1)} collective-permute-done((bf16[704,128]{1,0:T(8,128)(2,1)S(1)}, bf16[704,128]{1,0:T(8,128)(2,1)S(1)}, u32[]{:S(2)}, u32[]{:S(2)}) %collective-permute-start.43) | collective-permute-done | bytes 180256 | tf_op jit(solution)/shard_map/ppermute | solution.py:33
  226.8 5.7 %collective-permute-done.35.refs_0_ = bf16[704,128]{1,0:T(8,128)(2,1)S(1)} collective-permute-done((bf16[704,128]{1,0:T(8,128)(2,1)S(1)}, bf16[704,128]{1,0:T(8,128)(2,1)S(1)}, u32[]{:S(2)}, u32[]{:S(2)}) %collective-permute-start.35) | collective-permute-done | bytes 180256 | tf_op jit(solution)/shard_map/ppermute | solution.py:33
  236.5 3.4 %collective-permute-done.36.refs_1_ = bf16[704,128]{1,0:T(8,128)(2,1)S(1)} collective-permute-done((bf16[704,128]{1,0:T(8,128)(2,1)S(1)}, bf16[704,128]{1,0:T(8,128)(2,1)S(1)}, u32[]{:S(2)}, u32[]{:S(2)}) %collective-permute-start.36) | collective-permute-done | bytes 180256 | tf_op jit(solution)/shard_map/ppermute | solution.py:33
  239.9 2.9 %collective-permute-done.38.refs_3_ = bf16[704,128]{1,0:T(8,128)(2,1)S(1)} collective-permute-done((bf16[704,128]{1,0:T(8,128)(2,1)S(1)}, bf16[704,128]{1,0:T(8,128)(2,1)S(1)}, u32[]{:S(2)}, u32[]{:S(2)}) %collective-permute-start.38) | collective-permute-done | bytes 180256 | tf_op jit(solution)/shard_map/ppermute | solution.py:33
  246.7 2.4 collective-permute-start.50
  251.0 1.8 shard_map.118
  259.3 12.2 %collective-permute-done.41.refs_6_ = bf16[128,512]{1,0:T(8,128)(2,1)S(1)} collective-permute-done((bf16[128,512]{1,0:T(8,128)(2,1)S(1)}, bf16[128,512]{1,0:T(8,128)(2,1)S(1)}, u32[]{:S(2)}, u32[]{:S(2)}) %collective-permute-start.41) | collective-permute-done | bytes 131104 | tf_op jit(solution)/shard_map/ppermute | solution.py:33
  (112 shorter events, 58.2 us)
Async XLA Ops:
  0.0 26.3 %collective-permute-start.8 = (bf16[256,2048]{1,0:T(8,128)(2,1)}, bf16[256,2048]{1,0:T(8,128)(2,1)S(1)}, u32[]{:S(2)}, u32[]{:S(2)}) collective-permute-start(bf16[256,2048]{1,0:T(8,128)(2,1)} %refs_4_.1), channel_id=1, source_target_pairs={{0,2},{1,3},{2,0},{3,1},{4,6},{5,7},{6,4},{7,5},{8,10},{9,11},{10,... | collective-permute-start | bytes 3145736 | tf_op jit(solution)/shard_map/ppermute | solution.py:33
  3.0 73.2 %collective-permute-start.7 = (bf16[256,2048]{1,0:T(8,128)(2,1)}, bf16[256,2048]{1,0:T(8,128)(2,1)S(1)}, u32[]{:S(2)}, u32[]{:S(2)}) collective-permute-start(bf16[256,2048]{1,0:T(8,128)(2,1)} %refs_4_.1), channel_id=1, source_target_pairs={{0,1},{1,0},{2,3},{3,2},{4,5},{5,4},{6,7},{7,6},{8,9},{9,8},{10,11... | collective-permute-start | bytes 3145736 | tf_op jit(solution)/shard_map/ppermute | solution.py:33
  26.3 49.8 %collective-permute-start.9 = (bf16[256,2048]{1,0:T(8,128)(2,1)S(1)}, bf16[256,2048]{1,0:T(8,128)(2,1)S(1)}, u32[]{:S(2)}, u32[]{:S(2)}) collective-permute-start(bf16[256,2048]{1,0:T(8,128)(2,1)S(1)} %collective-permute-done.8.refs_6_), channel_id=1, source_target_pairs={{0,1},{1,0},{2,3},{3,2},{4,5},{5,4},{6,7},{7,6},{8,9},{9,8},{10,11... | collective-permute-start | bytes 3145736 | tf_op jit(solution)/shard_map/ppermute | solution.py:33
  29.7 52.5 %collective-permute-start.17 = (bf16[128,1408]{1,0:T(8,128)(2,1)S(1)}, bf16[128,1408]{1,0:T(8,128)(2,1)S(1)}, u32[]{:S(2)}, u32[]{:S(2)}) collective-permute-start(bf16[128,1408]{1,0:T(8,128)(2,1)S(1)} %get-tuple-element.55), channel_id=1, source_target_pairs={{0,16},{4,20},{8,24},{12,28},{16,0},{20,4},{24,8},{28,12},{1,17},{... | collective-permute-start | bytes 1081352 | tf_op jit(solution)/shard_map/ppermute | solution.py:33
  51.3 20.5 %collective-permute-start.5 = (bf16[128,256]{1,0:T(8,128)(2,1)S(1)}, bf16[128,256]{1,0:T(8,128)(2,1)S(1)}, u32[]{:S(2)}, u32[]{:S(2)}) collective-permute-start(bf16[128,256]{1,0:T(8,128)(2,1)S(1)} %get-tuple-element.51), channel_id=1, source_target_pairs={{0,2},{1,3},{2,0},{3,1},{4,6},{5,7},{6,4},{7,5},{8,10},{9,11},{10,... | collective-permute-start | bytes 196616 | tf_op jit(solution)/shard_map/ppermute | solution.py:33
  56.1 35.3 %collective-permute-start.19 = (bf16[128,1408]{1,0:T(8,128)(2,1)S(1)}, bf16[128,1408]{1,0:T(8,128)(2,1)S(1)}, u32[]{:S(2)}, u32[]{:S(2)}) collective-permute-start(bf16[128,1408]{1,0:T(8,128)(2,1)S(1)} %get-tuple-element.56), channel_id=1, source_target_pairs={{0,16},{4,20},{8,24},{12,28},{16,0},{20,4},{24,8},{28,12},{1,17},{... | collective-permute-start | bytes 1081352 | tf_op jit(solution)/shard_map/ppermute | solution.py:33
  76.2 16.3 %collective-permute-start.21 = (bf16[128,1408]{1,0:T(8,128)(2,1)S(1)}, bf16[128,1408]{1,0:T(8,128)(2,1)S(1)}, u32[]{:S(2)}, u32[]{:S(2)}) collective-permute-start(bf16[128,1408]{1,0:T(8,128)(2,1)S(1)} %get-tuple-element.57), channel_id=1, source_target_pairs={{0,24},{4,28},{8,16},{12,20},{16,8},{20,12},{24,0},{28,4},{1,25},{... | collective-permute-start | bytes 1081352 | tf_op jit(solution)/shard_map/ppermute | solution.py:33
  80.1 44.2 %collective-permute-start.11 = (bf16[128,2048]{1,0:T(8,128)(2,1)S(1)}, bf16[128,2048]{1,0:T(8,128)(2,1)S(1)}, u32[]{:S(2)}, u32[]{:S(2)}) collective-permute-start(bf16[128,2048]{1,0:T(8,128)(2,1)S(1)} %get-tuple-element.54.refs_0_), channel_id=1, source_target_pairs={{0,8},{4,12},{8,0},{12,4},{16,24},{20,28},{24,16},{28,20},{1,9},{5... | collective-permute-start | bytes 1572872 | tf_op jit(solution)/shard_map/ppermute | solution.py:33
  80.5 52.9 %collective-permute-start.26 = (bf16[256,1408]{1,0:T(8,128)(2,1)S(1)}, bf16[256,1408]{1,0:T(8,128)(2,1)S(1)}, u32[]{:S(2)}, u32[]{:S(2)}) collective-permute-start(bf16[256,1408]{1,0:T(8,128)(2,1)S(1)} %get-tuple-element.60), channel_id=1, source_target_pairs={{0,8},{4,12},{8,0},{12,4},{16,24},{20,28},{24,16},{28,20},{1,9},{5... | collective-permute-start | bytes 2162696 | tf_op jit(solution)/shard_map/ppermute | solution.py:33
  82.2 41.6 %collective-permute-start.23 = (bf16[128,1408]{1,0:T(8,128)(2,1)S(1)}, bf16[128,1408]{1,0:T(8,128)(2,1)S(1)}, u32[]{:S(2)}, u32[]{:S(2)}) collective-permute-start(bf16[128,1408]{1,0:T(8,128)(2,1)S(1)} %get-tuple-element.58), channel_id=1, source_target_pairs={{0,24},{4,28},{8,16},{12,20},{16,8},{20,12},{24,0},{28,4},{1,25},{... | collective-permute-start | bytes 1081352 | tf_op jit(solution)/shard_map/ppermute | solution.py:33
  91.4 44.1 %collective-permute-start.25 = (bf16[256,1408]{1,0:T(8,128)(2,1)S(1)}, bf16[256,1408]{1,0:T(8,128)(2,1)S(1)}, u32[]{:S(2)}, u32[]{:S(2)}) collective-permute-start(bf16[256,1408]{1,0:T(8,128)(2,1)S(1)} %get-tuple-element.59.refs_8_), channel_id=1, source_target_pairs={{0,4},{4,0},{8,12},{12,8},{16,20},{20,16},{24,28},{28,24},{1,5},{5... | collective-permute-start | bytes 2162696 | tf_op jit(solution)/shard_map/ppermute | solution.py:33
  92.4 41.0 %collective-permute-start.29 = (bf16[704,256]{1,0:T(8,128)(2,1)S(1)}, bf16[704,256]{1,0:T(8,128)(2,1)S(1)}, u32[]{:S(2)}, u32[]{:S(2)}) collective-permute-start(bf16[704,256]{1,0:T(8,128)(2,1)S(1)} %get-tuple-element.62), channel_id=1, source_target_pairs={{0,8},{4,12},{8,0},{12,4},{16,24},{20,28},{24,16},{28,20},{1,9},{5... | collective-permute-start | bytes 1081352 | tf_op jit(solution)/shard_map/ppermute | solution.py:33
  123.7 14.8 %collective-permute-start.10 = (bf16[128,2048]{1,0:T(8,128)(2,1)S(1)}, bf16[128,2048]{1,0:T(8,128)(2,1)S(1)}, u32[]{:S(2)}, u32[]{:S(2)}) collective-permute-start(bf16[128,2048]{1,0:T(8,128)(2,1)S(1)} %get-tuple-element.54.refs_0_), channel_id=1, source_target_pairs={{0,2},{1,3},{2,0},{3,1},{4,6},{5,7},{6,4},{7,5},{8,10},{9,11},{10,... | collective-permute-start | bytes 1572872 | tf_op jit(solution)/shard_map/ppermute | solution.py:33
  124.3 23.0 %collective-permute-start.12 = (bf16[128,2048]{1,0:T(8,128)(2,1)S(1)}, bf16[128,2048]{1,0:T(8,128)(2,1)S(1)}, u32[]{:S(2)}, u32[]{:S(2)}) collective-permute-start(bf16[128,2048]{1,0:T(8,128)(2,1)S(1)} %collective-permute-done.11.refs_2_), channel_id=1, source_target_pairs={{0,2},{1,3},{2,0},{3,1},{4,6},{5,7},{6,4},{7,5},{8,10},{9,11},{10,... | collective-permute-start | bytes 1572872 | tf_op jit(solution)/shard_map/ppermute | solution.py:33
  133.4 25.8 %collective-permute-start.27 = (bf16[256,1408]{1,0:T(8,128)(2,1)S(1)}, bf16[256,1408]{1,0:T(8,128)(2,1)S(1)}, u32[]{:S(2)}, u32[]{:S(2)}) collective-permute-start(bf16[256,1408]{1,0:T(8,128)(2,1)S(1)} %collective-permute-done.26.refs_10_), channel_id=1, source_target_pairs={{0,4},{4,0},{8,12},{12,8},{16,20},{20,16},{24,28},{28,24},{1,5},{5... | collective-permute-start | bytes 2162696 | tf_op jit(solution)/shard_map/ppermute | solution.py:33
  135.5 24.1 %collective-permute-start.13 = (bf16[128,2048]{1,0:T(8,128)(2,1)S(1)}, bf16[128,2048]{1,0:T(8,128)(2,1)S(1)}, u32[]{:S(2)}, u32[]{:S(2)}) collective-permute-start(bf16[128,2048]{1,0:T(8,128)(2,1)S(1)} %get-tuple-element.54.refs_0_), channel_id=1, source_target_pairs={{0,1},{1,0},{2,3},{3,2},{4,5},{5,4},{6,7},{7,6},{8,9},{9,8},{10,11... | collective-permute-start | bytes 1572872 | tf_op jit(solution)/shard_map/ppermute | solution.py:33
  138.5 22.7 %collective-permute-start.14 = (bf16[128,2048]{1,0:T(8,128)(2,1)S(1)}, bf16[128,2048]{1,0:T(8,128)(2,1)S(1)}, u32[]{:S(2)}, u32[]{:S(2)}) collective-permute-start(bf16[128,2048]{1,0:T(8,128)(2,1)S(1)} %collective-permute-done.10.refs_1_), channel_id=1, source_target_pairs={{0,1},{1,0},{2,3},{3,2},{4,5},{5,4},{6,7},{7,6},{8,9},{9,8},{10,11... | collective-permute-start | bytes 1572872 | tf_op jit(solution)/shard_map/ppermute | solution.py:33
  144.7 16.8 %collective-permute-start.15 = (bf16[128,2048]{1,0:T(8,128)(2,1)S(1)}, bf16[128,2048]{1,0:T(8,128)(2,1)S(1)}, u32[]{:S(2)}, u32[]{:S(2)}) collective-permute-start(bf16[128,2048]{1,0:T(8,128)(2,1)S(1)} %collective-permute-done.11.refs_2_), channel_id=1, source_target_pairs={{0,1},{1,0},{2,3},{3,2},{4,5},{5,4},{6,7},{7,6},{8,9},{9,8},{10,11... | collective-permute-start | bytes 1572872 | tf_op jit(solution)/shard_map/ppermute | solution.py:33
  147.3 16.0 %collective-permute-start.16 = (bf16[128,2048]{1,0:T(8,128)(2,1)S(1)}, bf16[128,2048]{1,0:T(8,128)(2,1)S(1)}, u32[]{:S(2)}, u32[]{:S(2)}) collective-permute-start(bf16[128,2048]{1,0:T(8,128)(2,1)S(1)} %collective-permute-done.12.refs_3_), channel_id=1, source_target_pairs={{0,1},{1,0},{2,3},{3,2},{4,5},{5,4},{6,7},{7,6},{8,9},{9,8},{10,11... | collective-permute-start | bytes 1572872 | tf_op jit(solution)/shard_map/ppermute | solution.py:33
  159.5 18.7 %collective-permute-start.22 = (bf16[128,1408]{1,0:T(8,128)(2,1)S(1)}, bf16[128,1408]{1,0:T(8,128)(2,1)S(1)}, u32[]{:S(2)}, u32[]{:S(2)}) collective-permute-start(bf16[128,1408]{1,0:T(8,128)(2,1)S(1)} %collective-permute-done.21.refs_12_), channel_id=1, source_target_pairs={{0,4},{4,0},{8,12},{12,8},{16,20},{20,16},{24,28},{28,24},{1,5},{5... | collective-permute-start | bytes 1081352 | tf_op jit(solution)/shard_map/ppermute | solution.py:33
  161.3 24.7 %collective-permute-start.24 = (bf16[128,1408]{1,0:T(8,128)(2,1)S(1)}, bf16[128,1408]{1,0:T(8,128)(2,1)S(1)}, u32[]{:S(2)}, u32[]{:S(2)}) collective-permute-start(bf16[128,1408]{1,0:T(8,128)(2,1)S(1)} %collective-permute-done.23.refs_14_), channel_id=1, source_target_pairs={{0,4},{4,0},{8,12},{12,8},{16,20},{20,16},{24,28},{28,24},{1,5},{5... | collective-permute-start | bytes 1081352 | tf_op jit(solution)/shard_map/ppermute | solution.py:33
  161.5 32.1 %collective-permute-start.28 = (bf16[704,256]{1,0:T(8,128)(2,1)S(1)}, bf16[704,256]{1,0:T(8,128)(2,1)S(1)}, u32[]{:S(2)}, u32[]{:S(2)}) collective-permute-start(bf16[704,256]{1,0:T(8,128)(2,1)S(1)} %get-tuple-element.61.refs_0_), channel_id=1, source_target_pairs={{0,4},{4,0},{8,12},{12,8},{16,20},{20,16},{24,28},{28,24},{1,5},{5... | collective-permute-start | bytes 1081352 | tf_op jit(solution)/shard_map/ppermute | solution.py:33
  163.3 36.3 %collective-permute-start.30 = (bf16[704,256]{1,0:T(8,128)(2,1)S(1)}, bf16[704,256]{1,0:T(8,128)(2,1)S(1)}, u32[]{:S(2)}, u32[]{:S(2)}) collective-permute-start(bf16[704,256]{1,0:T(8,128)(2,1)S(1)} %collective-permute-done.29.refs_2_), channel_id=1, source_target_pairs={{0,4},{4,0},{8,12},{12,8},{16,20},{20,16},{24,28},{28,24},{1,5},{5... | collective-permute-start | bytes 1081352 | tf_op jit(solution)/shard_map/ppermute | solution.py:33
  201.4 49.6 %collective-permute-start.31 = (bf16[512,1024]{1,0:T(8,128)(2,1)S(1)}, bf16[512,1024]{1,0:T(8,128)(2,1)S(1)}, u32[]{:S(2)}, u32[]{:S(2)}) collective-permute-start(bf16[512,1024]{1,0:T(8,128)(2,1)S(1)} %shard_map.117), channel_id=1, source_target_pairs={{0,1},{1,0},{2,3},{3,2},{4,5},{5,4},{6,7},{7,6},{8,9},{9,8},{10,11... | collective-permute-start | bytes 3145736 | tf_op jit(solution)/shard_map/ppermute | solution.py:33
  201.5 23.3 %collective-permute-start.43 = (bf16[704,128]{1,0:T(8,128)(2,1)S(1)}, bf16[704,128]{1,0:T(8,128)(2,1)S(1)}, u32[]{:S(2)}, u32[]{:S(2)}) collective-permute-start(bf16[704,128]{1,0:T(8,128)(2,1)S(1)} %get-tuple-element.73), channel_id=1, source_target_pairs={{0,16},{4,20},{8,24},{12,28},{16,0},{20,4},{24,8},{28,12},{1,17},{... | collective-permute-start | bytes 540680 | tf_op jit(solution)/shard_map/ppermute | solution.py:33
  202.2 23.1 %collective-permute-start.45 = (bf16[704,128]{1,0:T(8,128)(2,1)S(1)}, bf16[704,128]{1,0:T(8,128)(2,1)S(1)}, u32[]{:S(2)}, u32[]{:S(2)}) collective-permute-start(bf16[704,128]{1,0:T(8,128)(2,1)S(1)} %get-tuple-element.74), channel_id=1, source_target_pairs={{0,24},{4,28},{8,16},{12,20},{16,8},{20,12},{24,0},{28,4},{1,25},{... | collective-permute-start | bytes 540680 | tf_op jit(solution)/shard_map/ppermute | solution.py:33
  204.2 28.3 %collective-permute-start.35 = (bf16[704,128]{1,0:T(8,128)(2,1)S(1)}, bf16[704,128]{1,0:T(8,128)(2,1)S(1)}, u32[]{:S(2)}, u32[]{:S(2)}) collective-permute-start(bf16[704,128]{1,0:T(8,128)(2,1)S(1)} %get-tuple-element.67), channel_id=1, source_target_pairs={{0,16},{4,20},{8,24},{12,28},{16,0},{20,4},{24,8},{28,12},{1,17},{... | collective-permute-start | bytes 540680 | tf_op jit(solution)/shard_map/ppermute | solution.py:33
  206.2 26.9 %collective-permute-start.37 = (bf16[704,128]{1,0:T(8,128)(2,1)S(1)}, bf16[704,128]{1,0:T(8,128)(2,1)S(1)}, u32[]{:S(2)}, u32[]{:S(2)}) collective-permute-start(bf16[704,128]{1,0:T(8,128)(2,1)S(1)} %get-tuple-element.68), channel_id=1, source_target_pairs={{0,24},{4,28},{8,16},{12,20},{16,8},{20,12},{24,0},{28,4},{1,25},{... | collective-permute-start | bytes 540680 | tf_op jit(solution)/shard_map/ppermute | solution.py:33
  252.8 20.1 %collective-permute-start.32 = (bf16[128,1024]{1,0:T(8,128)(2,1)S(1)}, bf16[128,1024]{1,0:T(8,128)(2,1)S(1)}, u32[]{:S(2)}, u32[]{:S(2)}) collective-permute-start(bf16[128,1024]{1,0:T(8,128)(2,1)S(1)} %get-tuple-element.64), channel_id=1, source_target_pairs={{0,2},{1,3},{2,0},{3,1},{4,6},{5,7},{6,4},{7,5},{8,10},{9,11},{10,... | collective-permute-start | bytes 786440 | tf_op jit(solution)/shard_map/ppermute | solution.py:33
  254.4 18.6 %collective-permute-start.33 = (bf16[128,1024]{1,0:T(8,128)(2,1)S(1)}, bf16[128,1024]{1,0:T(8,128)(2,1)S(1)}, u32[]{:S(2)}, u32[]{:S(2)}) collective-permute-start(bf16[128,1024]{1,0:T(8,128)(2,1)S(1)} %get-tuple-element.65), channel_id=1, source_target_pairs={{0,8},{4,12},{8,0},{12,4},{16,24},{20,28},{24,16},{28,20},{1,9},{5... | collective-permute-start | bytes 786440 | tf_op jit(solution)/shard_map/ppermute | solution.py:33
  254.9 18.0 %collective-permute-start.34 = (bf16[128,1024]{1,0:T(8,128)(2,1)S(1)}, bf16[128,1024]{1,0:T(8,128)(2,1)S(1)}, u32[]{:S(2)}, u32[]{:S(2)}) collective-permute-start(bf16[128,1024]{1,0:T(8,128)(2,1)S(1)} %get-tuple-element.66), channel_id=1, source_target_pairs={{0,10},{1,11},{2,8},{3,9},{4,14},{5,15},{6,12},{7,13},{8,2},{9,3},... | collective-permute-start | bytes 786440 | tf_op jit(solution)/shard_map/ppermute | solution.py:33
  256.4 15.2 %collective-permute-start.41 = (bf16[128,512]{1,0:T(8,128)(2,1)S(1)}, bf16[128,512]{1,0:T(8,128)(2,1)S(1)}, u32[]{:S(2)}, u32[]{:S(2)}) collective-permute-start(bf16[128,512]{1,0:T(8,128)(2,1)S(1)} %get-tuple-element.71), channel_id=1, source_target_pairs={{0,8},{4,12},{8,0},{12,4},{16,24},{20,28},{24,16},{28,20},{1,9},{5... | collective-permute-start | bytes 393224 | tf_op jit(solution)/shard_map/ppermute | solution.py:33
  (32 other events, 221.5 us)

commit v4 on v3

--- a/solution.py
+++ b/solution.py
@@ -206,31 +206,23 @@
     )(place, w_gate, w_up)
 
 
-def split_kernel(far_cuts, y_bits, place_ref, down_ref, *refs):
+def split_kernel(y_bits, place_ref, down_ref, *refs):
     half = refs[0].shape[0]
-    for parity in (0, 1):
-        targets = refs[parity * (1 + far_cuts) : (parity + 1) * (1 + far_cuts)]
-        rows = pl.ds(pl.multiple_of(((place_ref[0] >> y_bits) & 1 ^ parity) * half, half), half)
-        value = down_ref[rows, :]
-        width = value.shape[1] // far_cuts
-        targets[0][...] = value
-        for cut in range(far_cuts):
-            targets[1 + cut][...] = value[:, cut * width : (cut + 1) * width]
-
-
-def split_down(place, y_bits, w_down, far_cuts):
+    for parity, ref in enumerate(refs):
+        lower = pl.multiple_of(((place_ref[0] >> y_bits) & 1 ^ parity) * half, half)
+        ref[...] = down_ref[pl.ds(lower, half), :]
+
+
+def split_down(place, y_bits, w_down):
     depth, width = w_down.shape
-    near = jax.ShapeDtypeStruct((depth // 2, width), jnp.bfloat16)
-    far = jax.ShapeDtypeStruct((depth // 2, width // far_cuts), jnp.bfloat16)
-    halves = pl.pallas_call(
-        functools.partial(split_kernel, far_cuts, y_bits),
-        out_shape=((near,) + (far,) * far_cuts) * 2,
+    return pl.pallas_call(
+        functools.partial(split_kernel, y_bits),
+        out_shape=(jax.ShapeDtypeStruct((depth // 2, width), jnp.bfloat16),) * 2,
         in_specs=[SMEM, VMEM],
-        out_specs=(VMEM,) * (2 * (1 + far_cuts)),
+        out_specs=(VMEM,) * 2,
         compiler_params=room(8),
         cost_estimate=pl.CostEstimate(flops=depth * width, bytes_accessed=8 * depth * width, transcendentals=0),
     )(place, w_down)
-    return halves[: 1 + far_cuts], halves[1 + far_cuts :]
 
 
 def project_kernel(count, resid_ref, gain_ref, *refs):
@@ -353,7 +345,7 @@
     )(place, *row_blocks, *flat, *([total] if total is not None else []))
 
 
-def down_kernel(pair_bits, masks, base, n_out, place_ref, hidden_ref, *refs):
+def down_kernel(skip_bits, pair_bits, masks, base, n_out, place_ref, hidden_ref, *refs):
     part_refs, refs = refs[: len(masks)], refs[len(masks) :]
     other_ref, refs = (refs[0], refs[1:]) if n_out > 1 else (None, refs)
     out_refs, (weight, sems) = refs[:n_out], refs[n_out:]
@@ -361,7 +353,7 @@
     for i, ref in enumerate(part_refs):
         start = 0
         if len(masks) > 1:
-            within = (place_ref[0] ^ masks[i]) & ((1 << pair_bits) - 1)
+            within = ((place_ref[0] ^ masks[i]) & ((1 << pair_bits) - 1)) >> skip_bits
             start = pl.multiple_of(within * ref.shape[1], ref.shape[1])
         copies.append(pltpu.make_async_copy(ref, weight.at[:, pl.ds(start, ref.shape[1])], sems.at[i]))
     for copy in copies:
@@ -383,11 +375,11 @@
             out_refs[start // height][...] = total[start - lower : start - lower + height]
 
 
-def down_rows(place, pair_bits, masks, hidden, parts, other, n_out):
+def down_rows(place, skip_bits, pair_bits, masks, hidden, parts, other, n_out):
     rows, depth = hidden.shape
     width = sum(part.shape[1] for part in parts)
     return pl.pallas_call(
-        functools.partial(down_kernel, pair_bits, masks, 1 if other is None else 0, n_out),
+        functools.partial(down_kernel, skip_bits, pair_bits, masks, 1 if other is None else 0, n_out),
         out_shape=(jax.ShapeDtypeStruct((rows // 2 // n_out, width), jnp.bfloat16),) * n_out,
         in_specs=[SMEM, VMEM] + [HBM] * len(parts) + ([] if other is None else [VMEM]),
         out_specs=(VMEM,) * n_out,
@@ -402,8 +394,10 @@
 
 def finish_kernel(pair_bits, plan, per_chunk, place_ref, middle_ref, *refs):
     out_ref = refs[-1]
-    for chunk, (pair, span, strips, pitch, shift) in enumerate(plan):
+    for chunk, (pair, span, strips, dy) in enumerate(plan):
         base = ((place_ref[0] >> pair_bits) ^ pair) * span
+        pitch = span // strips
+        shift = 0 if dy is None else ((place_ref[0] & ((1 << pair_bits - 1) - 1)) ^ dy) * (pitch >> pair_bits - 1)
         totals = refs[chunk * per_chunk : (chunk + 1) * per_chunk]
         width = totals[0].shape[1] // strips
         for strip in range(strips):
@@ -452,7 +446,6 @@
     depth, piece = w_gate.shape[0], w_down.shape[1]
 
     gu_cuts = 2 if depth % 32 == 0 else 1
-    down_cuts = 2 if piece % 256 == 0 else 1
     step = depth // gu_cuts
     cuts = [(cut * step, (cut + 1) * step) for cut in range(gu_cuts)]
     wanted = [[(1, 0, depth), (0, *cuts[0]), (1, *cuts[0])], [(0, 0, depth)]]
@@ -462,7 +455,7 @@
         packed = pack_gate_up(place, y_bits, w_gate, w_up, tuple(group))
         for (parity, low, high), value in zip(group, packed):
             gu_half[parity, low, high] = value
-    down_half = split_down(place, y_bits, w_down, down_cuts)
+    down_half = split_down(place, y_bits, w_down)
 
     gu = {}
     for dz in range(n_z):
@@ -473,13 +466,11 @@
             for dy in range(n_y):
                 start = (dz * n_y + dy, depth, cut * height)
                 gu.setdefault(dz // 2, []).append((swap(held, dy), start))
-    down, cuts_of = {}, {}
+    down = {}
     for dz in range(n_z):
-        cuts = cuts_of[dz // 2] = 1 if dz < 2 else down_cuts
-        for cut in range(cuts):
-            held = swap(down_half[dz % 2][cut + 1 if dz >= 2 else 0], dz * n_y)
-            for dy in range(n_y):
-                down[dz, cut, dy] = swap(held, dy)
+        held = swap(down_half[dz % 2], dz * n_y)
+        for dy in range(n_y):
+            down[dz, dy] = swap(held, dy)
 
     attended = attention(place, q_proj, k_proj, v_proj, doc_ids, sinks)
 
@@ -515,19 +506,20 @@
 
     span = 2 * n_y * piece
     plan, chunks = [], []
-    for pair, cuts in cuts_of.items():
-        width = piece // cuts
-        for cut in range(cuts):
-            keys = [(2 * pair + b, dy) for b in (0, 1) for dy in range(n_y)]
+    for pair in range(n_z // 2):
+        groups = [[dy] for dy in range(n_y)] if pair and piece % 128 == 0 else [list(range(n_y))]
+        for group in groups:
+            keys = [(2 * pair + b, dy) for b in (0, 1) for dy in group]
             masks = [dz * n_y + dy for dz, dy in keys]
-            parts = [down[dz, cut, dy] for dz, dy in keys]
-            if width % 128:
-                starts = [((place[0] ^ mask) % (2 * n_y)) * width for mask in masks]
+            parts = [down[key] for key in keys]
+            if piece % 128:
+                starts = [((place[0] ^ mask) % (2 * n_y)) * piece for mask in masks]
                 parts, masks = [lay_out(parts, starts, 1)], [0]
-            (sent,) = down_rows(place, y_bits + 1, masks, hidden, parts, None, 1)
+            skip = y_bits if len(groups) > 1 else 0
+            (sent,) = down_rows(place, skip, y_bits + 1, masks, hidden, parts, None, 1)
             other = swap(sent, 0, 1)
-            totals = down_rows(place, y_bits + 1, masks, hidden, parts, other, len(order) // 2)
-            plan.append((pair, span) + ((1, span, 0) if cuts == 1 else (2 * n_y, piece, cut * width)))
+            totals = down_rows(place, skip, y_bits + 1, masks, hidden, parts, other, len(order) // 2)
+            plan.append((pair, span, 2, group[0]) if len(groups) > 1 else (pair, span, 1, None))
             chunks.append([swap(totals[i], a * n_y, t) for i, (a, t) in enumerate(order[: len(order) // 2])])
     return finish(place, y_bits + 1, plan, middle, chunks)
 

time: 275 us -> 254 us (0.924)
  waiting for transfers between devices: 161 us -> 144 us
  starting transfers between devices: 70.3 us -> 66.1 us
    ppermute x47 -> x43, waiting for transfers between devices: 158 us -> 141 us  [swap(): return lax.ppermute(block, axis, pairs)]
    ppermute x47 -> x43, starting transfers between devices: 64.5 us -> 60.4 us  [swap(): return lax.ppermute(block, axis, pairs)]
  transfers between devices with their start and end apart: 51 -> 47, of which waited for: 24 -> 22; matrix products, arithmetic and copies ran while one was open for 0% -> 0% of each run, Pallas kernels for 10% -> 12%
where the time goes in v4:
time: 254 us; the launch traced here: 253 us
  waiting for transfers between devices  144 us (57%)
  starting transfers between devices  66.1 us (26%)
  Pallas kernels  31.2 us (12%)
  local copies, waits for them, and re-layouts  11.5 us (5%)
    ppermute x43, waiting for transfers between devices, swap(): return lax.ppermute(block, axis, pairs)  141 us
    ppermute x43, starting transfers between devices, swap(): return lax.ppermute(block, axis, pairs)  60.4 us
    pallas_call x2, Pallas kernels, hidden_units(): pl.pallas_call(functools.partial(hidden_kernel, len(row_blocks), pair_bit...  11.9 us
    unnamed x26, local copies, waits for them, and re-layouts  11.5 us
    pallas_call x6, Pallas kernels, down_rows(): pl.pallas_call(functools.partial(down_kernel, skip_bits, pair_bits, masks...  8.38 us
    ppermute x4, starting transfers between devices, trade(): return lax.ppermute(block, 'sp', pairs + [(b, a) for a, b in pairs])  5.77 us
    pallas_call x1, Pallas kernels, attention(): pl.pallas_call(functools.partial(attention_kernel, n_sp, n_tp), out_shape...  5.18 us
  transfers between devices with their start and end apart: 47, of which 22 were waited for; matrix products, arithmetic and copies ran while one was open for 0% of the time, Pallas kernels for 12%

profile of v4, /device:TPU:0, one launch (start us, length us, event | category | flops | bytes accessed | tf_op | source)
XLA Modules:
  0.0 253.0 jit_solution(3870732083997953891)
XLA Ops:
  0.0 3.0 %collective-permute-start.8 = (bf16[256,2048]{1,0:T(8,128)(2,1)}, bf16[256,2048]{1,0:T(8,128)(2,1)S(1)}, u32[]{:S(2)}, u32[]{:S(2)}) collective-permute-start(bf16[256,2048]{1,0:T(8,128)(2,1)} %refs_4_.1), channel_id=1, source_target_pairs={{0,2},{1,3},{2,0},{3,1},{4,6},{5,7},{6,4},{7,5},{8,10},{9,11},{10,... | collective-permute-start | bytes 3145736 | tf_op jit(solution)/shard_map/ppermute | solution.py:33
  3.0 23.4 %collective-permute-done.8.refs_6_ = bf16[256,2048]{1,0:T(8,128)(2,1)S(1)} collective-permute-done((bf16[256,2048]{1,0:T(8,128)(2,1)}, bf16[256,2048]{1,0:T(8,128)(2,1)S(1)}, u32[]{:S(2)}, u32[]{:S(2)}) %collective-permute-start.8) | collective-permute-done | bytes 1048608 | tf_op jit(solution)/shard_map/ppermute | solution.py:33
  29.7 2.9 %collective-permute-start.17 = (bf16[128,1408]{1,0:T(8,128)(2,1)S(1)}, bf16[128,1408]{1,0:T(8,128)(2,1)S(1)}, u32[]{:S(2)}, u32[]{:S(2)}) collective-permute-start(bf16[128,1408]{1,0:T(8,128)(2,1)S(1)} %get-tuple-element.51), channel_id=1, source_target_pairs={{0,16},{4,20},{8,24},{12,28},{16,0},{20,4},{24,8},{28,12},{1,17},{... | collective-permute-start | bytes 1081352 | tf_op jit(solution)/shard_map/ppermute | solution.py:33
  39.3 2.9 %collective-permute-start = (bf16[128,256]{1,0:T(8,128)(2,1)S(1)}, bf16[128,256]{1,0:T(8,128)(2,1)S(1)}, u32[]{:S(2)}, u32[]{:S(2)}) collective-permute-start(bf16[128,256]{1,0:T(8,128)(2,1)S(1)} %get-tuple-element.41), channel_id=1, source_target_pairs={{0,4},{8,12},{16,20},{24,28},{4,0},{12,8},{20,16},{28,24},{1,5},{9... | collective-permute-start | bytes 196616 | tf_op jit(solution)/shard_map/ppermute | solution.py:139
  46.1 5.2 %shard_map.110 = (bf16[128,256]{1,0:T(8,128)(2,1)S(1)}, bf16[128,256]{1,0:T(8,128)(2,1)S(1)}, bf16[128,256]{1,0:T(8,128)(2,1)S(1)}, bf16[128,256]{1,0:T(8,128)(2,1)S(1)}) custom-call(s32[2]{0:T(128)S(1)} %pad_add_fusion.place_ref, f32[4]{0:T(128)S(1)} %copy-done.12, s32[1,512]{1,0:T(1,128)S(1)} %get-tuple-element.38.docs_ref, ...), custom_call_target="tpu_custom_call" | custom-call | flops 201326592 | bytes 1048576 | tf_op jit(solution)/shard_map/pallas_call | solution.py:144
  56.1 15.7 %collective-permute-start.19 = (bf16[128,1408]{1,0:T(8,128)(2,1)S(1)}, bf16[128,1408]{1,0:T(8,128)(2,1)S(1)}, u32[]{:S(2)}, u32[]{:S(2)}) collective-permute-start(bf16[128,1408]{1,0:T(8,128)(2,1)S(1)} %get-tuple-element.52), channel_id=1, source_target_pairs={{0,16},{4,20},{8,24},{12,28},{16,0},{20,4},{24,8},{28,12},{1,17},{... | collective-permute-start | bytes 1081352 | tf_op jit(solution)/shard_map/ppermute | solution.py:33
  71.8 4.3 %collective-permute-done.6.refs_3_ = bf16[128,256]{1,0:T(8,128)(2,1)S(1)} collective-permute-done((bf16[128,256]{1,0:T(8,128)(2,1)S(1)}, bf16[128,256]{1,0:T(8,128)(2,1)S(1)}, u32[]{:S(2)}, u32[]{:S(2)}) %collective-permute-start.6) | collective-permute-done | bytes 65568 | tf_op jit(solution)/shard_map/ppermute | solution.py:33
  82.2 3.8 %collective-permute-start.23 = (bf16[128,1408]{1,0:T(8,128)(2,1)S(1)}, bf16[128,1408]{1,0:T(8,128)(2,1)S(1)}, u32[]{:S(2)}, u32[]{:S(2)}) collective-permute-start(bf16[128,1408]{1,0:T(8,128)(2,1)S(1)} %get-tuple-element.54), channel_id=1, source_target_pairs={{0,24},{4,28},{8,16},{12,20},{16,8},{20,12},{24,0},{28,4},{1,25},{... | collective-permute-start | bytes 1081352 | tf_op jit(solution)/shard_map/ppermute | solution.py:33
  86.0 5.4 %collective-permute-done.19.refs_10_ = bf16[128,1408]{1,0:T(8,128)(2,1)S(1)} collective-permute-done((bf16[128,1408]{1,0:T(8,128)(2,1)S(1)}, bf16[128,1408]{1,0:T(8,128)(2,1)S(1)}, u32[]{:S(2)}, u32[]{:S(2)}) %collective-permute-start.19) | collective-permute-done | bytes 360480 | tf_op jit(solution)/shard_map/ppermute | solution.py:33
  92.3 7.4 %collective-permute-start.29 = (bf16[704,256]{1,0:T(8,128)(2,1)S(1)}, bf16[704,256]{1,0:T(8,128)(2,1)S(1)}, u32[]{:S(2)}, u32[]{:S(2)}) collective-permute-start(bf16[704,256]{1,0:T(8,128)(2,1)S(1)} %get-tuple-element.58), channel_id=1, source_target_pairs={{0,8},{4,12},{8,0},{12,4},{16,24},{20,28},{24,16},{28,20},{1,9},{5... | collective-permute-start | bytes 1081352 | tf_op jit(solution)/shard_map/ppermute | solution.py:33
  99.7 24.0 %collective-permute-done.23.refs_14_ = bf16[128,1408]{1,0:T(8,128)(2,1)S(1)} collective-permute-done((bf16[128,1408]{1,0:T(8,128)(2,1)S(1)}, bf16[128,1408]{1,0:T(8,128)(2,1)S(1)}, u32[]{:S(2)}, u32[]{:S(2)}) %collective-permute-start.23) | collective-permute-done | bytes 360480 | tf_op jit(solution)/shard_map/ppermute | solution.py:33
  125.8 7.7 %collective-permute-done.29.refs_2_ = bf16[704,256]{1,0:T(8,128)(2,1)S(1)} collective-permute-done((bf16[704,256]{1,0:T(8,128)(2,1)S(1)}, bf16[704,256]{1,0:T(8,128)(2,1)S(1)}, u32[]{:S(2)}, u32[]{:S(2)}) %collective-permute-start.29) | collective-permute-done | bytes 360480 | tf_op jit(solution)/shard_map/ppermute | solution.py:33
  133.4 2.0 collective-permute-start.27
  135.5 3.1 %collective-permute-done.10.refs_1_ = bf16[128,2048]{1,0:T(8,128)(2,1)S(1)} collective-permute-done((bf16[128,2048]{1,0:T(8,128)(2,1)S(1)}, bf16[128,2048]{1,0:T(8,128)(2,1)S(1)}, u32[]{:S(2)}, u32[]{:S(2)}) %collective-permute-start.10) | collective-permute-done | bytes 524320 | tf_op jit(solution)/shard_map/ppermute | solution.py:33
  138.5 6.2 %collective-permute-done.18.refs_9_ = bf16[128,1408]{1,0:T(8,128)(2,1)S(1)} collective-permute-done((bf16[128,1408]{1,0:T(8,128)(2,1)S(1)}, bf16[128,1408]{1,0:T(8,128)(2,1)S(1)}, u32[]{:S(2)}, u32[]{:S(2)}) %collective-permute-start.18) | collective-permute-done | bytes 360480 | tf_op jit(solution)/shard_map/ppermute | solution.py:33
  144.7 2.6 %collective-permute-done.12.refs_3_ = bf16[128,2048]{1,0:T(8,128)(2,1)S(1)} collective-permute-done((bf16[128,2048]{1,0:T(8,128)(2,1)S(1)}, bf16[128,2048]{1,0:T(8,128)(2,1)S(1)}, u32[]{:S(2)}, u32[]{:S(2)}) %collective-permute-start.12) | collective-permute-done | bytes 524320 | tf_op jit(solution)/shard_map/ppermute | solution.py:33
  147.3 11.9 %collective-permute-done.27.refs_11_ = bf16[256,1408]{1,0:T(8,128)(2,1)S(1)} collective-permute-done((bf16[256,1408]{1,0:T(8,128)(2,1)S(1)}, bf16[256,1408]{1,0:T(8,128)(2,1)S(1)}, u32[]{:S(2)}, u32[]{:S(2)}) %collective-permute-start.27) | collective-permute-done | bytes 720928 | tf_op jit(solution)/shard_map/ppermute | solution.py:33
  159.5 1.7 collective-permute-start.22
  161.5 1.7 collective-permute-start.28
  163.6 5.8 %shard_map.114.refs_16_ = f32[1024,1408]{1,0:T(8,128)S(1)} custom-call(s32[2]{0:T(128)S(1)} %pad_add_fusion.place_ref, bf16[128,2048]{1,0:T(8,128)(2,1)S(1)} %get-tuple-element.50.refs_0_, bf16[128,2048]{1,0:T(8,128)(2,1)S(1)} %collective-permute-done.10.refs_1_, bf16[128,2048]{1,0:T(8,128)(2,1)S(1)} %collective-permute-done.11.refs_2_, ...), custom_call_target="tpu_custom_call" | custom-call | flops 2952790016 | bytes 8388608 | tf_op jit(solution)/shard_map/pallas_call | solution.py:324
  171.2 7.0 %collective-permute-done.22.refs_13_ = bf16[128,1408]{1,0:T(8,128)(2,1)S(1)} collective-permute-done((bf16[128,1408]{1,0:T(8,128)(2,1)S(1)}, bf16[128,1408]{1,0:T(8,128)(2,1)S(1)}, u32[]{:S(2)}, u32[]{:S(2)}) %collective-permute-start.22) | collective-permute-done | bytes 360480 | tf_op jit(solution)/shard_map/ppermute | solution.py:33
  178.2 2.6 %collective-permute-start.36 = (bf16[704,256]{1,0:T(8,128)(2,1)S(1)}, bf16[704,256]{1,0:T(8,128)(2,1)S(1)}, u32[]{:S(2)}, u32[]{:S(2)}) collective-permute-start(bf16[704,256]{1,0:T(8,128)(2,1)S(1)} %get-tuple-element.58), channel_id=1, source_target_pairs={{0,24},{4,28},{8,16},{12,20},{16,8},{20,12},{24,0},{28,4},{1,25},{... | collective-permute-start | bytes 1081352 | tf_op jit(solution)/shard_map/ppermute | solution.py:33
  180.8 5.1 %collective-permute-done.24.refs_15_ = bf16[128,1408]{1,0:T(8,128)(2,1)S(1)} collective-permute-done((bf16[128,1408]{1,0:T(8,128)(2,1)S(1)}, bf16[128,1408]{1,0:T(8,128)(2,1)S(1)}, u32[]{:S(2)}, u32[]{:S(2)}) %collective-permute-start.24) | collective-permute-done | bytes 360480 | tf_op jit(solution)/shard_map/ppermute | solution.py:33
  186.0 6.2 %shard_map.115.hidden_ref = bf16[1024,704]{1,0:T(8,128)(2,1)S(1)} custom-call(s32[2]{0:T(128)S(1)} %pad_add_fusion.place_ref, bf16[128,2048]{1,0:T(8,128)(2,1)S(1)} %get-tuple-element.50.refs_0_, bf16[128,2048]{1,0:T(8,128)(2,1)S(1)} %collective-permute-done.10.refs_1_, bf16[128,2048]{1,0:T(8,128)(2,1)S(1)} %collective-permute-done.11.refs_2_, ...), custom_call_target="tpu_custom_call" | custom-call | flops 2952790016 | bytes 8388608 | tf_op jit(solution)/shard_map/pallas_call | solution.py:324
  193.7 5.9 %collective-permute-done.30.refs_3_ = bf16[704,256]{1,0:T(8,128)(2,1)S(1)} collective-permute-done((bf16[704,256]{1,0:T(8,128)(2,1)S(1)}, bf16[704,256]{1,0:T(8,128)(2,1)S(1)}, u32[]{:S(2)}, u32[]{:S(2)}) %collective-permute-start.30) | collective-permute-done | bytes 360480 | tf_op jit(solution)/shard_map/ppermute | solution.py:33
  199.6 1.8 shard_map.117
  203.6 9.3 %collective-permute-done.41.refs_0_ = bf16[704,256]{1,0:T(8,128)(2,1)S(1)} collective-permute-done((bf16[704,256]{1,0:T(8,128)(2,1)S(1)}, bf16[704,256]{1,0:T(8,128)(2,1)S(1)}, u32[]{:S(2)}, u32[]{:S(2)}) %collective-permute-start.41) | collective-permute-done | bytes 360480 | tf_op jit(solution)/shard_map/ppermute | solution.py:33
  212.9 7.2 %collective-permute-done.42.refs_1_ = bf16[704,256]{1,0:T(8,128)(2,1)S(1)} collective-permute-done((bf16[704,256]{1,0:T(8,128)(2,1)S(1)}, bf16[704,256]{1,0:T(8,128)(2,1)S(1)}, u32[]{:S(2)}, u32[]{:S(2)}) %collective-permute-start.42) | collective-permute-done | bytes 360480 | tf_op jit(solution)/shard_map/ppermute | solution.py:33
  225.0 2.9 %collective-permute-start.46 = (bf16[128,512]{1,0:T(8,128)(2,1)S(1)}, bf16[128,512]{1,0:T(8,128)(2,1)S(1)}, u32[]{:S(2)}, u32[]{:S(2)}) collective-permute-start(bf16[128,512]{1,0:T(8,128)(2,1)S(1)} %get-tuple-element.70), channel_id=1, source_target_pairs={{0,10},{1,11},{2,8},{3,9},{4,14},{5,15},{6,12},{7,13},{8,2},{9,3},... | collective-permute-start | bytes 393224 | tf_op jit(solution)/shard_map/ppermute | solution.py:33
  229.8 1.8 shard_map.118
  233.2 2.0 collective-permute-start.34
  238.1 11.9 %collective-permute-done.39.refs_6_ = bf16[128,512]{1,0:T(8,128)(2,1)S(1)} collective-permute-done((bf16[128,512]{1,0:T(8,128)(2,1)S(1)}, bf16[128,512]{1,0:T(8,128)(2,1)S(1)}, u32[]{:S(2)}, u32[]{:S(2)}) %collective-permute-start.39) | collective-permute-done | bytes 131104 | tf_op jit(solution)/shard_map/ppermute | solution.py:33
  (104 shorter events, 48.5 us)
Async XLA Ops:
  0.0 26.3 %collective-permute-start.8 = (bf16[256,2048]{1,0:T(8,128)(2,1)}, bf16[256,2048]{1,0:T(8,128)(2,1)S(1)}, u32[]{:S(2)}, u32[]{:S(2)}) collective-permute-start(bf16[256,2048]{1,0:T(8,128)(2,1)} %refs_4_.1), channel_id=1, source_target_pairs={{0,2},{1,3},{2,0},{3,1},{4,6},{5,7},{6,4},{7,5},{8,10},{9,11},{10,... | collective-permute-start | bytes 3145736 | tf_op jit(solution)/shard_map/ppermute | solution.py:33
  3.0 73.2 %collective-permute-start.7 = (bf16[256,2048]{1,0:T(8,128)(2,1)}, bf16[256,2048]{1,0:T(8,128)(2,1)S(1)}, u32[]{:S(2)}, u32[]{:S(2)}) collective-permute-start(bf16[256,2048]{1,0:T(8,128)(2,1)} %refs_4_.1), channel_id=1, source_target_pairs={{0,1},{1,0},{2,3},{3,2},{4,5},{5,4},{6,7},{7,6},{8,9},{9,8},{10,11... | collective-permute-start | bytes 3145736 | tf_op jit(solution)/shard_map/ppermute | solution.py:33
  26.3 49.8 %collective-permute-start.9 = (bf16[256,2048]{1,0:T(8,128)(2,1)S(1)}, bf16[256,2048]{1,0:T(8,128)(2,1)S(1)}, u32[]{:S(2)}, u32[]{:S(2)}) collective-permute-start(bf16[256,2048]{1,0:T(8,128)(2,1)S(1)} %collective-permute-done.8.refs_6_), channel_id=1, source_target_pairs={{0,1},{1,0},{2,3},{3,2},{4,5},{5,4},{6,7},{7,6},{8,9},{9,8},{10,11... | collective-permute-start | bytes 3145736 | tf_op jit(solution)/shard_map/ppermute | solution.py:33
  29.7 52.5 %collective-permute-start.17 = (bf16[128,1408]{1,0:T(8,128)(2,1)S(1)}, bf16[128,1408]{1,0:T(8,128)(2,1)S(1)}, u32[]{:S(2)}, u32[]{:S(2)}) collective-permute-start(bf16[128,1408]{1,0:T(8,128)(2,1)S(1)} %get-tuple-element.51), channel_id=1, source_target_pairs={{0,16},{4,20},{8,24},{12,28},{16,0},{20,4},{24,8},{28,12},{1,17},{... | collective-permute-start | bytes 1081352 | tf_op jit(solution)/shard_map/ppermute | solution.py:33
  51.3 20.5 %collective-permute-start.5 = (bf16[128,256]{1,0:T(8,128)(2,1)S(1)}, bf16[128,256]{1,0:T(8,128)(2,1)S(1)}, u32[]{:S(2)}, u32[]{:S(2)}) collective-permute-start(bf16[128,256]{1,0:T(8,128)(2,1)S(1)} %get-tuple-element.47), channel_id=1, source_target_pairs={{0,2},{1,3},{2,0},{3,1},{4,6},{5,7},{6,4},{7,5},{8,10},{9,11},{10,... | collective-permute-start | bytes 196616 | tf_op jit(solution)/shard_map/ppermute | solution.py:33
  56.1 35.3 %collective-permute-start.19 = (bf16[128,1408]{1,0:T(8,128)(2,1)S(1)}, bf16[128,1408]{1,0:T(8,128)(2,1)S(1)}, u32[]{:S(2)}, u32[]{:S(2)}) collective-permute-start(bf16[128,1408]{1,0:T(8,128)(2,1)S(1)} %get-tuple-element.52), channel_id=1, source_target_pairs={{0,16},{4,20},{8,24},{12,28},{16,0},{20,4},{24,8},{28,12},{1,17},{... | collective-permute-start | bytes 1081352 | tf_op jit(solution)/shard_map/ppermute | solution.py:33
  76.2 16.2 %collective-permute-start.21 = (bf16[128,1408]{1,0:T(8,128)(2,1)S(1)}, bf16[128,1408]{1,0:T(8,128)(2,1)S(1)}, u32[]{:S(2)}, u32[]{:S(2)}) collective-permute-start(bf16[128,1408]{1,0:T(8,128)(2,1)S(1)} %get-tuple-element.53), channel_id=1, source_target_pairs={{0,24},{4,28},{8,16},{12,20},{16,8},{20,12},{24,0},{28,4},{1,25},{... | collective-permute-start | bytes 1081352 | tf_op jit(solution)/shard_map/ppermute | solution.py:33
  80.1 44.2 %collective-permute-start.11 = (bf16[128,2048]{1,0:T(8,128)(2,1)S(1)}, bf16[128,2048]{1,0:T(8,128)(2,1)S(1)}, u32[]{:S(2)}, u32[]{:S(2)}) collective-permute-start(bf16[128,2048]{1,0:T(8,128)(2,1)S(1)} %get-tuple-element.50.refs_0_), channel_id=1, source_target_pairs={{0,8},{4,12},{8,0},{12,4},{16,24},{20,28},{24,16},{28,20},{1,9},{5... | collective-permute-start | bytes 1572872 | tf_op jit(solution)/shard_map/ppermute | solution.py:33
  80.5 52.9 %collective-permute-start.26 = (bf16[256,1408]{1,0:T(8,128)(2,1)S(1)}, bf16[256,1408]{1,0:T(8,128)(2,1)S(1)}, u32[]{:S(2)}, u32[]{:S(2)}) collective-permute-start(bf16[256,1408]{1,0:T(8,128)(2,1)S(1)} %get-tuple-element.56), channel_id=1, source_target_pairs={{0,8},{4,12},{8,0},{12,4},{16,24},{20,28},{24,16},{28,20},{1,9},{5... | collective-permute-start | bytes 2162696 | tf_op jit(solution)/shard_map/ppermute | solution.py:33
  82.2 41.6 %collective-permute-start.23 = (bf16[128,1408]{1,0:T(8,128)(2,1)S(1)}, bf16[128,1408]{1,0:T(8,128)(2,1)S(1)}, u32[]{:S(2)}, u32[]{:S(2)}) collective-permute-start(bf16[128,1408]{1,0:T(8,128)(2,1)S(1)} %get-tuple-element.54), channel_id=1, source_target_pairs={{0,24},{4,28},{8,16},{12,20},{16,8},{20,12},{24,0},{28,4},{1,25},{... | collective-permute-start | bytes 1081352 | tf_op jit(solution)/shard_map/ppermute | solution.py:33
  91.4 44.1 %collective-permute-start.25 = (bf16[256,1408]{1,0:T(8,128)(2,1)S(1)}, bf16[256,1408]{1,0:T(8,128)(2,1)S(1)}, u32[]{:S(2)}, u32[]{:S(2)}) collective-permute-start(bf16[256,1408]{1,0:T(8,128)(2,1)S(1)} %get-tuple-element.55.refs_8_), channel_id=1, source_target_pairs={{0,4},{4,0},{8,12},{12,8},{16,20},{20,16},{24,28},{28,24},{1,5},{5... | collective-permute-start | bytes 2162696 | tf_op jit(solution)/shard_map/ppermute | solution.py:33
  92.3 41.1 %collective-permute-start.29 = (bf16[704,256]{1,0:T(8,128)(2,1)S(1)}, bf16[704,256]{1,0:T(8,128)(2,1)S(1)}, u32[]{:S(2)}, u32[]{:S(2)}) collective-permute-start(bf16[704,256]{1,0:T(8,128)(2,1)S(1)} %get-tuple-element.58), channel_id=1, source_target_pairs={{0,8},{4,12},{8,0},{12,4},{16,24},{20,28},{24,16},{28,20},{1,9},{5... | collective-permute-start | bytes 1081352 | tf_op jit(solution)/shard_map/ppermute | solution.py:33
  123.7 14.8 %collective-permute-start.10 = (bf16[128,2048]{1,0:T(8,128)(2,1)S(1)}, bf16[128,2048]{1,0:T(8,128)(2,1)S(1)}, u32[]{:S(2)}, u32[]{:S(2)}) collective-permute-start(bf16[128,2048]{1,0:T(8,128)(2,1)S(1)} %get-tuple-element.50.refs_0_), channel_id=1, source_target_pairs={{0,2},{1,3},{2,0},{3,1},{4,6},{5,7},{6,4},{7,5},{8,10},{9,11},{10,... | collective-permute-start | bytes 1572872 | tf_op jit(solution)/shard_map/ppermute | solution.py:33
  124.3 23.0 %collective-permute-start.12 = (bf16[128,2048]{1,0:T(8,128)(2,1)S(1)}, bf16[128,2048]{1,0:T(8,128)(2,1)S(1)}, u32[]{:S(2)}, u32[]{:S(2)}) collective-permute-start(bf16[128,2048]{1,0:T(8,128)(2,1)S(1)} %collective-permute-done.11.refs_2_), channel_id=1, source_target_pairs={{0,2},{1,3},{2,0},{3,1},{4,6},{5,7},{6,4},{7,5},{8,10},{9,11},{10,... | collective-permute-start | bytes 1572872 | tf_op jit(solution)/shard_map/ppermute | solution.py:33
  133.4 25.8 %collective-permute-start.27 = (bf16[256,1408]{1,0:T(8,128)(2,1)S(1)}, bf16[256,1408]{1,0:T(8,128)(2,1)S(1)}, u32[]{:S(2)}, u32[]{:S(2)}) collective-permute-start(bf16[256,1408]{1,0:T(8,128)(2,1)S(1)} %collective-permute-done.26.refs_10_), channel_id=1, source_target_pairs={{0,4},{4,0},{8,12},{12,8},{16,20},{20,16},{24,28},{28,24},{1,5},{5... | collective-permute-start | bytes 2162696 | tf_op jit(solution)/shard_map/ppermute | solution.py:33
  135.5 24.1 %collective-permute-start.13 = (bf16[128,2048]{1,0:T(8,128)(2,1)S(1)}, bf16[128,2048]{1,0:T(8,128)(2,1)S(1)}, u32[]{:S(2)}, u32[]{:S(2)}) collective-permute-start(bf16[128,2048]{1,0:T(8,128)(2,1)S(1)} %get-tuple-element.50.refs_0_), channel_id=1, source_target_pairs={{0,1},{1,0},{2,3},{3,2},{4,5},{5,4},{6,7},{7,6},{8,9},{9,8},{10,11... | collective-permute-start | bytes 1572872 | tf_op jit(solution)/shard_map/ppermute | solution.py:33
  138.5 22.7 %collective-permute-start.14 = (bf16[128,2048]{1,0:T(8,128)(2,1)S(1)}, bf16[128,2048]{1,0:T(8,128)(2,1)S(1)}, u32[]{:S(2)}, u32[]{:S(2)}) collective-permute-start(bf16[128,2048]{1,0:T(8,128)(2,1)S(1)} %collective-permute-done.10.refs_1_), channel_id=1, source_target_pairs={{0,1},{1,0},{2,3},{3,2},{4,5},{5,4},{6,7},{7,6},{8,9},{9,8},{10,11... | collective-permute-start | bytes 1572872 | tf_op jit(solution)/shard_map/ppermute | solution.py:33
  144.7 16.8 %collective-permute-start.15 = (bf16[128,2048]{1,0:T(8,128)(2,1)S(1)}, bf16[128,2048]{1,0:T(8,128)(2,1)S(1)}, u32[]{:S(2)}, u32[]{:S(2)}) collective-permute-start(bf16[128,2048]{1,0:T(8,128)(2,1)S(1)} %collective-permute-done.11.refs_2_), channel_id=1, source_target_pairs={{0,1},{1,0},{2,3},{3,2},{4,5},{5,4},{6,7},{7,6},{8,9},{9,8},{10,11... | collective-permute-start | bytes 1572872 | tf_op jit(solution)/shard_map/ppermute | solution.py:33
  147.3 16.0 %collective-permute-start.16 = (bf16[128,2048]{1,0:T(8,128)(2,1)S(1)}, bf16[128,2048]{1,0:T(8,128)(2,1)S(1)}, u32[]{:S(2)}, u32[]{:S(2)}) collective-permute-start(bf16[128,2048]{1,0:T(8,128)(2,1)S(1)} %collective-permute-done.12.refs_3_), channel_id=1, source_target_pairs={{0,1},{1,0},{2,3},{3,2},{4,5},{5,4},{6,7},{7,6},{8,9},{9,8},{10,11... | collective-permute-start | bytes 1572872 | tf_op jit(solution)/shard_map/ppermute | solution.py:33
  159.5 18.7 %collective-permute-start.22 = (bf16[128,1408]{1,0:T(8,128)(2,1)S(1)}, bf16[128,1408]{1,0:T(8,128)(2,1)S(1)}, u32[]{:S(2)}, u32[]{:S(2)}) collective-permute-start(bf16[128,1408]{1,0:T(8,128)(2,1)S(1)} %collective-permute-done.21.refs_12_), channel_id=1, source_target_pairs={{0,4},{4,0},{8,12},{12,8},{16,20},{20,16},{24,28},{28,24},{1,5},{5... | collective-permute-start | bytes 1081352 | tf_op jit(solution)/shard_map/ppermute | solution.py:33
  161.3 24.7 %collective-permute-start.24 = (bf16[128,1408]{1,0:T(8,128)(2,1)S(1)}, bf16[128,1408]{1,0:T(8,128)(2,1)S(1)}, u32[]{:S(2)}, u32[]{:S(2)}) collective-permute-start(bf16[128,1408]{1,0:T(8,128)(2,1)S(1)} %collective-permute-done.23.refs_14_), channel_id=1, source_target_pairs={{0,4},{4,0},{8,12},{12,8},{16,20},{20,16},{24,28},{28,24},{1,5},{5... | collective-permute-start | bytes 1081352 | tf_op jit(solution)/shard_map/ppermute | solution.py:33
  161.5 32.1 %collective-permute-start.28 = (bf16[704,256]{1,0:T(8,128)(2,1)S(1)}, bf16[704,256]{1,0:T(8,128)(2,1)S(1)}, u32[]{:S(2)}, u32[]{:S(2)}) collective-permute-start(bf16[704,256]{1,0:T(8,128)(2,1)S(1)} %get-tuple-element.57.refs_0_), channel_id=1, source_target_pairs={{0,4},{4,0},{8,12},{12,8},{16,20},{20,16},{24,28},{28,24},{1,5},{5... | collective-permute-start | bytes 1081352 | tf_op jit(solution)/shard_map/ppermute | solution.py:33
  163.3 36.3 %collective-permute-start.30 = (bf16[704,256]{1,0:T(8,128)(2,1)S(1)}, bf16[704,256]{1,0:T(8,128)(2,1)S(1)}, u32[]{:S(2)}, u32[]{:S(2)}) collective-permute-start(bf16[704,256]{1,0:T(8,128)(2,1)S(1)} %collective-permute-done.29.refs_2_), channel_id=1, source_target_pairs={{0,4},{4,0},{8,12},{12,8},{16,20},{20,16},{24,28},{28,24},{1,5},{5... | collective-permute-start | bytes 1081352 | tf_op jit(solution)/shard_map/ppermute | solution.py:33
  170.5 31.0 %collective-permute-start.35 = (bf16[704,256]{1,0:T(8,128)(2,1)S(1)}, bf16[704,256]{1,0:T(8,128)(2,1)S(1)}, u32[]{:S(2)}, u32[]{:S(2)}) collective-permute-start(bf16[704,256]{1,0:T(8,128)(2,1)S(1)} %get-tuple-element.57.refs_0_), channel_id=1, source_target_pairs={{0,16},{4,20},{8,24},{12,28},{16,0},{20,4},{24,8},{28,12},{1,17},{... | collective-permute-start | bytes 1081352 | tf_op jit(solution)/shard_map/ppermute | solution.py:33
  178.2 23.9 %collective-permute-start.36 = (bf16[704,256]{1,0:T(8,128)(2,1)S(1)}, bf16[704,256]{1,0:T(8,128)(2,1)S(1)}, u32[]{:S(2)}, u32[]{:S(2)}) collective-permute-start(bf16[704,256]{1,0:T(8,128)(2,1)S(1)} %get-tuple-element.58), channel_id=1, source_target_pairs={{0,24},{4,28},{8,16},{12,20},{16,8},{20,12},{24,0},{28,4},{1,25},{... | collective-permute-start | bytes 1081352 | tf_op jit(solution)/shard_map/ppermute | solution.py:33
  201.4 28.4 %collective-permute-start.31 = (bf16[512,1024]{1,0:T(8,128)(2,1)S(1)}, bf16[512,1024]{1,0:T(8,128)(2,1)S(1)}, u32[]{:S(2)}, u32[]{:S(2)}) collective-permute-start(bf16[512,1024]{1,0:T(8,128)(2,1)S(1)} %shard_map.117), channel_id=1, source_target_pairs={{0,1},{1,0},{2,3},{3,2},{4,5},{5,4},{6,7},{7,6},{8,9},{9,8},{10,11... | collective-permute-start | bytes 3145736 | tf_op jit(solution)/shard_map/ppermute | solution.py:33
  202.1 17.9 %collective-permute-start.42 = (bf16[704,256]{1,0:T(8,128)(2,1)S(1)}, bf16[704,256]{1,0:T(8,128)(2,1)S(1)}, u32[]{:S(2)}, u32[]{:S(2)}) collective-permute-start(bf16[704,256]{1,0:T(8,128)(2,1)S(1)} %collective-permute-done.36.refs_1_), channel_id=1, source_target_pairs={{0,4},{4,0},{8,12},{12,8},{16,20},{20,16},{24,28},{28,24},{1,5},{5... | collective-permute-start | bytes 1081352 | tf_op jit(solution)/shard_map/ppermute | solution.py:33
  231.6 19.8 %collective-permute-start.32 = (bf16[128,1024]{1,0:T(8,128)(2,1)S(1)}, bf16[128,1024]{1,0:T(8,128)(2,1)S(1)}, u32[]{:S(2)}, u32[]{:S(2)}) collective-permute-start(bf16[128,1024]{1,0:T(8,128)(2,1)S(1)} %get-tuple-element.60), channel_id=1, source_target_pairs={{0,2},{1,3},{2,0},{3,1},{4,6},{5,7},{6,4},{7,5},{8,10},{9,11},{10,... | collective-permute-start | bytes 786440 | tf_op jit(solution)/shard_map/ppermute | solution.py:33
  233.2 18.2 %collective-permute-start.33 = (bf16[128,1024]{1,0:T(8,128)(2,1)S(1)}, bf16[128,1024]{1,0:T(8,128)(2,1)S(1)}, u32[]{:S(2)}, u32[]{:S(2)}) collective-permute-start(bf16[128,1024]{1,0:T(8,128)(2,1)S(1)} %get-tuple-element.61), channel_id=1, source_target_pairs={{0,8},{4,12},{8,0},{12,4},{16,24},{20,28},{24,16},{28,20},{1,9},{5... | collective-permute-start | bytes 786440 | tf_op jit(solution)/shard_map/ppermute | solution.py:33
  233.2 18.2 %collective-permute-start.34 = (bf16[128,1024]{1,0:T(8,128)(2,1)S(1)}, bf16[128,1024]{1,0:T(8,128)(2,1)S(1)}, u32[]{:S(2)}, u32[]{:S(2)}) collective-permute-start(bf16[128,1024]{1,0:T(8,128)(2,1)S(1)} %get-tuple-element.62), channel_id=1, source_target_pairs={{0,10},{1,11},{2,8},{3,9},{4,14},{5,15},{6,12},{7,13},{8,2},{9,3},... | collective-permute-start | bytes 786440 | tf_op jit(solution)/shard_map/ppermute | solution.py:33
  235.2 14.8 %collective-permute-start.39 = (bf16[128,512]{1,0:T(8,128)(2,1)S(1)}, bf16[128,512]{1,0:T(8,128)(2,1)S(1)}, u32[]{:S(2)}, u32[]{:S(2)}) collective-permute-start(bf16[128,512]{1,0:T(8,128)(2,1)S(1)} %get-tuple-element.65), channel_id=1, source_target_pairs={{0,8},{4,12},{8,0},{12,4},{16,24},{20,28},{24,16},{28,20},{1,9},{5... | collective-permute-start | bytes 393224 | tf_op jit(solution)/shard_map/ppermute | solution.py:33
  236.9 14.4 %collective-permute-start.40 = (bf16[128,512]{1,0:T(8,128)(2,1)S(1)}, bf16[128,512]{1,0:T(8,128)(2,1)S(1)}, u32[]{:S(2)}, u32[]{:S(2)}) collective-permute-start(bf16[128,512]{1,0:T(8,128)(2,1)S(1)} %get-tuple-element.66), channel_id=1, source_target_pairs={{0,10},{1,11},{2,8},{3,9},{4,14},{5,15},{6,12},{7,13},{8,2},{9,3},... | collective-permute-start | bytes 393224 | tf_op jit(solution)/shard_map/ppermute | solution.py:33
  (28 other events, 175.8 us)
